TPU v7x, 32 devices: a whole 2x2x4 slice. The times are simulated.
32 devices in a mesh: sp: 8 (over z, x), tp: 4 (over y, core).
Axes of the slice: x: 2, y: 2, z: 4, core: 2. Of those that a mesh axis runs over, the one named last changes fastest.
Arguments:
- out_grad: bfloat16 [1024, 2048], P('sp', 'tp'), may hold values from -6 to 6
- moe_input: bfloat16 [1024, 2048], P('sp', 'tp'), may hold values from -6 to 6
- route_weight: float32 [1024, 2], P('sp'), may hold values from 0.2 to 1
- route_ids: int32 [1024, 2], P('sp'), may hold values from 0 to 7, all different within a row; in each aligned block of 128 rows (0 to 127, 128 to 255, ...) at most 64 rows name the same one
- gate_proj: bfloat16 [8, 2048, 2816], P('sp', None, 'tp'), may hold values from -0.125 to 0.125
- up_proj: bfloat16 [8, 2048, 2816], P('sp', None, 'tp'), may hold values from -0.125 to 0.125
- down_proj: bfloat16 [8, 2816, 2048], P('sp', 'tp'), may hold values from -0.109375 to 0.109375
- out_proj: bfloat16 [2048, 2048], P(None, 'tp'), may hold values from -0.125 to 0.125
- conv_out: bfloat16 [1024, 2048], P('sp', 'tp'), may hold values from -6 to 6
- gate_b: bfloat16 [1024, 2048], P('sp', 'tp'), may hold values from -6 to 6
- gate_c: bfloat16 [1024, 2048], P('sp', 'tp'), may hold values from -6 to 6
- value_v: bfloat16 [1024, 2048], P('sp', 'tp'), may hold values from -6 to 6
- conv_taps: float32 [3, 2048], P(None, 'tp'), may hold values from -3 to 3
Outputs:
- grad_gate: bfloat16 [8, 2048, 2816], P('sp', None, 'tp')
- grad_up: bfloat16 [8, 2048, 2816], P('sp', None, 'tp')
- grad_down: bfloat16 [8, 2816, 2048], P('sp', 'tp')
- grad_out: float32 [2048, 2048], P('sp', 'tp')
- grad_b: bfloat16 [1024, 2048], P('sp', 'tp')
- grad_c: bfloat16 [1024, 2048], P('sp', 'tp')
- grad_v: bfloat16 [1024, 2048], P('sp', 'tp')
Inputs may be any that keep to these rules, and one draw needn't show every extreme that they name: `route_ids`: each row names two different experts; within the 128 rows of one index of sp no expert is named by more than 64 rows, a bound that some block reaches.
All inputs are finite; a program needn't handle non-finite values.
Results may differ from a plain program's by a relative error of at most 0.019.
Values may be sent and summed in bfloat16 or wider, within the bound.
No kernel may reach another device: no remote copies, remote signals or barrier semaphores. Data moves between devices by JAX's collectives and lax.ppermute only.
A program may use at most 64 MiB of HBM per device.

v0:
```python
import functools
import math

import jax
import jax.numpy as jnp
from jax import lax
from jax.experimental import pallas as pl
from jax.experimental.pallas import tpu as pltpu
from jax.sharding import PartitionSpec as P


EXPERT_MIB, GRAD_MIB = 16, 14
BF = jnp.bfloat16
F32 = jnp.float32
VMEM = pl.BlockSpec(memory_space=pltpu.VMEM)
SMEM = pl.BlockSpec(memory_space=pltpu.SMEM)
HBM = pl.BlockSpec(memory_space=pltpu.HBM)


def call(body, outs, args, smem=1, flops=0, scratch=(), vmem=8, hbm=()):
    args = [
        pltpu.with_memory_space_constraint(a, pltpu.HBM) if i in hbm else a
        for i, a in enumerate(args)
    ]
    moved = sum(a.size * a.dtype.itemsize for a in args) + sum(
        math.prod(o.shape) * o.dtype.itemsize for o in outs
    )
    return pl.pallas_call(
        body,
        out_shape=tuple(outs),
        in_specs=[SMEM if i < smem else HBM if i in hbm else VMEM for i in range(len(args))],
        out_specs=tuple([VMEM] * len(outs)),
        scratch_shapes=list(scratch),
        cost_estimate=pl.CostEstimate(flops=flops, transcendentals=0, bytes_accessed=moved),
        compiler_params=pltpu.CompilerParams(vmem_limit_bytes=vmem * 1024 * 1024),
    )(*args)


def shape(dims, dtype=BF):
    return jax.ShapeDtypeStruct(dims, dtype)


def nt(a, b):
    return lax.dot_general(a, b, (((1,), (1,)), ((), ())), preferred_element_type=F32)


def tn(a, b):
    return lax.dot_general(a, b, (((0,), (0,)), ((), ())), preferred_element_type=F32)


def routing(n_sp, nx, z, x, ids, wts):
    nz = n_sp // nx
    tok = ids.shape[1]
    first = lax.broadcasted_iota(jnp.int32, (n_sp, tok), 0)
    rz, rx = first // nx, first % nx
    zz, xx = rz + z, rx + x
    zz = jnp.where(zz >= nz, zz - nz, zz)
    xx = jnp.where(xx >= nx, xx - nx, xx)
    expert = zz * nx + xx
    hit0, hit1 = ids[0:1, :] == expert, ids[1:2, :] == expert
    named = jnp.where(hit0 | hit1, 1.0, 0.0)
    weight = 0.0
    if wts is not None:
        weight = jnp.where(hit0, wts[0:1, :], 0.0) + jnp.where(hit1, wts[1:2, :], 0.0)
    earlier = (
        lax.broadcasted_iota(jnp.int32, (tok, tok), 0)
        < lax.broadcasted_iota(jnp.int32, (tok, tok), 1)
    )
    before = jnp.dot(
        named.astype(BF), jnp.where(earlier, 1.0, 0.0).astype(BF), preferred_element_type=F32
    )
    return jnp.where(named > 0.5, before, -1.0), weight


def select_body(n_sp, nx, cap, me_ref, ids_ref, sel_ref):
    slot, _ = routing(n_sp, nx, me_ref[0], me_ref[1], ids_ref[...], None)
    place = lax.broadcasted_iota(jnp.int32, (cap, slot.shape[1]), 0).astype(F32)
    for r in range(n_sp):
        take = jnp.where(slot[r : r + 1, :] == place, 1.0, 0.0)
        sel_ref[r * cap : (r + 1) * cap, :] = take.astype(BF)


def dispatch_body(n_sp, nx, cap, me_ref, *refs):
    far, outs, near, sems = refs[:4], refs[4 : 4 + n_sp], refs[4 + n_sp : 8 + n_sp], refs[-1]
    copies = [pltpu.make_async_copy(f, n, sems.at[i]) for i, (f, n) in enumerate(zip(far, near))]
    for copy in copies:
        copy.start()
    for copy in copies:
        copy.wait()
    ids_ref, w_ref, x_ref, og_ref = near
    slot, weight = routing(n_sp, nx, me_ref[0], me_ref[1], ids_ref[...], w_ref[...])
    tok = x_ref.shape[0]
    place = lax.broadcasted_iota(jnp.int32, (cap, tok), 0).astype(F32)
    xv, og = x_ref[...], og_ref[...]
    for r in range(n_sp):
        take = jnp.where(slot[r : r + 1, :] == place, 1.0, 0.0)
        scale = jnp.sum(take * weight[r : r + 1, :], axis=1, keepdims=True)
        take = take.astype(BF)
        outs[r][:cap, :] = jnp.dot(take, xv, preferred_element_type=F32).astype(BF)
        outs[r][cap:, :] = (scale * jnp.dot(take, og, preferred_element_type=F32)).astype(BF)


def rows_of(refs, cap, which):
    return jnp.concatenate(
        [
            ref[at + which * cap : at + (which + 1) * cap, :]
            for ref in refs
            for at in range(0, ref.shape[0], 2 * cap)
        ],
        axis=0,
    )


def load_body(wg, wu, wd, wg_out, wu_out, wd_out, sems):
    pairs = [(wg, wg_out), (wu, wu_out), (wd, wd_out)]
    half = wg.shape[0] // 16 * 8
    rows = wg.shape[0]
    copies = []
    for i, (f, n) in enumerate(pairs):
        for j, (lo, hi) in enumerate(((0, half), (half, rows))):
            copies.append(
                pltpu.make_async_copy(f.at[lo:hi, :], n.at[lo:hi, :], sems.at[2 * i + j])
            )
    for copy in copies:
        copy.start()
    for copy in copies:
        copy.wait()


def mix_body(gb, co, mixed_ref, gb_near, co_near, sems):
    copies = [
        pltpu.make_async_copy(gb, gb_near, sems.at[0]),
        pltpu.make_async_copy(co, co_near, sems.at[1]),
    ]
    for copy in copies:
        copy.start()
    for copy in copies:
        copy.wait()
    mixed_ref[...] = (gb_near[...].astype(F32) * co_near[...].astype(F32)).astype(BF)


def expert_body(n_b, n_g, cap, blk_ref, dst_ref, *refs):
    blocks, refs = refs[: n_b * n_g], refs[n_b * n_g :]
    wg, wu, wd, hid_ref, dg_ref, du_ref = refs[:6]
    outs = refs[6:]
    ch = blocks[0].shape[1]
    gate = up = dhid = None
    for b in range(n_b):
        cols = pl.ds(pl.multiple_of(blk_ref[b] * ch, ch), ch)
        xb, dyb = rows_of(blocks[b::n_b], cap, 0), rows_of(blocks[b::n_b], cap, 1)
        g, u, d = nt(xb, wg[:, cols]), nt(xb, wu[:, cols]), nt(dyb, wd[:, cols])
        gate = g if gate is None else gate + g
        up = u if up is None else up + u
        dhid = d if dhid is None else dhid + d
    sig = jax.nn.sigmoid(gate)
    act = gate * sig
    hid_ref[...] = (act * up).astype(BF)
    dg = (dhid * up * (sig * (1.0 + gate * (1.0 - sig)))).astype(BF)
    du = (dhid * act).astype(BF)
    dg_ref[...] = dg
    du_ref[...] = du
    for b in range(n_b):
        cols = pl.ds(pl.multiple_of(dst_ref[b] * ch, ch), ch)
        part = jnp.dot(dg, wg[:, cols], preferred_element_type=F32) + jnp.dot(
            du, wu[:, cols], preferred_element_type=F32
        )
        outs[b][...] = part.astype(BF)


def weight_grad_body(n_c, n_b, cap, which, blk_ref, *refs):
    lefts, rights, out = refs[:n_c], refs[n_c:-1], refs[-1]
    ch = rights[0].shape[1]
    held = jnp.concatenate([l[...] for l in lefts], axis=0).T
    for b in range(n_b):
        total = jnp.dot(held, rows_of(rights[b::n_b], cap, which), preferred_element_type=F32)
        out[:, pl.ds(pl.multiple_of(blk_ref[b] * ch, ch), ch)] = total.astype(BF)


def add_body(n_out, *refs):
    ins, outs = refs[:-n_out], refs[-n_out:]
    for i in range(n_out):
        outs[i][...] = (ins[2 * i][...].astype(F32) + ins[2 * i + 1][...].astype(F32)).astype(BF)


def sum_split_body(n_in, *refs):
    ins, outs = refs[:n_in], refs[n_in:]
    rows = outs[0].shape[0]
    for i, out in enumerate(outs):
        total = None
        for ref in ins:
            v = ref[i * rows : (i + 1) * rows, :].astype(F32)
            total = v if total is None else total + v
        out[...] = total.astype(BF)


def combine_body(n_sp, sel_ref, og_ref, *refs):
    backs, dh_ref = refs[:n_sp], refs[n_sp]
    rows = jnp.concatenate([b[...] for b in backs], axis=0) if n_sp > 1 else backs[0][...]
    moe = tn(sel_ref[...], rows)
    dh_ref[...] = (og_ref[...].astype(F32) + moe).astype(BF)


def spread_body(n_b, n_sp, blk_ref, tgt_ref, *refs):
    blocks, full_ref, outs = refs[:n_b], refs[n_b], refs[n_b + 1 :]
    ch = blocks[0].shape[1]
    for b in range(n_b):
        full_ref[:, pl.ds(pl.multiple_of(blk_ref[b] * ch, ch), ch)] = blocks[b][...]
    rows, w = full_ref.shape[0], outs[0].shape[1]
    nx, lane = len(outs), 128
    for r in range(n_sp):
        out = outs[r % nx].at[r // nx * rows : (r // nx + 1) * rows, :]
        if w % lane == 0:
            out[...] = full_ref[:, pl.ds(pl.multiple_of(tgt_ref[r] * w, lane), w)]
            continue
        fold = lane // w
        wide = full_ref[:, pl.ds(pl.multiple_of(tgt_ref[r] // fold * lane, lane), lane)]
        piece = wide[:, :w]
        for i in range(1, fold):
            piece = jnp.where(tgt_ref[r] % fold == i, wide[:, i * w : (i + 1) * w], piece)
        out[...] = piece


def regroup_body(nx, *refs):
    ins, outs = refs[:nx], refs[nx:]
    rows = outs[0].shape[0] // nx
    for rz, out in enumerate(outs):
        for rx, ref in enumerate(ins):
            out[rx * rows : (rx + 1) * rows, :] = ref[rz * rows : (rz + 1) * rows, :]


def mixer_body(full_ref, wo_ref, gb_ref, co_ref, dconv_ref, grad_b_ref, first_ref, last_ref):
    dz = jnp.dot(full_ref[...], wo_ref[...], preferred_element_type=F32)
    dconv = (dz * gb_ref[...].astype(F32)).astype(BF)
    dconv_ref[...] = dconv
    grad_b_ref[...] = (dz * co_ref[...].astype(F32)).astype(BF)
    rows = dconv.shape[0]
    first_ref[...] = dconv[0:1, :]
    last_ref[...] = dconv[rows - 1 : rows, :]


def conv_body(dconv_ref, low_ref, high_ref, taps_ref, v_ref, c_ref, gc_ref, gv_ref):
    mid = dconv_ref[...].astype(F32)
    rows = mid.shape[0]
    at = lax.broadcasted_iota(jnp.int32, mid.shape, 0)
    prev = jnp.where(at == 0, low_ref[...].astype(F32), pltpu.roll(mid, 1, 0))
    succ = jnp.where(at == rows - 1, high_ref[...].astype(F32), pltpu.roll(mid, rows - 1, 0))
    taps = taps_ref[...]
    du = taps[0:1, :] * succ + taps[1:2, :] * mid + taps[2:3, :] * prev
    gc_ref[...] = (du * v_ref[...].astype(F32)).astype(BF)
    gv_ref[...] = (du * c_ref[...].astype(F32)).astype(BF)


def grad_out_body(nz, *refs):
    lefts, rights, out = refs[:nz], refs[nz:-1], refs[-1]
    left = jnp.concatenate([l[...] for l in lefts], axis=0)
    right = jnp.concatenate([r[...] for r in rights], axis=0)
    out[...] = tn(left, right)


def grid(n_sp, n_tp):
    ny = n_tp // 2
    nx = ny if n_sp % ny == 0 else 1
    return n_sp // nx, nx, ny


def local(
    out_grad,
    moe_input,
    route_weight,
    route_ids,
    gate_proj,
    up_proj,
    down_proj,
    out_proj,
    conv_out,
    gate_b,
    gate_c,
    value_v,
    conv_taps,
):
    tok, ch = out_grad.shape
    n_sp, n_tp = lax.axis_size("sp"), lax.axis_size("tp")
    cap = 4 * tok // n_sp
    nz, nx, ny = grid(n_sp, n_tp)
    me, mt = lax.axis_index("sp"), lax.axis_index("tp")
    z, x, y, c = me // nx, me % nx, mt // 2, mt % 2
    i32 = functools.partial(jnp.asarray, dtype=jnp.int32)

    def sp_perm(rz, rx):
        return [
            (i, ((i // nx + rz) % nz) * nx + (i % nx + rx) % nx) for i in range(n_sp)
        ]

    def send_sp(v, rz, rx):
        if rz % nz == 0 and rx % nx == 0:
            return v
        return lax.ppermute(v, "sp", sp_perm(rz, rx))

    def send_y(v, jy):
        return lax.ppermute(v, "tp", [(k, ((k // 2 + jy) % ny) * 2 + k % 2) for k in range(n_tp)])

    def send_core(v):
        return lax.ppermute(v, "tp", [(k, k ^ 1) for k in range(n_tp)])

    def gather_tp(v):
        blocks = []
        for jy in range(ny):
            b = send_y(v, jy) if jy else v
            blocks += [b, send_core(b)]
        return blocks

    rel = [(rz, rx) for rz in range(nz) for rx in range(nx)]
    blk = i32([0]) + jnp.stack(
        [((y - jy) % ny) * 2 + (c + cc) % 2 for jy in range(ny) for cc in range(2)]
    ).astype(jnp.int32)
    dst = jnp.stack(
        [((y + jy) % ny) * 2 + (c + cc) % 2 for jy in range(ny) for cc in range(2)]
    ).astype(jnp.int32)
    tgt = jnp.stack([((z + rz) % nz) * nx + (x + rx) % nx for rz, rx in rel]).astype(jnp.int32)

    near = [
        pltpu.VMEM((2, tok), jnp.int32), pltpu.VMEM((2, tok), F32),
        pltpu.VMEM((tok, ch), BF), pltpu.VMEM((tok, ch), BF), pltpu.SemaphoreType.DMA((4,)),
    ]
    at = jnp.stack([z, x]).astype(jnp.int32)
    sent = call(
        functools.partial(dispatch_body, n_sp, nx, cap),
        [shape((2 * cap, ch))] * n_sp,
        [at, route_ids.T, route_weight.T, moe_input, out_grad],
        flops=4 * n_sp * cap * tok * ch, scratch=near, hbm=(1, 2, 3, 4),
    )
    groups = []
    for rz in range(nz):
        got = [send_sp(sent[rz * nx + rx], rz, rx) for rx in range(nx)]
        groups.append(gather_tp(jnp.concatenate(got, axis=0)))

    ff = down_proj.shape[1]
    weights = [gate_proj[0].T, up_proj[0].T, down_proj[0]]
    mixed = call(
        mix_body, [shape((tok, ch))], [gate_b, conv_out], smem=0, hbm=range(2),
        flops=tok * ch,
        scratch=[pltpu.VMEM((tok, ch), BF)] * 2 + [pltpu.SemaphoreType.DMA((2,))],
    )[0]
    weights = call(
        load_body, [shape((ff, ch * n_tp))] * 3, weights, smem=0, hbm=range(3),
        scratch=[pltpu.SemaphoreType.DMA((6,))],
    )
    row = jnp.concatenate([send_sp(mixed, 0, rx) for rx in range(nx)], axis=0)
    mixed_all = [row]
    for _ in range(1, nz):
        row = send_sp(row, 1, 0)
        mixed_all.append(row)

    n_c = 2 if nz % 2 == 0 else 1
    gpc, per = nz // n_c, n_sp // n_c
    rows = per * cap
    hid, dgs, dus, backs = [], [], [], []
    for g in range(n_c):
        outs = call(
            functools.partial(expert_body, n_tp, gpc, cap),
            [shape((rows, ff))] * 3 + [shape((rows, ch))] * n_tp,
            [blk, dst, *[b for group in groups[g * gpc : (g + 1) * gpc] for b in group],
             *weights],
            smem=2, vmem=EXPERT_MIB,
            flops=10 * rows * ff * ch * n_tp,
        )
        blk = lax.optimization_barrier((blk, outs[0]))[0]
        hid.append(outs[0])
        dgs.append(outs[1])
        dus.append(outs[2])
        parts = outs[3:]
        theirs = [send_core(parts[2 * jy + 1]) for jy in range(ny)]
        pairs = [v for jy in range(ny) for v in (parts[2 * jy], theirs[jy])]
        summed = call(
            functools.partial(add_body, ny), [shape((rows, ch))] * ny, pairs, smem=0,
            flops=ny * rows * ch,
        )
        arrived = [summed[0]] + [send_y(summed[jy], jy) for jy in range(1, ny)]
        pieces = call(
            functools.partial(sum_split_body, ny), [shape((cap, ch))] * per, arrived,
            smem=0, flops=ny * rows * ch,
        )
        for i, (rz, rx) in enumerate(rel[g * per : (g + 1) * per]):
            backs.append(send_sp(pieces[i], -rz, -rx))

    def weight_grad(lefts, which):
        return call(
            functools.partial(weight_grad_body, n_c, n_tp, cap, which),
            [shape((ff, ch * n_tp))],
            [blk, *lefts, *[b for group in groups for b in group]],
            flops=2 * n_sp * cap * ff * ch * n_tp, vmem=GRAD_MIB,
        )[0]

    grad_down = weight_grad(hid, 1)
    grad_gate = weight_grad(dgs, 0)
    grad_up = weight_grad(dus, 0)
    *backs, grad_down, grad_gate, grad_up = lax.optimization_barrier(
        (*backs, grad_down, grad_gate, grad_up)
    )
    grad_gate, grad_up = grad_gate.T, grad_up.T

    sel = call(
        functools.partial(select_body, n_sp, nx, cap), [shape((n_sp * cap, tok))],
        [at, route_ids.T], flops=2 * n_sp * cap * tok * tok,
    )[0]
    dh = call(
        functools.partial(combine_body, n_sp), [shape((tok, ch))],
        [sel, out_grad, *backs], smem=0, flops=2 * n_sp * cap * tok * ch,
    )[0]
    dh_blocks = gather_tp(dh)
    width = ch * n_tp // n_sp
    outs = call(
        functools.partial(spread_body, n_tp, n_sp),
        [shape((tok, ch * n_tp))] + [shape((nz * tok, width))] * nx,
        [blk, tgt, *dh_blocks], smem=2, flops=tok * ch * n_tp,
    )
    full_h, slices = outs[0], outs[1:]
    slices = [send_sp(slices[rx], 0, rx) for rx in range(nx)]
    slices = call(
        functools.partial(regroup_body, nx), [shape((nx * tok, width))] * nz, slices,
        smem=0, flops=tok * width,
    )
    dh_all = [send_sp(slices[rz], rz, 0) for rz in range(nz)]

    dconv, grad_b, first, last = call(
        mixer_body, [shape((tok, ch)), shape((tok, ch)), shape((1, ch)), shape((1, ch))],
        [full_h, out_proj, gate_b, conv_out], smem=0, flops=2 * tok * ch * ch * n_tp,
    )
    up_pairs = [(i, i + 1) for i in range(n_sp - 1)]
    low = lax.ppermute(last, "sp", up_pairs)
    high = lax.ppermute(first, "sp", [(b, a) for a, b in up_pairs])
    grad_c, grad_v = call(
        conv_body, [shape((tok, ch))] * 2,
        [dconv, low, high, conv_taps, value_v, gate_c], smem=0, flops=8 * tok * ch,
    )
    grad_out = call(
        functools.partial(grad_out_body, nz), [shape((width, ch), F32)],
        [*dh_all, *mixed_all], smem=0, flops=2 * n_sp * tok * width * ch,
    )[0]
    return (grad_gate[None], grad_up[None], grad_down[None], grad_out, grad_b, grad_c, grad_v)


def solution(mesh):
    in_specs = (
        P("sp", "tp"),
        P("sp", "tp"),
        P("sp", None),
        P("sp", None),
        P("sp", None, "tp"),
        P("sp", None, "tp"),
        P("sp", "tp", None),
        P(None, "tp"),
        P("sp", "tp"),
        P("sp", "tp"),
        P("sp", "tp"),
        P("sp", "tp"),
        P(None, "tp"),
    )
    out_specs = (
        P("sp", None, "tp"),
        P("sp", None, "tp"),
        P("sp", "tp", None),
        P("sp", "tp"),
        P("sp", "tp"),
        P("sp", "tp"),
        P("sp", "tp"),
    )
    return jax.shard_map(local, mesh=mesh, in_specs=in_specs, out_specs=out_specs, check_vma=False)
```

profile of v0, /device:TPU:0, one launch (start us, length us, event | category | flops | bytes accessed | tf_op | source)
XLA Modules:
  0.0 139.3 jit_solution(10224969765548809633)
XLA Ops:
  0.7 2.1 %shard_map.189 = (bf16[128,512]{1,0:T(8,128)(2,1)S(1)}, bf16[128,512]{1,0:T(8,128)(2,1)S(1)}, bf16[128,512]{1,0:T(8,128)(2,1)S(1)}, bf16[128,512]{1,0:T(8,128)(2...) custom-call(s32[2]{0:T(128)S(1)} %pad_add_fusion.3.me_ref, ...), custom_call_target="tpu_custom_call" | custom-call | flops 134217728 | bytes 1312776 | tf_op jit(solution)/shard_map/pallas_call | solution.py:28
  2.9 3.1 %collective-permute-start.4 = (bf16[128,512]{1,0:T(8,128)(2,1)S(1)}, bf16[128,512]{1,0:T(8,128)(2,1)S(1)}, u32[]{:S(2)}, u32[]{:S(2)}) collective-permute-start(bf16[128,512]{1,0:T(8,128)(2,1)S(1)} %get-tuple-element.72), channel_id=1, source_target_pairs={{0,8},{4,12},{8,16},{12,20},{16,24},{20,28},{24,0},{28,4},{1,9},{5... | collective-permute-start | bytes 393224 | tf_op jit(solution)/shard_map/ppermute | solution.py:297
  6.0 1.5 %collective-permute-start = (bf16[128,512]{1,0:T(8,128)(2,1)S(1)}, bf16[128,512]{1,0:T(8,128)(2,1)S(1)}, u32[]{:S(2)}, u32[]{:S(2)}) collective-permute-start(bf16[128,512]{1,0:T(8,128)(2,1)S(1)} %get-tuple-element.71), channel_id=1, source_target_pairs={{0,4},{4,0},{8,12},{12,8},{16,20},{20,16},{24,28},{28,24},{1,5},{5... | collective-permute-start | bytes 393224 | tf_op jit(solution)/shard_map/ppermute | solution.py:297
  7.5 1.5 %collective-permute-start.5 = (bf16[128,512]{1,0:T(8,128)(2,1)S(1)}, bf16[128,512]{1,0:T(8,128)(2,1)S(1)}, u32[]{:S(2)}, u32[]{:S(2)}) collective-permute-start(bf16[128,512]{1,0:T(8,128)(2,1)S(1)} %get-tuple-element.73), channel_id=1, source_target_pairs={{0,12},{4,8},{8,20},{12,16},{16,28},{20,24},{24,4},{28,0},{1,13},{... | collective-permute-start | bytes 393224 | tf_op jit(solution)/shard_map/ppermute | solution.py:297
  9.0 1.1 collective-permute-start.15
  10.1 2.8 %collective-permute-start.16 = (bf16[128,512]{1,0:T(8,128)(2,1)S(1)}, bf16[128,512]{1,0:T(8,128)(2,1)S(1)}, u32[]{:S(2)}, u32[]{:S(2)}) collective-permute-start(bf16[128,512]{1,0:T(8,128)(2,1)S(1)} %get-tuple-element.90), channel_id=1, source_target_pairs={{0,20},{4,16},{8,28},{12,24},{16,4},{20,0},{24,12},{28,8},{1,21},{... | collective-permute-start | bytes 393224 | tf_op jit(solution)/shard_map/ppermute | solution.py:297
  12.9 2.3 %collective-permute-start.20 = (bf16[128,512]{1,0:T(8,128)(2,1)S(1)}, bf16[128,512]{1,0:T(8,128)(2,1)S(1)}, u32[]{:S(2)}, u32[]{:S(2)}) collective-permute-start(bf16[128,512]{1,0:T(8,128)(2,1)S(1)} %get-tuple-element.91), channel_id=1, source_target_pairs={{0,24},{4,28},{8,0},{12,4},{16,8},{20,12},{24,16},{28,20},{1,25},{... | collective-permute-start | bytes 393224 | tf_op jit(solution)/shard_map/ppermute | solution.py:297
  15.2 0.9 collective-permute-start.21
  16.1 6.8 %collective-permute-done.15 = bf16[128,512]{1,0:T(8,128)(2,1)S(1)} collective-permute-done((bf16[128,512]{1,0:T(8,128)(2,1)S(1)}, bf16[128,512]{1,0:T(8,128)(2,1)S(1)}, u32[]{:S(2)}, u32[]{:S(2)}) %collective-permute-start.15) | collective-permute-done | bytes 131104 | tf_op jit(solution)/shard_map/ppermute | solution.py:297
  23.0 1.6 %collective-permute-start.2 = (bf16[256,512]{1,0:T(8,128)(2,1)S(1)}, bf16[256,512]{1,0:T(8,128)(2,1)S(1)}, u32[]{:S(2)}, u32[]{:S(2)}) collective-permute-start(bf16[256,512]{1,0:T(8,128)(2,1)S(1)} %constant_dynamic-update-slice_fusion.refs_0_.refs_2_), channel_id=1, source_target_pairs={{0,2},{1,3},{2,0},{3,1},{4,6},{5,7},{6,4},{7,5},{8,10},{9,11},{10,... | collective-permute-start | bytes 786440 | tf_op jit(solution)/shard_map/ppermute | solution.py:300
  24.6 0.6 collective-permute-start.7
  25.2 1.5 %collective-permute-done.16 = bf16[128,512]{1,0:T(8,128)(2,1)S(1)} collective-permute-done((bf16[128,512]{1,0:T(8,128)(2,1)S(1)}, bf16[128,512]{1,0:T(8,128)(2,1)S(1)}, u32[]{:S(2)}, u32[]{:S(2)}) %collective-permute-start.16) | collective-permute-done | bytes 131104 | tf_op jit(solution)/shard_map/ppermute | solution.py:297
  26.6 1.6 %collective-permute-start.18 = (bf16[256,512]{1,0:T(8,128)(2,1)S(1)}, bf16[256,512]{1,0:T(8,128)(2,1)S(1)}, u32[]{:S(2)}, u32[]{:S(2)}) collective-permute-start(bf16[256,512]{1,0:T(8,128)(2,1)S(1)} %constant_dynamic-update-slice_fusion.4.refs_0_.refs_10_), channel_id=1, source_target_pairs={{0,2},{1,3},{2,0},{3,1},{4,6},{5,7},{6,4},{7,5},{8,10},{9,11},{10,... | collective-permute-start | bytes 786440 | tf_op jit(solution)/shard_map/ppermute | solution.py:300
  28.2 0.6 collective-permute-start.23
  28.8 3.4 %collective-permute-done.2.refs_2_.refs_4_ = bf16[256,512]{1,0:T(8,128)(2,1)S(1)} collective-permute-done((bf16[256,512]{1,0:T(8,128)(2,1)S(1)}, bf16[256,512]{1,0:T(8,128)(2,1)S(1)}, u32[]{:S(2)}, u32[]{:S(2)}) %collective-permute-start.2) | collective-permute-done | bytes 262176 | tf_op jit(solution)/shard_map/ppermute | solution.py:300
  32.2 5.6 %collective-permute-done.7.refs_6_.refs_8_ = bf16[256,512]{1,0:T(8,128)(2,1)S(1)} collective-permute-done((bf16[256,512]{1,0:T(8,128)(2,1)S(1)}, bf16[256,512]{1,0:T(8,128)(2,1)S(1)}, u32[]{:S(2)}, u32[]{:S(2)}) %collective-permute-start.7) | collective-permute-done | bytes 262176 | tf_op jit(solution)/shard_map/ppermute | solution.py:300
  37.8 3.6 %shard_map.190 = (bf16[704,2048]{1,0:T(8,128)(2,1)S(1)}, bf16[704,2048]{1,0:T(8,128)(2,1)S(1)}, bf16[704,2048]{1,0:T(8,128)(2,1)S(1)}) custom-call(bf16[704,2048]{1,0:T(8,128)(2,1)} %bitcast.34, bf16[704,2048]{1,0:T(8,128)(2,1)} %bitcast.35, bf16[704,2048]{1,0:T(8,128)(2,1)} %bitcast.36), custom_call_target="tpu_custom_call" | custom-call | bytes 17301504 | tf_op jit(solution)/shard_map/pallas_call | solution.py:28
  41.5 0.5 collective-permute-start.17
  42.1 1.4 collective-permute-done.18.refs_2_.refs_12_
  43.4 5.2 %collective-permute-done.23.refs_6_.refs_16_ = bf16[256,512]{1,0:T(8,128)(2,1)S(1)} collective-permute-done((bf16[256,512]{1,0:T(8,128)(2,1)S(1)}, bf16[256,512]{1,0:T(8,128)(2,1)S(1)}, u32[]{:S(2)}, u32[]{:S(2)}) %collective-permute-start.23) | collective-permute-done | bytes 262176 | tf_op jit(solution)/shard_map/ppermute | solution.py:300
  48.6 0.5 collective-permute-start.24
  49.1 5.0 %shard_map.191 = (bf16[256,704]{1,0:T(8,128)(2,1)S(1)}, bf16[256,704]{1,0:T(8,128)(2,1)S(1)}, bf16[256,704]{1,0:T(8,128)(2,1)S(1)}, bf16[256,512]{1,0:T(8,128)(2...) custom-call(s32[4]{0:T(128)S(1)} %pad_add_fusion.blk_ref, ...), custom_call_target="tpu_custom_call" | custom-call | flops 3690987520 | bytes 12877856 | tf_op jit(solution)/shard_map/pallas_call | solution.py:28
  54.7 5.0 %shard_map.194 = (bf16[256,704]{1,0:T(8,128)(2,1)S(1)}, bf16[256,704]{1,0:T(8,128)(2,1)S(1)}, bf16[256,704]{1,0:T(8,128)(2,1)S(1)}, bf16[256,512]{1,0:T(8,128)(2...) custom-call(s32[4]{0:T(128)S(1)} %pad_add_fusion.blk_ref, ...), custom_call_target="tpu_custom_call" | custom-call | flops 3690987520 | bytes 12877856 | tf_op jit(solution)/shard_map/pallas_call | solution.py:28
  60.3 1.0 shard_map.204
  61.3 1.6 %collective-permute-start.39 = (bf16[128,512]{1,0:T(8,128)(2,1)S(1)}, bf16[128,512]{1,0:T(8,128)(2,1)S(1)}, u32[]{:S(2)}, u32[]{:S(2)}) collective-permute-start(bf16[128,512]{1,0:T(8,128)(2,1)S(1)} %shard_map.204), channel_id=1, source_target_pairs={{0,4},{4,0},{8,12},{12,8},{16,20},{20,16},{24,28},{28,24},{1,5},{5... | collective-permute-start | bytes 393224 | tf_op jit(solution)/shard_map/ppermute | solution.py:297
  63.0 1.6 %collective-permute-start.11 = (bf16[256,512]{1,0:T(8,128)(2,1)S(1)}, bf16[256,512]{1,0:T(8,128)(2,1)S(1)}, u32[]{:S(2)}, u32[]{:S(2)}) collective-permute-start(bf16[256,512]{1,0:T(8,128)(2,1)S(1)} %get-tuple-element.82), channel_id=1, source_target_pairs={{0,2},{1,3},{2,0},{3,1},{4,6},{5,7},{6,4},{7,5},{8,10},{9,11},{10,... | collective-permute-start | bytes 786440 | tf_op jit(solution)/shard_map/ppermute | solution.py:300
  64.6 0.7 shard_map.200.sel_ref
  65.3 1.6 %collective-permute-done.39 = bf16[128,512]{1,0:T(8,128)(2,1)S(1)} collective-permute-done((bf16[128,512]{1,0:T(8,128)(2,1)S(1)}, bf16[128,512]{1,0:T(8,128)(2,1)S(1)}, u32[]{:S(2)}, u32[]{:S(2)}) %collective-permute-start.39) | collective-permute-done | bytes 131104 | tf_op jit(solution)/shard_map/ppermute | solution.py:297
  66.9 5.8 %collective-permute-start.40 = (bf16[256,512]{1,0:T(8,128)(2,1)S(1)}, bf16[256,512]{1,0:T(8,128)(2,1)}, u32[]{:S(2)}, u32[]{:S(2)}) collective-permute-start(bf16[256,512]{1,0:T(8,128)(2,1)S(1)} %pad_maximum_fusion.refs_4_), channel_id=1, source_target_pairs={{0,8},{4,12},{8,16},{12,20},{16,24},{20,28},{24,0},{28,4},{1,9},{5... | collective-permute-start | bytes 786440 | tf_op jit(solution)/shard_map/ppermute | solution.py:297
  72.9 1.6 %collective-permute-start.27 = (bf16[256,512]{1,0:T(8,128)(2,1)S(1)}, bf16[256,512]{1,0:T(8,128)(2,1)S(1)}, u32[]{:S(2)}, u32[]{:S(2)}) collective-permute-start(bf16[256,512]{1,0:T(8,128)(2,1)S(1)} %get-tuple-element.98), channel_id=1, source_target_pairs={{0,2},{1,3},{2,0},{3,1},{4,6},{5,7},{6,4},{7,5},{8,10},{9,11},{10,... | collective-permute-start | bytes 786440 | tf_op jit(solution)/shard_map/ppermute | solution.py:300
  74.5 3.8 %shard_map.197 = bf16[704,2048]{1,0:T(8,128)(2,1)} custom-call(s32[4]{0:T(128)S(1)} %pad_add_fusion.blk_ref, bf16[256,704]{1,0:T(8,128)(2,1)S(1)} %get-tuple-element.87.refs_0_, bf16[256,704]{1,0:T(8,128)(2,1)S(1)} %get-tuple-element.103.refs_1_, bf16[256,512]{1,0:T(8,128)(2,1)S(1)} %constant_dynamic-update-slice_fusion.refs_0_.refs_2_, ...), custom_call_target="tpu_custom_call" | custom-call | flops 1476395008 | bytes 7798800 | tf_op jit(solution)/shard_map/pallas_call | solution.py:28
  78.3 1.5 %collective-permute-start.12 = (bf16[64,512]{1,0:T(8,128)(2,1)S(1)}, bf16[64,512]{1,0:T(8,128)(2,1)S(1)}, u32[]{:S(2)}, u32[]{:S(2)}) collective-permute-start(bf16[64,512]{1,0:T(8,128)(2,1)S(1)} %get-tuple-element.84), channel_id=1, source_target_pairs={{0,4},{4,0},{8,12},{12,8},{16,20},{20,16},{24,28},{28,24},{1,5},{5... | collective-permute-start | bytes 196616 | tf_op jit(solution)/shard_map/ppermute | solution.py:297
  79.9 2.9 %collective-permute-start.13 = (bf16[64,512]{1,0:T(8,128)(2,1)S(1)}, bf16[64,512]{1,0:T(8,128)(2,1)S(1)}, u32[]{:S(2)}, u32[]{:S(2)}) collective-permute-start(bf16[64,512]{1,0:T(8,128)(2,1)S(1)} %get-tuple-element.85), channel_id=1, source_target_pairs={{0,24},{4,28},{8,0},{12,4},{16,8},{20,12},{24,16},{28,20},{1,25},{... | collective-permute-start | bytes 196616 | tf_op jit(solution)/shard_map/ppermute | solution.py:297
  82.7 2.0 %collective-permute-start.14 = (bf16[64,512]{1,0:T(8,128)(2,1)S(1)}, bf16[64,512]{1,0:T(8,128)(2,1)S(1)}, u32[]{:S(2)}, u32[]{:S(2)}) collective-permute-start(bf16[64,512]{1,0:T(8,128)(2,1)S(1)} %get-tuple-element.86), channel_id=1, source_target_pairs={{0,28},{4,24},{8,4},{12,0},{16,12},{20,8},{24,20},{28,16},{1,29},{... | collective-permute-start | bytes 196616 | tf_op jit(solution)/shard_map/ppermute | solution.py:297
  84.7 3.8 %shard_map.198 = bf16[704,2048]{1,0:T(8,128)(2,1)} custom-call(s32[4]{0:T(128)S(1)} %pad_add_fusion.blk_ref, bf16[256,704]{1,0:T(8,128)(2,1)S(1)} %get-tuple-element.105.refs_0_, bf16[256,704]{1,0:T(8,128)(2,1)S(1)} %get-tuple-element.106.refs_1_, bf16[256,512]{1,0:T(8,128)(2,1)S(1)} %constant_dynamic-update-slice_fusion.refs_0_.refs_2_, ...), custom_call_target="tpu_custom_call" | custom-call | flops 1476395008 | bytes 7798800 | tf_op jit(solution)/shard_map/pallas_call | solution.py:28
  88.7 3.8 %collective-permute-start.29 = (bf16[64,512]{1,0:T(8,128)(2,1)S(1)}, bf16[64,512]{1,0:T(8,128)(2,1)S(1)}, u32[]{:S(2)}, u32[]{:S(2)}) collective-permute-start(bf16[64,512]{1,0:T(8,128)(2,1)S(1)} %get-tuple-element.100), channel_id=1, source_target_pairs={{0,20},{4,16},{8,28},{12,24},{16,4},{20,0},{24,12},{28,8},{1,21},{... | collective-permute-start | bytes 196616 | tf_op jit(solution)/shard_map/ppermute | solution.py:297
  92.5 0.6 collective-permute-start.31
  93.1 3.8 %shard_map.199 = bf16[704,2048]{1,0:T(8,128)(2,1)} custom-call(s32[4]{0:T(128)S(1)} %pad_add_fusion.blk_ref, bf16[256,704]{1,0:T(8,128)(2,1)S(1)} %get-tuple-element.107.refs_0_, bf16[256,704]{1,0:T(8,128)(2,1)S(1)} %get-tuple-element.108.refs_1_, bf16[256,512]{1,0:T(8,128)(2,1)S(1)} %constant_dynamic-update-slice_fusion.refs_0_.refs_2_, ...), custom_call_target="tpu_custom_call" | custom-call | flops 1476395008 | bytes 7798800 | tf_op jit(solution)/shard_map/pallas_call | solution.py:28
  97.0 0.8 collective-permute-done.29.refs_5_
  97.7 0.8 collective-permute-done.30.refs_6_
  98.6 1.0 collective-permute-done.31.refs_7_
  99.8 0.6 collective-permute-start.33
  100.4 4.4 %collective-permute-done.33.refs_2_ = bf16[128,512]{1,0:T(8,128)(2,1)S(1)} collective-permute-done((bf16[128,512]{1,0:T(8,128)(2,1)S(1)}, bf16[128,512]{1,0:T(8,128)(2,1)S(1)}, u32[]{:S(2)}, u32[]{:S(2)}) %collective-permute-start.33) | collective-permute-done | bytes 131104 | tf_op jit(solution)/shard_map/ppermute | solution.py:300
  105.0 0.6 copy-done.6
  106.2 0.7 copy-done.8
  106.8 0.9 copy-done.7
  107.7 0.9 copy-done.9
  108.6 0.6 shard_map.202
  109.3 1.3 collective-permute-start.35
  110.6 5.0 %collective-permute-done.41.refs_6_ = bf16[256,512]{1,0:T(8,128)(2,1)S(1)} collective-permute-done((bf16[256,512]{1,0:T(8,128)(2,1)}, bf16[256,512]{1,0:T(8,128)(2,1)S(1)}, u32[]{:S(2)}, u32[]{:S(2)}) %collective-permute-start.41) | collective-permute-done | bytes 262176 | tf_op jit(solution)/shard_map/ppermute | solution.py:297
  115.6 2.2 %collective-permute-done.35.refs_1_ = bf16[512,256]{1,0:T(8,128)(2,1)S(1)} collective-permute-done((bf16[512,256]{1,0:T(8,128)(2,1)S(1)}, bf16[512,256]{1,0:T(8,128)(2,1)S(1)}, u32[]{:S(2)}, u32[]{:S(2)}) %collective-permute-start.35) | collective-permute-done | bytes 262176 | tf_op jit(solution)/shard_map/ppermute | solution.py:297
  117.8 1.3 collective-permute-start.36
  119.1 2.6 %collective-permute-start.37 = (bf16[256,256]{1,0:T(8,128)(2,1)S(1)}, bf16[256,256]{1,0:T(8,128)(2,1)S(1)}, u32[]{:S(2)}, u32[]{:S(2)}) collective-permute-start(bf16[256,256]{1,0:T(8,128)(2,1)S(1)} %get-tuple-element.124), channel_id=1, source_target_pairs={{0,16},{4,20},{8,24},{12,28},{16,0},{20,4},{24,8},{28,12},{1,17},{... | collective-permute-start | bytes 393224 | tf_op jit(solution)/shard_map/ppermute | solution.py:297
  121.7 1.1 collective-permute-start.38
  122.8 0.9 copy-done.2
  123.7 1.1 shard_map.206
  124.8 2.6 %collective-permute-start.43 = (bf16[1,512]{1,0:T(2,128)(2,1)S(1)}, bf16[1,512]{1,0:T(2,128)(2,1)S(1)}, u32[]{:S(2)}, u32[]{:S(2)}) collective-permute-start(bf16[1,512]{1,0:T(2,128)(2,1)S(1)} %get-tuple-element.129), channel_id=1, source_target_pairs={{0,4},{4,8},{8,12},{12,16},{16,20},{20,24},{24,28},{1,5},{5,9},{9,... | collective-permute-start | bytes 3080 | tf_op jit(solution)/shard_map/ppermute | solution.py:430
  127.3 1.3 collective-permute-done.43.low_ref
  128.6 1.3 collective-permute-start.44
  129.9 4.5 %collective-permute-done.44.high_ref = bf16[1,512]{1,0:T(2,128)(2,1)S(1)} collective-permute-done((bf16[1,512]{1,0:T(2,128)(2,1)S(1)}, bf16[1,512]{1,0:T(2,128)(2,1)S(1)}, u32[]{:S(2)}, u32[]{:S(2)}) %collective-permute-start.44) | collective-permute-done | bytes 1056 | tf_op jit(solution)/shard_map/ppermute | solution.py:431
  134.4 0.9 copy-done.4
  135.3 0.9 copy-done.5
  136.2 0.8 shard_map.207
  137.1 2.2 %shard_map.205 = f32[256,512]{1,0:T(8,128)} custom-call(bf16[256,256]{1,0:T(8,128)(2,1)S(1)} %get-tuple-element.122.refs_0_, bf16[256,256]{1,0:T(8,128)(2,1)S(1)} %collective-permute-done.36.refs_1_, bf16[256,256]{1,0:T(8,128)(2,1)S(1)} %collective-permute-done.37.refs_2_, bf16[256,256]{1,0:T(8,128)(2,1)S(1)} %collective-permute-done.38.refs_3_, ...), custom_call_target="tpu_custom_call" | custom-call | flops 268435456 | bytes 2097152 | tf_op jit(solution)/shard_map/pallas_call | solution.py:28
  (82 shorter events, 2.9 us)
Async XLA Ops:
  2.9 10.0 %collective-permute-start.4 = (bf16[128,512]{1,0:T(8,128)(2,1)S(1)}, bf16[128,512]{1,0:T(8,128)(2,1)S(1)}, u32[]{:S(2)}, u32[]{:S(2)}) collective-permute-start(bf16[128,512]{1,0:T(8,128)(2,1)S(1)} %get-tuple-element.72), channel_id=1, source_target_pairs={{0,8},{4,12},{8,16},{12,20},{16,24},{20,28},{24,0},{28,4},{1,9},{5... | collective-permute-start | bytes 393224 | tf_op jit(solution)/shard_map/ppermute | solution.py:297
  6.0 9.2 %collective-permute-start = (bf16[128,512]{1,0:T(8,128)(2,1)S(1)}, bf16[128,512]{1,0:T(8,128)(2,1)S(1)}, u32[]{:S(2)}, u32[]{:S(2)}) collective-permute-start(bf16[128,512]{1,0:T(8,128)(2,1)S(1)} %get-tuple-element.71), channel_id=1, source_target_pairs={{0,4},{4,0},{8,12},{12,8},{16,20},{20,16},{24,28},{28,24},{1,5},{5... | collective-permute-start | bytes 393224 | tf_op jit(solution)/shard_map/ppermute | solution.py:297
  7.5 15.5 %collective-permute-start.5 = (bf16[128,512]{1,0:T(8,128)(2,1)S(1)}, bf16[128,512]{1,0:T(8,128)(2,1)S(1)}, u32[]{:S(2)}, u32[]{:S(2)}) collective-permute-start(bf16[128,512]{1,0:T(8,128)(2,1)S(1)} %get-tuple-element.73), channel_id=1, source_target_pairs={{0,12},{4,8},{8,20},{12,16},{16,28},{20,24},{24,4},{28,0},{1,13},{... | collective-permute-start | bytes 393224 | tf_op jit(solution)/shard_map/ppermute | solution.py:297
  9.0 13.9 %collective-permute-start.15 = (bf16[128,512]{1,0:T(8,128)(2,1)S(1)}, bf16[128,512]{1,0:T(8,128)(2,1)S(1)}, u32[]{:S(2)}, u32[]{:S(2)}) collective-permute-start(bf16[128,512]{1,0:T(8,128)(2,1)S(1)} %get-tuple-element.89), channel_id=1, source_target_pairs={{0,16},{4,20},{8,24},{12,28},{16,0},{20,4},{24,8},{28,12},{1,17},{... | collective-permute-start | bytes 393224 | tf_op jit(solution)/shard_map/ppermute | solution.py:297
  10.1 16.5 %collective-permute-start.16 = (bf16[128,512]{1,0:T(8,128)(2,1)S(1)}, bf16[128,512]{1,0:T(8,128)(2,1)S(1)}, u32[]{:S(2)}, u32[]{:S(2)}) collective-permute-start(bf16[128,512]{1,0:T(8,128)(2,1)S(1)} %get-tuple-element.90), channel_id=1, source_target_pairs={{0,20},{4,16},{8,28},{12,24},{16,4},{20,0},{24,12},{28,8},{1,21},{... | collective-permute-start | bytes 393224 | tf_op jit(solution)/shard_map/ppermute | solution.py:297
  12.9 11.7 %collective-permute-start.20 = (bf16[128,512]{1,0:T(8,128)(2,1)S(1)}, bf16[128,512]{1,0:T(8,128)(2,1)S(1)}, u32[]{:S(2)}, u32[]{:S(2)}) collective-permute-start(bf16[128,512]{1,0:T(8,128)(2,1)S(1)} %get-tuple-element.91), channel_id=1, source_target_pairs={{0,24},{4,28},{8,0},{12,4},{16,8},{20,12},{24,16},{28,20},{1,25},{... | collective-permute-start | bytes 393224 | tf_op jit(solution)/shard_map/ppermute | solution.py:297
  15.2 11.4 %collective-permute-start.21 = (bf16[128,512]{1,0:T(8,128)(2,1)S(1)}, bf16[128,512]{1,0:T(8,128)(2,1)S(1)}, u32[]{:S(2)}, u32[]{:S(2)}) collective-permute-start(bf16[128,512]{1,0:T(8,128)(2,1)S(1)} %get-tuple-element.92), channel_id=1, source_target_pairs={{0,28},{4,24},{8,4},{12,0},{16,12},{20,8},{24,20},{28,16},{1,29},{... | collective-permute-start | bytes 393224 | tf_op jit(solution)/shard_map/ppermute | solution.py:297
  22.9 5.3 %collective-permute-start.1 = (bf16[256,512]{1,0:T(8,128)(2,1)S(1)}, bf16[256,512]{1,0:T(8,128)(2,1)S(1)}, u32[]{:S(2)}, u32[]{:S(2)}) collective-permute-start(bf16[256,512]{1,0:T(8,128)(2,1)S(1)} %constant_dynamic-update-slice_fusion.refs_0_.refs_2_), channel_id=1, source_target_pairs={{0,1},{1,0},{2,3},{3,2},{4,5},{5,4},{6,7},{7,6},{8,9},{9,8},{10,11... | collective-permute-start | bytes 786440 | tf_op jit(solution)/shard_map/ppermute | solution.py:303
  23.0 9.2 %collective-permute-start.2 = (bf16[256,512]{1,0:T(8,128)(2,1)S(1)}, bf16[256,512]{1,0:T(8,128)(2,1)S(1)}, u32[]{:S(2)}, u32[]{:S(2)}) collective-permute-start(bf16[256,512]{1,0:T(8,128)(2,1)S(1)} %constant_dynamic-update-slice_fusion.refs_0_.refs_2_), channel_id=1, source_target_pairs={{0,2},{1,3},{2,0},{3,1},{4,6},{5,7},{6,4},{7,5},{8,10},{9,11},{10,... | collective-permute-start | bytes 786440 | tf_op jit(solution)/shard_map/ppermute | solution.py:300
  24.6 13.3 %collective-permute-start.7 = (bf16[256,512]{1,0:T(8,128)(2,1)S(1)}, bf16[256,512]{1,0:T(8,128)(2,1)S(1)}, u32[]{:S(2)}, u32[]{:S(2)}) collective-permute-start(bf16[256,512]{1,0:T(8,128)(2,1)S(1)} %constant_dynamic-update-slice_fusion.2.refs_4_.refs_6_), channel_id=1, source_target_pairs={{0,2},{1,3},{2,0},{3,1},{4,6},{5,7},{6,4},{7,5},{8,10},{9,11},{10,... | collective-permute-start | bytes 786440 | tf_op jit(solution)/shard_map/ppermute | solution.py:300
  26.6 14.9 %collective-permute-start.6 = (bf16[256,512]{1,0:T(8,128)(2,1)S(1)}, bf16[256,512]{1,0:T(8,128)(2,1)S(1)}, u32[]{:S(2)}, u32[]{:S(2)}) collective-permute-start(bf16[256,512]{1,0:T(8,128)(2,1)S(1)} %constant_dynamic-update-slice_fusion.2.refs_4_.refs_6_), channel_id=1, source_target_pairs={{0,1},{1,0},{2,3},{3,2},{4,5},{5,4},{6,7},{7,6},{8,9},{9,8},{10,11... | collective-permute-start | bytes 786440 | tf_op jit(solution)/shard_map/ppermute | solution.py:303
  26.6 16.8 %collective-permute-start.18 = (bf16[256,512]{1,0:T(8,128)(2,1)S(1)}, bf16[256,512]{1,0:T(8,128)(2,1)S(1)}, u32[]{:S(2)}, u32[]{:S(2)}) collective-permute-start(bf16[256,512]{1,0:T(8,128)(2,1)S(1)} %constant_dynamic-update-slice_fusion.4.refs_0_.refs_10_), channel_id=1, source_target_pairs={{0,2},{1,3},{2,0},{3,1},{4,6},{5,7},{6,4},{7,5},{8,10},{9,11},{10,... | collective-permute-start | bytes 786440 | tf_op jit(solution)/shard_map/ppermute | solution.py:300
  28.2 20.3 %collective-permute-start.23 = (bf16[256,512]{1,0:T(8,128)(2,1)S(1)}, bf16[256,512]{1,0:T(8,128)(2,1)S(1)}, u32[]{:S(2)}, u32[]{:S(2)}) collective-permute-start(bf16[256,512]{1,0:T(8,128)(2,1)S(1)} %constant_dynamic-update-slice_fusion.6.refs_4_.refs_14_), channel_id=1, source_target_pairs={{0,2},{1,3},{2,0},{3,1},{4,6},{5,7},{6,4},{7,5},{8,10},{9,11},{10,... | collective-permute-start | bytes 786440 | tf_op jit(solution)/shard_map/ppermute | solution.py:300
  32.2 16.4 %collective-permute-start.3 = (bf16[256,512]{1,0:T(8,128)(2,1)S(1)}, bf16[256,512]{1,0:T(8,128)(2,1)S(1)}, u32[]{:S(2)}, u32[]{:S(2)}) collective-permute-start(bf16[256,512]{1,0:T(8,128)(2,1)S(1)} %collective-permute-done.2.refs_2_.refs_4_), channel_id=1, source_target_pairs={{0,1},{1,0},{2,3},{3,2},{4,5},{5,4},{6,7},{7,6},{8,9},{9,8},{10,11... | collective-permute-start | bytes 786440 | tf_op jit(solution)/shard_map/ppermute | solution.py:303
  37.8 11.3 %collective-permute-start.8 = (bf16[256,512]{1,0:T(8,128)(2,1)S(1)}, bf16[256,512]{1,0:T(8,128)(2,1)S(1)}, u32[]{:S(2)}, u32[]{:S(2)}) collective-permute-start(bf16[256,512]{1,0:T(8,128)(2,1)S(1)} %collective-permute-done.7.refs_6_.refs_8_), channel_id=1, source_target_pairs={{0,1},{1,0},{2,3},{3,2},{4,5},{5,4},{6,7},{7,6},{8,9},{9,8},{10,11... | collective-permute-start | bytes 786440 | tf_op jit(solution)/shard_map/ppermute | solution.py:303
  41.5 12.7 %collective-permute-start.17 = (bf16[256,512]{1,0:T(8,128)(2,1)S(1)}, bf16[256,512]{1,0:T(8,128)(2,1)S(1)}, u32[]{:S(2)}, u32[]{:S(2)}) collective-permute-start(bf16[256,512]{1,0:T(8,128)(2,1)S(1)} %constant_dynamic-update-slice_fusion.4.refs_0_.refs_10_), channel_id=1, source_target_pairs={{0,1},{1,0},{2,3},{3,2},{4,5},{5,4},{6,7},{7,6},{8,9},{9,8},{10,11... | collective-permute-start | bytes 786440 | tf_op jit(solution)/shard_map/ppermute | solution.py:303
  43.4 11.3 %collective-permute-start.22 = (bf16[256,512]{1,0:T(8,128)(2,1)S(1)}, bf16[256,512]{1,0:T(8,128)(2,1)S(1)}, u32[]{:S(2)}, u32[]{:S(2)}) collective-permute-start(bf16[256,512]{1,0:T(8,128)(2,1)S(1)} %constant_dynamic-update-slice_fusion.6.refs_4_.refs_14_), channel_id=1, source_target_pairs={{0,1},{1,0},{2,3},{3,2},{4,5},{5,4},{6,7},{7,6},{8,9},{9,8},{10,11... | collective-permute-start | bytes 786440 | tf_op jit(solution)/shard_map/ppermute | solution.py:303
  48.6 6.1 %collective-permute-start.19 = (bf16[256,512]{1,0:T(8,128)(2,1)S(1)}, bf16[256,512]{1,0:T(8,128)(2,1)S(1)}, u32[]{:S(2)}, u32[]{:S(2)}) collective-permute-start(bf16[256,512]{1,0:T(8,128)(2,1)S(1)} %collective-permute-done.18.refs_2_.refs_12_), channel_id=1, source_target_pairs={{0,1},{1,0},{2,3},{3,2},{4,5},{5,4},{6,7},{7,6},{8,9},{9,8},{10,11... | collective-permute-start | bytes 786440 | tf_op jit(solution)/shard_map/ppermute | solution.py:303
  48.6 6.1 %collective-permute-start.24 = (bf16[256,512]{1,0:T(8,128)(2,1)S(1)}, bf16[256,512]{1,0:T(8,128)(2,1)S(1)}, u32[]{:S(2)}, u32[]{:S(2)}) collective-permute-start(bf16[256,512]{1,0:T(8,128)(2,1)S(1)} %collective-permute-done.23.refs_6_.refs_16_), channel_id=1, source_target_pairs={{0,1},{1,0},{2,3},{3,2},{4,5},{5,4},{6,7},{7,6},{8,9},{9,8},{10,11... | collective-permute-start | bytes 786440 | tf_op jit(solution)/shard_map/ppermute | solution.py:303
  54.1 8.8 %collective-permute-start.9 = (bf16[256,512]{1,0:T(8,128)(2,1)S(1)}, bf16[256,512]{1,0:T(8,128)(2,1)S(1)}, u32[]{:S(2)}, u32[]{:S(2)}) collective-permute-start(bf16[256,512]{1,0:T(8,128)(2,1)S(1)} %get-tuple-element.78), channel_id=1, source_target_pairs={{0,1},{1,0},{2,3},{3,2},{4,5},{5,4},{6,7},{7,6},{8,9},{9,8},{10,11... | collective-permute-start | bytes 786440 | tf_op jit(solution)/shard_map/ppermute | solution.py:303
  54.2 10.4 %copy-start.11 = (s32[128,2]{0,1:T(2,128)S(1)}, s32[128,2]{0,1:T(2,128)}, u32[]{:S(2)}) copy-start(s32[128,2]{0,1:T(2,128)} %param.17) | copy-start | bytes 3076
  54.2 8.7 %collective-permute-start.10 = (bf16[256,512]{1,0:T(8,128)(2,1)S(1)}, bf16[256,512]{1,0:T(8,128)(2,1)S(1)}, u32[]{:S(2)}, u32[]{:S(2)}) collective-permute-start(bf16[256,512]{1,0:T(8,128)(2,1)S(1)} %get-tuple-element.80), channel_id=1, source_target_pairs={{0,1},{1,0},{2,3},{3,2},{4,5},{5,4},{6,7},{7,6},{8,9},{9,8},{10,11... | collective-permute-start | bytes 786440 | tf_op jit(solution)/shard_map/ppermute | solution.py:303
  59.7 13.0 %collective-permute-start.25 = (bf16[256,512]{1,0:T(8,128)(2,1)S(1)}, bf16[256,512]{1,0:T(8,128)(2,1)S(1)}, u32[]{:S(2)}, u32[]{:S(2)}) collective-permute-start(bf16[256,512]{1,0:T(8,128)(2,1)S(1)} %get-tuple-element.94), channel_id=1, source_target_pairs={{0,1},{1,0},{2,3},{3,2},{4,5},{5,4},{6,7},{7,6},{8,9},{9,8},{10,11... | collective-permute-start | bytes 786440 | tf_op jit(solution)/shard_map/ppermute | solution.py:303
  59.9 12.9 %collective-permute-start.26 = (bf16[256,512]{1,0:T(8,128)(2,1)S(1)}, bf16[256,512]{1,0:T(8,128)(2,1)S(1)}, u32[]{:S(2)}, u32[]{:S(2)}) collective-permute-start(bf16[256,512]{1,0:T(8,128)(2,1)S(1)} %get-tuple-element.96), channel_id=1, source_target_pairs={{0,1},{1,0},{2,3},{3,2},{4,5},{5,4},{6,7},{7,6},{8,9},{9,8},{10,11... | collective-permute-start | bytes 786440 | tf_op jit(solution)/shard_map/ppermute | solution.py:303
  61.3 5.6 %collective-permute-start.39 = (bf16[128,512]{1,0:T(8,128)(2,1)S(1)}, bf16[128,512]{1,0:T(8,128)(2,1)S(1)}, u32[]{:S(2)}, u32[]{:S(2)}) collective-permute-start(bf16[128,512]{1,0:T(8,128)(2,1)S(1)} %shard_map.204), channel_id=1, source_target_pairs={{0,4},{4,0},{8,12},{12,8},{16,20},{20,16},{24,28},{28,24},{1,5},{5... | collective-permute-start | bytes 393224 | tf_op jit(solution)/shard_map/ppermute | solution.py:297
  63.0 15.3 %collective-permute-start.11 = (bf16[256,512]{1,0:T(8,128)(2,1)S(1)}, bf16[256,512]{1,0:T(8,128)(2,1)S(1)}, u32[]{:S(2)}, u32[]{:S(2)}) collective-permute-start(bf16[256,512]{1,0:T(8,128)(2,1)S(1)} %get-tuple-element.82), channel_id=1, source_target_pairs={{0,2},{1,3},{2,0},{3,1},{4,6},{5,7},{6,4},{7,5},{8,10},{9,11},{10,... | collective-permute-start | bytes 786440 | tf_op jit(solution)/shard_map/ppermute | solution.py:300
  66.9 37.9 %collective-permute-start.40 = (bf16[256,512]{1,0:T(8,128)(2,1)S(1)}, bf16[256,512]{1,0:T(8,128)(2,1)}, u32[]{:S(2)}, u32[]{:S(2)}) collective-permute-start(bf16[256,512]{1,0:T(8,128)(2,1)S(1)} %pad_maximum_fusion.refs_4_), channel_id=1, source_target_pairs={{0,8},{4,12},{8,16},{12,20},{16,24},{20,28},{24,0},{28,4},{1,9},{5... | collective-permute-start | bytes 786440 | tf_op jit(solution)/shard_map/ppermute | solution.py:297
  72.9 15.6 %collective-permute-start.27 = (bf16[256,512]{1,0:T(8,128)(2,1)S(1)}, bf16[256,512]{1,0:T(8,128)(2,1)S(1)}, u32[]{:S(2)}, u32[]{:S(2)}) collective-permute-start(bf16[256,512]{1,0:T(8,128)(2,1)S(1)} %get-tuple-element.98), channel_id=1, source_target_pairs={{0,2},{1,3},{2,0},{3,1},{4,6},{5,7},{6,4},{7,5},{8,10},{9,11},{10,... | collective-permute-start | bytes 786440 | tf_op jit(solution)/shard_map/ppermute | solution.py:300
  78.3 10.3 %collective-permute-start.12 = (bf16[64,512]{1,0:T(8,128)(2,1)S(1)}, bf16[64,512]{1,0:T(8,128)(2,1)S(1)}, u32[]{:S(2)}, u32[]{:S(2)}) collective-permute-start(bf16[64,512]{1,0:T(8,128)(2,1)S(1)} %get-tuple-element.84), channel_id=1, source_target_pairs={{0,4},{4,0},{8,12},{12,8},{16,20},{20,16},{24,28},{28,24},{1,5},{5... | collective-permute-start | bytes 196616 | tf_op jit(solution)/shard_map/ppermute | solution.py:297
  79.9 12.6 %collective-permute-start.13 = (bf16[64,512]{1,0:T(8,128)(2,1)S(1)}, bf16[64,512]{1,0:T(8,128)(2,1)S(1)}, u32[]{:S(2)}, u32[]{:S(2)}) collective-permute-start(bf16[64,512]{1,0:T(8,128)(2,1)S(1)} %get-tuple-element.85), channel_id=1, source_target_pairs={{0,24},{4,28},{8,0},{12,4},{16,8},{20,12},{24,16},{28,20},{1,25},{... | collective-permute-start | bytes 196616 | tf_op jit(solution)/shard_map/ppermute | solution.py:297
  82.7 9.8 %collective-permute-start.14 = (bf16[64,512]{1,0:T(8,128)(2,1)S(1)}, bf16[64,512]{1,0:T(8,128)(2,1)S(1)}, u32[]{:S(2)}, u32[]{:S(2)}) collective-permute-start(bf16[64,512]{1,0:T(8,128)(2,1)S(1)} %get-tuple-element.86), channel_id=1, source_target_pairs={{0,28},{4,24},{8,4},{12,0},{16,12},{20,8},{24,20},{28,16},{1,29},{... | collective-permute-start | bytes 196616 | tf_op jit(solution)/shard_map/ppermute | solution.py:297
  88.6 8.4 %collective-permute-start.28 = (bf16[64,512]{1,0:T(8,128)(2,1)S(1)}, bf16[64,512]{1,0:T(8,128)(2,1)S(1)}, u32[]{:S(2)}, u32[]{:S(2)}) collective-permute-start(bf16[64,512]{1,0:T(8,128)(2,1)S(1)} %get-tuple-element.99), channel_id=1, source_target_pairs={{0,16},{4,20},{8,24},{12,28},{16,0},{20,4},{24,8},{28,12},{1,17},{... | collective-permute-start | bytes 196616 | tf_op jit(solution)/shard_map/ppermute | solution.py:297
  88.7 9.0 %collective-permute-start.29 = (bf16[64,512]{1,0:T(8,128)(2,1)S(1)}, bf16[64,512]{1,0:T(8,128)(2,1)S(1)}, u32[]{:S(2)}, u32[]{:S(2)}) collective-permute-start(bf16[64,512]{1,0:T(8,128)(2,1)S(1)} %get-tuple-element.100), channel_id=1, source_target_pairs={{0,20},{4,16},{8,28},{12,24},{16,4},{20,0},{24,12},{28,8},{1,21},{... | collective-permute-start | bytes 196616 | tf_op jit(solution)/shard_map/ppermute | solution.py:297
  92.5 6.1 %collective-permute-start.30 = (bf16[64,512]{1,0:T(8,128)(2,1)S(1)}, bf16[64,512]{1,0:T(8,128)(2,1)S(1)}, u32[]{:S(2)}, u32[]{:S(2)}) collective-permute-start(bf16[64,512]{1,0:T(8,128)(2,1)S(1)} %get-tuple-element.101), channel_id=1, source_target_pairs={{0,8},{4,12},{8,16},{12,20},{16,24},{20,28},{24,0},{28,4},{1,9},{5... | collective-permute-start | bytes 196616 | tf_op jit(solution)/shard_map/ppermute | solution.py:297
  92.5 7.0 %collective-permute-start.31 = (bf16[64,512]{1,0:T(8,128)(2,1)S(1)}, bf16[64,512]{1,0:T(8,128)(2,1)S(1)}, u32[]{:S(2)}, u32[]{:S(2)}) collective-permute-start(bf16[64,512]{1,0:T(8,128)(2,1)S(1)} %get-tuple-element.102), channel_id=1, source_target_pairs={{0,12},{4,8},{8,20},{12,16},{16,28},{20,24},{24,4},{28,0},{1,13},{... | collective-permute-start | bytes 196616 | tf_op jit(solution)/shard_map/ppermute | solution.py:297
  93.1 6.4 %copy-start.3 = (bf16[128,512]{1,0:T(8,128)(2,1)S(1)}, bf16[128,512]{1,0:T(8,128)(2,1)}, u32[]{:S(2)}) copy-start(bf16[128,512]{1,0:T(8,128)(2,1)} %og_ref.1) | copy-start | bytes 393220
  93.1 29.6 %copy-start.1 = (bf16[128,512]{1,0:T(8,128)(2,1)S(1)}, bf16[128,512]{1,0:T(8,128)(2,1)}, u32[]{:S(2)}) copy-start(bf16[128,512]{1,0:T(8,128)(2,1)} %gb_ref.1) | copy-start | bytes 393220
  93.1 41.3 %copy-start.10 = (f32[3,512]{1,0:T(4,128)S(1)}, f32[3,512]{1,0:T(4,128)}, u32[]{:S(2)}) copy-start(f32[3,512]{1,0:T(4,128)} %taps_ref.1) | copy-start | bytes 18436
  96.9 25.8 %copy-start = (bf16[2048,512]{1,0:T(8,128)(2,1)S(1)}, bf16[2048,512]{1,0:T(8,128)(2,1)}, u32[]{:S(2)}) copy-start(bf16[2048,512]{1,0:T(8,128)(2,1)} %wo_ref.1) | copy-start | bytes 6291460
  99.8 5.0 %collective-permute-start.33 = (bf16[128,512]{1,0:T(8,128)(2,1)S(1)}, bf16[128,512]{1,0:T(8,128)(2,1)S(1)}, u32[]{:S(2)}, u32[]{:S(2)}) collective-permute-start(bf16[128,512]{1,0:T(8,128)(2,1)S(1)} %shard_map.201.refs_0_), channel_id=1, source_target_pairs={{0,2},{1,3},{2,0},{3,1},{4,6},{5,7},{6,4},{7,5},{8,10},{9,11},{10,... | collective-permute-start | bytes 393224 | tf_op jit(solution)/shard_map/ppermute | solution.py:300
  100.4 4.6 %collective-permute-start.32 = (bf16[128,512]{1,0:T(8,128)(2,1)S(1)}, bf16[128,512]{1,0:T(8,128)(2,1)S(1)}, u32[]{:S(2)}, u32[]{:S(2)}) collective-permute-start(bf16[128,512]{1,0:T(8,128)(2,1)S(1)} %shard_map.201.refs_0_), channel_id=1, source_target_pairs={{0,1},{1,0},{2,3},{3,2},{4,5},{5,4},{6,7},{7,6},{8,9},{9,8},{10,11... | collective-permute-start | bytes 393224 | tf_op jit(solution)/shard_map/ppermute | solution.py:303
  104.8 1.3 collective-permute-start.34
  104.8 10.7 %collective-permute-start.41 = (bf16[256,512]{1,0:T(8,128)(2,1)}, bf16[256,512]{1,0:T(8,128)(2,1)S(1)}, u32[]{:S(2)}, u32[]{:S(2)}) collective-permute-start(bf16[256,512]{1,0:T(8,128)(2,1)} %collective-permute-done.40.refs_5_), channel_id=1, source_target_pairs={{0,8},{4,12},{8,16},{12,20},{16,24},{20,28},{24,0},{28,4},{1,9},{5... | collective-permute-start | bytes 786440 | tf_op jit(solution)/shard_map/ppermute | solution.py:297
  105.0 0.7 copy-start.6
  106.2 0.7 copy-start.8
  106.8 0.9 copy-start.7
  107.7 0.9 copy-start.9
  109.3 8.4 %collective-permute-start.35 = (bf16[512,256]{1,0:T(8,128)(2,1)S(1)}, bf16[512,256]{1,0:T(8,128)(2,1)S(1)}, u32[]{:S(2)}, u32[]{:S(2)}) collective-permute-start(bf16[512,256]{1,0:T(8,128)(2,1)S(1)} %get-tuple-element.121), channel_id=1, source_target_pairs={{0,4},{4,0},{8,12},{12,8},{16,20},{20,16},{24,28},{28,24},{1,5},{5... | collective-permute-start | bytes 786440 | tf_op jit(solution)/shard_map/ppermute | solution.py:297
  115.6 21.5 %collective-permute-start.42 = (bf16[256,512]{1,0:T(8,128)(2,1)S(1)}, bf16[256,512]{1,0:T(8,128)(2,1)S(1)}, u32[]{:S(2)}, u32[]{:S(2)}) collective-permute-start(bf16[256,512]{1,0:T(8,128)(2,1)S(1)} %collective-permute-done.41.refs_6_), channel_id=1, source_target_pairs={{0,8},{4,12},{8,16},{12,20},{16,24},{20,28},{24,0},{28,4},{1,9},{5... | collective-permute-start | bytes 786440 | tf_op jit(solution)/shard_map/ppermute | solution.py:297
  117.8 19.3 %collective-permute-start.36 = (bf16[256,256]{1,0:T(8,128)(2,1)S(1)}, bf16[256,256]{1,0:T(8,128)(2,1)S(1)}, u32[]{:S(2)}, u32[]{:S(2)}) collective-permute-start(bf16[256,256]{1,0:T(8,128)(2,1)S(1)} %get-tuple-element.123), channel_id=1, source_target_pairs={{0,8},{4,12},{8,16},{12,20},{16,24},{20,28},{24,0},{28,4},{1,9},{5... | collective-permute-start | bytes 393224 | tf_op jit(solution)/shard_map/ppermute | solution.py:297
  119.1 18.0 %collective-permute-start.37 = (bf16[256,256]{1,0:T(8,128)(2,1)S(1)}, bf16[256,256]{1,0:T(8,128)(2,1)S(1)}, u32[]{:S(2)}, u32[]{:S(2)}) collective-permute-start(bf16[256,256]{1,0:T(8,128)(2,1)S(1)} %get-tuple-element.124), channel_id=1, source_target_pairs={{0,16},{4,20},{8,24},{12,28},{16,0},{20,4},{24,8},{28,12},{1,17},{... | collective-permute-start | bytes 393224 | tf_op jit(solution)/shard_map/ppermute | solution.py:297
  121.7 15.4 %collective-permute-start.38 = (bf16[256,256]{1,0:T(8,128)(2,1)S(1)}, bf16[256,256]{1,0:T(8,128)(2,1)S(1)}, u32[]{:S(2)}, u32[]{:S(2)}) collective-permute-start(bf16[256,256]{1,0:T(8,128)(2,1)S(1)} %get-tuple-element.125), channel_id=1, source_target_pairs={{0,24},{4,28},{8,0},{12,4},{16,8},{20,12},{24,16},{28,20},{1,25},{... | collective-permute-start | bytes 393224 | tf_op jit(solution)/shard_map/ppermute | solution.py:297
  122.8 0.9 copy-start.2
  124.8 3.9 %collective-permute-start.43 = (bf16[1,512]{1,0:T(2,128)(2,1)S(1)}, bf16[1,512]{1,0:T(2,128)(2,1)S(1)}, u32[]{:S(2)}, u32[]{:S(2)}) collective-permute-start(bf16[1,512]{1,0:T(2,128)(2,1)S(1)} %get-tuple-element.129), channel_id=1, source_target_pairs={{0,4},{4,8},{8,12},{12,16},{16,20},{20,24},{24,28},{1,5},{5,9},{9,... | collective-permute-start | bytes 3080 | tf_op jit(solution)/shard_map/ppermute | solution.py:430
  128.6 5.8 %collective-permute-start.44 = (bf16[1,512]{1,0:T(2,128)(2,1)S(1)}, bf16[1,512]{1,0:T(2,128)(2,1)S(1)}, u32[]{:S(2)}, u32[]{:S(2)}) collective-permute-start(bf16[1,512]{1,0:T(2,128)(2,1)S(1)} %get-tuple-element.130), channel_id=1, source_target_pairs={{4,0},{8,4},{12,8},{16,12},{20,16},{24,20},{28,24},{5,1},{9,5},{13... | collective-permute-start | bytes 3080 | tf_op jit(solution)/shard_map/ppermute | solution.py:431
  134.4 0.9 copy-start.4
  135.3 0.9 copy-start.5
where the time goes:
time: 142 us; the launch traced here: 139 us
  starting transfers between devices  51.8 us (36%)
  waiting for transfers between devices  45.9 us (32%)
  Pallas kernels  34.3 us (24%)
  local copies, waits for them, and re-layouts  6.01 us (4%)
    ppermute x22, starting transfers between devices, send_sp(): return lax.ppermute(v, 'sp', sp_perm(rz, rx))  37.7 us
    pallas_call x19, Pallas kernels, call(): pl.pallas_call(body, out_shape=tuple(outs), in_specs=[SMEM if i < smem el...  34.3 us
    ppermute x7, waiting for transfers between devices, send_y(): lax.ppermute(v, 'tp', [(k, (k // 2 + jy) % ny * 2 + k % 2) for k in range...  20 us
    ppermute x22, waiting for transfers between devices, send_sp(): return lax.ppermute(v, 'sp', sp_perm(rz, rx))  19.6 us
    ppermute x7, starting transfers between devices, send_y(): lax.ppermute(v, 'tp', [(k, (k // 2 + jy) % ny * 2 + k % 2) for k in range...  8.08 us
    unnamed x28, local copies, waits for them, and re-layouts  5.89 us
    ppermute x1, waiting for transfers between devices, local(): high = lax.ppermute(first, 'sp', [(b, a) for a, b in up_pairs])  4.46 us
  transfers between devices with their start and end apart: 45, of which 16 were waited for; matrix products, arithmetic and copies ran while one was open for 0% of the time, Pallas kernels for 21%

commit v1 on v0

--- a/solution.py
+++ b/solution.py
@@ -10,6 +10,7 @@
 
 
 EXPERT_MIB, GRAD_MIB = 16, 14
+LOAD_CUTS = 4
 BF = jnp.bfloat16
 F32 = jnp.float32
 VMEM = pl.BlockSpec(memory_space=pltpu.VMEM)
@@ -17,7 +18,7 @@
 HBM = pl.BlockSpec(memory_space=pltpu.HBM)
 
 
-def call(body, outs, args, smem=1, flops=0, scratch=(), vmem=8, hbm=()):
+def call(body, outs, args, smem=1, flops=0, scratch=(), vmem=8, hbm=(), far=False):
     args = [
         pltpu.with_memory_space_constraint(a, pltpu.HBM) if i in hbm else a
         for i, a in enumerate(args)
@@ -29,7 +30,7 @@
         body,
         out_shape=tuple(outs),
         in_specs=[SMEM if i < smem else HBM if i in hbm else VMEM for i in range(len(args))],
-        out_specs=tuple([VMEM] * len(outs)),
+        out_specs=tuple([HBM if far else VMEM] * len(outs)),
         scratch_shapes=list(scratch),
         cost_estimate=pl.CostEstimate(flops=flops, transcendentals=0, bytes_accessed=moved),
         compiler_params=pltpu.CompilerParams(vmem_limit_bytes=vmem * 1024 * 1024),
@@ -113,13 +114,14 @@
 
 def load_body(wg, wu, wd, wg_out, wu_out, wd_out, sems):
     pairs = [(wg, wg_out), (wu, wu_out), (wd, wd_out)]
-    half = wg.shape[0] // 16 * 8
     rows = wg.shape[0]
+    step = -(-rows // 8 // LOAD_CUTS) * 8
     copies = []
-    for i, (f, n) in enumerate(pairs):
-        for j, (lo, hi) in enumerate(((0, half), (half, rows))):
+    for f, n in pairs:
+        for at in range(0, rows, step):
+            cut = pl.ds(at, min(step, rows - at))
             copies.append(
-                pltpu.make_async_copy(f.at[lo:hi, :], n.at[lo:hi, :], sems.at[2 * i + j])
+                pltpu.make_async_copy(f.at[cut, :], n.at[cut, :], sems.at[len(copies)])
             )
     for copy in copies:
         copy.start()
@@ -127,7 +129,15 @@
         copy.wait()
 
 
-def mix_body(gb, co, mixed_ref, gb_near, co_near, sems):
+def fetch_body(n, *refs):
+    copies = [pltpu.make_async_copy(refs[i], refs[n + i], refs[-1].at[i]) for i in range(n)]
+    for copy in copies:
+        copy.start()
+    for copy in copies:
+        copy.wait()
+
+
+def mix_body(core_ref, gb, co, mixed_ref, gb_near, co_near, sems):
     copies = [
         pltpu.make_async_copy(gb, gb_near, sems.at[0]),
         pltpu.make_async_copy(co, co_near, sems.at[1]),
@@ -136,7 +146,13 @@
         copy.start()
     for copy in copies:
         copy.wait()
-    mixed_ref[...] = (gb_near[...].astype(F32) * co_near[...].astype(F32)).astype(BF)
+    half = mixed_ref.shape[0] // 2
+    for i in range(2):
+        at = pl.multiple_of((core_ref[0] + i) % 2 * half, half)
+        gb_half, co_half = gb_near[pl.ds(at, half), :], co_near[pl.ds(at, half), :]
+        mixed_ref[i * half : (i + 1) * half, :] = (
+            gb_half.astype(F32) * co_half.astype(F32)
+        ).astype(BF)
 
 
 def expert_body(n_b, n_g, cap, blk_ref, dst_ref, *refs):
@@ -168,12 +184,25 @@
 
 
 def weight_grad_body(n_c, n_b, cap, which, blk_ref, *refs):
-    lefts, rights, out = refs[:n_c], refs[n_c:-1], refs[-1]
+    lefts, rights, out, held, sems = refs[:n_c], refs[n_c:-3], refs[-3], refs[-2], refs[-1]
     ch = rights[0].shape[1]
-    held = jnp.concatenate([l[...] for l in lefts], axis=0).T
+    left = jnp.concatenate([l[...] for l in lefts], axis=0).T
+    copies = []
     for b in range(n_b):
-        total = jnp.dot(held, rows_of(rights[b::n_b], cap, which), preferred_element_type=F32)
-        out[:, pl.ds(pl.multiple_of(blk_ref[b] * ch, ch), ch)] = total.astype(BF)
+        total = jnp.dot(left, rows_of(rights[b::n_b], cap, which), preferred_element_type=F32)
+        held[b, :, :] = total.astype(BF)
+        cols = pl.ds(pl.multiple_of(blk_ref[b] * ch, ch), ch)
+        copies.append(pltpu.make_async_copy(held.at[b], out.at[:, cols], sems.at[b]))
+        copies[b].start()
+    for copy in copies:
+        copy.wait()
+
+
+def join_body(*refs):
+    at = 0
+    for ref in refs[:-1]:
+        refs[-1][at : at + ref.shape[0], :] = ref[...]
+        at += ref.shape[0]
 
 
 def add_body(n_out, *refs):
@@ -200,20 +229,21 @@
     dh_ref[...] = (og_ref[...].astype(F32) + moe).astype(BF)
 
 
-def spread_body(n_b, n_sp, blk_ref, tgt_ref, *refs):
+def spread_body(n_b, n_sp, blk_ref, tgt_ref, core_ref, *refs):
     blocks, full_ref, outs = refs[:n_b], refs[n_b], refs[n_b + 1 :]
     ch = blocks[0].shape[1]
     for b in range(n_b):
         full_ref[:, pl.ds(pl.multiple_of(blk_ref[b] * ch, ch), ch)] = blocks[b][...]
-    rows, w = full_ref.shape[0], outs[0].shape[1]
+    rows, w = full_ref.shape[0] // 2, outs[0].shape[1]
     nx, lane = len(outs), 128
+    mine = pl.ds(pl.multiple_of(core_ref[0] * rows, rows), rows)
     for r in range(n_sp):
         out = outs[r % nx].at[r // nx * rows : (r // nx + 1) * rows, :]
         if w % lane == 0:
-            out[...] = full_ref[:, pl.ds(pl.multiple_of(tgt_ref[r] * w, lane), w)]
+            out[...] = full_ref[mine, pl.ds(pl.multiple_of(tgt_ref[r] * w, lane), w)]
             continue
         fold = lane // w
-        wide = full_ref[:, pl.ds(pl.multiple_of(tgt_ref[r] // fold * lane, lane), lane)]
+        wide = full_ref[mine, pl.ds(pl.multiple_of(tgt_ref[r] // fold * lane, lane), lane)]
         piece = wide[:, :w]
         for i in range(1, fold):
             piece = jnp.where(tgt_ref[r] % fold == i, wide[:, i * w : (i + 1) * w], piece)
@@ -228,11 +258,28 @@
             out[rx * rows : (rx + 1) * rows, :] = ref[rz * rows : (rz + 1) * rows, :]
 
 
-def mixer_body(full_ref, wo_ref, gb_ref, co_ref, dconv_ref, grad_b_ref, first_ref, last_ref):
-    dz = jnp.dot(full_ref[...], wo_ref[...], preferred_element_type=F32)
-    dconv = (dz * gb_ref[...].astype(F32)).astype(BF)
+def mixer_body(n_b, full_ref, wo_far, gb_far, co_far, *refs):
+    dconv_ref, grad_b_ref, first_ref, last_ref, wo, gb, co, sems = refs
+    ch = wo.shape[0] // n_b
+    copies = []
+    for b in range(n_b):
+        at = slice(b * ch, (b + 1) * ch)
+        copies.append(pltpu.make_async_copy(wo_far.at[at, :], wo.at[at, :], sems.at[b]))
+    copies.append(pltpu.make_async_copy(gb_far, gb, sems.at[n_b]))
+    copies.append(pltpu.make_async_copy(co_far, co, sems.at[n_b + 1]))
+    for copy in copies:
+        copy.start()
+    dz = None
+    for b in range(n_b):
+        at = slice(b * ch, (b + 1) * ch)
+        copies[b].wait()
+        part = jnp.dot(full_ref[:, at], wo[at, :], preferred_element_type=F32)
+        dz = part if dz is None else dz + part
+    copies[n_b].wait()
+    copies[n_b + 1].wait()
+    dconv = (dz * gb[...].astype(F32)).astype(BF)
     dconv_ref[...] = dconv
-    grad_b_ref[...] = (dz * co_ref[...].astype(F32)).astype(BF)
+    grad_b_ref[...] = (dz * co[...].astype(F32)).astype(BF)
     rows = dconv.shape[0]
     first_ref[...] = dconv[0:1, :]
     last_ref[...] = dconv[rows - 1 : rows, :]
@@ -250,11 +297,16 @@
     gv_ref[...] = (du * c_ref[...].astype(F32)).astype(BF)
 
 
-def grad_out_body(nz, *refs):
-    lefts, rights, out = refs[:nz], refs[nz:-1], refs[-1]
-    left = jnp.concatenate([l[...] for l in lefts], axis=0)
-    right = jnp.concatenate([r[...] for r in rights], axis=0)
-    out[...] = tn(left, right)
+def grad_out_body(nz, nx, *refs):
+    mine, other, mixed, out = refs[:nz], refs[nz : 2 * nz], refs[2 * nz : 3 * nz], refs[-1]
+    half = mine[0].shape[0] // nx
+    lefts, rights = [], []
+    for which, held in enumerate((mine, other)):
+        for left, right in zip(held, mixed):
+            lefts.append(left[...])
+            for rx in range(nx):
+                rights.append(right[(2 * rx + which) * half : (2 * rx + which + 1) * half, :])
+    out[...] = tn(jnp.concatenate(lefts, axis=0), jnp.concatenate(rights, axis=0))
 
 
 def grid(n_sp, n_tp):
@@ -332,20 +384,25 @@
     groups = []
     for rz in range(nz):
         got = [send_sp(sent[rz * nx + rx], rz, rx) for rx in range(nx)]
-        groups.append(gather_tp(jnp.concatenate(got, axis=0)))
+        if nx > 1:
+            got = call(join_body, [shape((nx * 2 * cap, ch))], got, smem=0, flops=cap)
+        groups.append(gather_tp(got[0]))
+
+    core = c.reshape(1).astype(jnp.int32)
 
     ff = down_proj.shape[1]
     weights = [gate_proj[0].T, up_proj[0].T, down_proj[0]]
     mixed = call(
-        mix_body, [shape((tok, ch))], [gate_b, conv_out], smem=0, hbm=range(2),
+        mix_body, [shape((tok, ch))], [core, gate_b, conv_out], hbm=(1, 2),
         flops=tok * ch,
         scratch=[pltpu.VMEM((tok, ch), BF)] * 2 + [pltpu.SemaphoreType.DMA((2,))],
     )[0]
     weights = call(
         load_body, [shape((ff, ch * n_tp))] * 3, weights, smem=0, hbm=range(3),
-        scratch=[pltpu.SemaphoreType.DMA((6,))],
-    )
-    row = jnp.concatenate([send_sp(mixed, 0, rx) for rx in range(nx)], axis=0)
+        scratch=[pltpu.SemaphoreType.DMA((3 * LOAD_CUTS,))],
+    )
+    row = [send_sp(mixed, 0, rx) for rx in range(nx)]
+    row = call(join_body, [shape((nx * tok, ch))], row, smem=0, flops=tok)[0]
     mixed_all = [row]
     for _ in range(1, nz):
         row = send_sp(row, 1, 0)
@@ -386,17 +443,15 @@
     def weight_grad(lefts, which):
         return call(
             functools.partial(weight_grad_body, n_c, n_tp, cap, which),
-            [shape((ff, ch * n_tp))],
+            [pltpu.HBM((ff, ch * n_tp), BF)],
             [blk, *lefts, *[b for group in groups for b in group]],
-            flops=2 * n_sp * cap * ff * ch * n_tp, vmem=GRAD_MIB,
+            flops=2 * n_sp * cap * ff * ch * n_tp, vmem=GRAD_MIB, far=True,
+            scratch=[pltpu.VMEM((n_tp, ff, ch), BF), pltpu.SemaphoreType.DMA((n_tp,))],
         )[0]
 
     grad_down = weight_grad(hid, 1)
     grad_gate = weight_grad(dgs, 0)
     grad_up = weight_grad(dus, 0)
-    *backs, grad_down, grad_gate, grad_up = lax.optimization_barrier(
-        (*backs, grad_down, grad_gate, grad_up)
-    )
     grad_gate, grad_up = grad_gate.T, grad_up.T
 
     sel = call(
@@ -408,23 +463,28 @@
         [sel, out_grad, *backs], smem=0, flops=2 * n_sp * cap * tok * ch,
     )[0]
     dh_blocks = gather_tp(dh)
-    width = ch * n_tp // n_sp
+    width, half = ch * n_tp // n_sp, tok // 2
     outs = call(
         functools.partial(spread_body, n_tp, n_sp),
-        [shape((tok, ch * n_tp))] + [shape((nz * tok, width))] * nx,
-        [blk, tgt, *dh_blocks], smem=2, flops=tok * ch * n_tp,
+        [shape((tok, ch * n_tp))] + [shape((nz * half, width))] * nx,
+        [blk, tgt, core, *dh_blocks], smem=3, flops=tok * ch * n_tp,
     )
     full_h, slices = outs[0], outs[1:]
     slices = [send_sp(slices[rx], 0, rx) for rx in range(nx)]
     slices = call(
-        functools.partial(regroup_body, nx), [shape((nx * tok, width))] * nz, slices,
+        functools.partial(regroup_body, nx), [shape((nx * half, width))] * nz, slices,
         smem=0, flops=tok * width,
     )
-    dh_all = [send_sp(slices[rz], rz, 0) for rz in range(nz)]
+    dh_mine = [send_sp(slices[rz], rz, 0) for rz in range(nz)]
+    dh_other = [send_core(v) for v in dh_mine]
 
     dconv, grad_b, first, last = call(
-        mixer_body, [shape((tok, ch)), shape((tok, ch)), shape((1, ch)), shape((1, ch))],
-        [full_h, out_proj, gate_b, conv_out], smem=0, flops=2 * tok * ch * ch * n_tp,
+        functools.partial(mixer_body, n_tp), [shape((tok, ch)), shape((tok, ch)), shape((1, ch)), shape((1, ch))],
+        [full_h, out_proj, gate_b, conv_out], smem=0, flops=2 * tok * ch * ch * n_tp, hbm=(1, 2, 3),
+        scratch=[
+            pltpu.VMEM(out_proj.shape, BF), pltpu.VMEM((tok, ch), BF), pltpu.VMEM((tok, ch), BF),
+            pltpu.SemaphoreType.DMA((n_tp + 2,)),
+        ],
     )
     up_pairs = [(i, i + 1) for i in range(n_sp - 1)]
     low = lax.ppermute(last, "sp", up_pairs)
@@ -433,9 +493,13 @@
         conv_body, [shape((tok, ch))] * 2,
         [dconv, low, high, conv_taps, value_v, gate_c], smem=0, flops=8 * tok * ch,
     )
+    mixed_all = call(
+        functools.partial(fetch_body, nz), [shape((nx * tok, ch))] * nz, mixed_all,
+        smem=0, hbm=range(nz), scratch=[pltpu.SemaphoreType.DMA((nz,))],
+    )
     grad_out = call(
-        functools.partial(grad_out_body, nz), [shape((width, ch), F32)],
-        [*dh_all, *mixed_all], smem=0, flops=2 * n_sp * tok * width * ch,
+        functools.partial(grad_out_body, nz, nx), [shape((width, ch), F32)],
+        [*dh_mine, *dh_other, *mixed_all], smem=0, flops=2 * n_sp * tok * width * ch,
     )[0]
     return (grad_gate[None], grad_up[None], grad_down[None], grad_out, grad_b, grad_c, grad_v)
 

time: 142 us -> 131 us (0.923)
  waiting for transfers between devices: 45.9 us -> 35.8 us
  starting transfers between devices: 51.8 us -> 49 us
  local copies, waits for them, and re-layouts: 6.01 us -> 7.92 us
    ppermute x7, waiting for transfers between devices: 20 us -> 12.3 us  [send_y(): lax.ppermute(v, 'tp', [(k, (k // 2 + jy) % ny * 2 + k % 2) for k in range...]
    ppermute x1, waiting for transfers between devices: 4.46 us -> 0.01 us  [local(): high = lax.ppermute(first, 'sp', [(b, a) for a, b in up_pairs])]
    ppermute x22, starting transfers between devices: 37.7 us -> 33.3 us  [send_sp(): return lax.ppermute(v, 'sp', sp_perm(rz, rx))]
    ppermute x22, waiting for transfers between devices: 19.6 us -> 22.6 us  [send_sp(): return lax.ppermute(v, 'sp', sp_perm(rz, rx))]
    unnamed x28 -> x50, local copies, waits for them, and re-layouts: 5.89 us -> 7.84 us
    ppermute x14 -> x18, starting transfers between devices: 2.18 us -> 3.33 us  [send_core(): return lax.ppermute(v, 'tp', [(k, k ^ 1) for k in range(n_tp)])]
    pallas_call x19 -> x25, Pallas kernels: 34.3 us -> 34.6 us  [call(): pl.pallas_call(body, out_shape=tuple(outs), in_specs=[SMEM if i < smem el...]
  transfers between devices with their start and end apart: 45 -> 49, of which waited for: 16 -> 15; matrix products, arithmetic and copies ran while one was open for 0% -> 0% of each run, Pallas kernels for 21% -> 20%
where the time goes in v1:
time: 131 us; the launch traced here: 129 us
  starting transfers between devices  49 us (37%)
  waiting for transfers between devices  35.8 us (27%)
  Pallas kernels  34.6 us (26%)
  local copies, waits for them, and re-layouts  7.92 us (6%)
    pallas_call x25, Pallas kernels, call(): pl.pallas_call(body, out_shape=tuple(outs), in_specs=[SMEM if i < smem el...  34.6 us
    ppermute x22, starting transfers between devices, send_sp(): return lax.ppermute(v, 'sp', sp_perm(rz, rx))  33.3 us
    ppermute x22, waiting for transfers between devices, send_sp(): return lax.ppermute(v, 'sp', sp_perm(rz, rx))  22.6 us
    ppermute x7, waiting for transfers between devices, send_y(): lax.ppermute(v, 'tp', [(k, (k // 2 + jy) % ny * 2 + k % 2) for k in range...  12.3 us
    ppermute x7, starting transfers between devices, send_y(): lax.ppermute(v, 'tp', [(k, (k // 2 + jy) % ny * 2 + k % 2) for k in range...  7.99 us
    unnamed x50, local copies, waits for them, and re-layouts  7.84 us
    ppermute x18, starting transfers between devices, send_core(): return lax.ppermute(v, 'tp', [(k, k ^ 1) for k in range(n_tp)])  3.33 us
    ppermute x1, starting transfers between devices, local(): low = lax.ppermute(last, 'sp', up_pairs)  3.06 us
  transfers between devices with their start and end apart: 49, of which 15 were waited for; matrix products, arithmetic and copies ran while one was open for 0% of the time, Pallas kernels for 20%

profile of v1, /device:TPU:0, one launch (start us, length us, event | category | flops | bytes accessed | tf_op | source)
XLA Modules:
  0.0 128.8 jit_solution(16601616420547063918)
XLA Ops:
  0.7 2.1 %shard_map.189 = (bf16[128,512]{1,0:T(8,128)(2,1)S(1)}, bf16[128,512]{1,0:T(8,128)(2,1)S(1)}, bf16[128,512]{1,0:T(8,128)(2,1)S(1)}, bf16[128,512]{1,0:T(8,128)(2...) custom-call(s32[2]{0:T(128)S(1)} %pad_add_fusion.3.me_ref, ...), custom_call_target="tpu_custom_call" | custom-call | flops 134217728 | bytes 1312776 | tf_op jit(solution)/shard_map/pallas_call | solution.py:29
  2.9 3.1 %collective-permute-start.4 = (bf16[128,512]{1,0:T(8,128)(2,1)S(1)}, bf16[128,512]{1,0:T(8,128)(2,1)S(1)}, u32[]{:S(2)}, u32[]{:S(2)}) collective-permute-start(bf16[128,512]{1,0:T(8,128)(2,1)S(1)} %get-tuple-element.65), channel_id=1, source_target_pairs={{0,8},{4,12},{8,16},{12,20},{16,24},{20,28},{24,0},{28,4},{1,9},{5... | collective-permute-start | bytes 393224 | tf_op jit(solution)/shard_map/ppermute | solution.py:349
  6.0 2.5 %collective-permute-start.5 = (bf16[128,512]{1,0:T(8,128)(2,1)S(1)}, bf16[128,512]{1,0:T(8,128)(2,1)S(1)}, u32[]{:S(2)}, u32[]{:S(2)}) collective-permute-start(bf16[128,512]{1,0:T(8,128)(2,1)S(1)} %get-tuple-element.66), channel_id=1, source_target_pairs={{0,12},{4,8},{8,20},{12,16},{16,28},{20,24},{24,4},{28,0},{1,13},{... | collective-permute-start | bytes 393224 | tf_op jit(solution)/shard_map/ppermute | solution.py:349
  8.5 0.5 collective-permute-start
  9.0 2.2 %collective-permute-start.10 = (bf16[128,512]{1,0:T(8,128)(2,1)S(1)}, bf16[128,512]{1,0:T(8,128)(2,1)S(1)}, u32[]{:S(2)}, u32[]{:S(2)}) collective-permute-start(bf16[128,512]{1,0:T(8,128)(2,1)S(1)} %get-tuple-element.73), channel_id=1, source_target_pairs={{0,20},{4,16},{8,28},{12,24},{16,4},{20,0},{24,12},{28,8},{1,21},{... | collective-permute-start | bytes 393224 | tf_op jit(solution)/shard_map/ppermute | solution.py:349
  11.2 1.7 %collective-permute-start.9 = (bf16[128,512]{1,0:T(8,128)(2,1)S(1)}, bf16[128,512]{1,0:T(8,128)(2,1)S(1)}, u32[]{:S(2)}, u32[]{:S(2)}) collective-permute-start(bf16[128,512]{1,0:T(8,128)(2,1)S(1)} %get-tuple-element.72), channel_id=1, source_target_pairs={{0,16},{4,20},{8,24},{12,28},{16,0},{20,4},{24,8},{28,12},{1,17},{... | collective-permute-start | bytes 393224 | tf_op jit(solution)/shard_map/ppermute | solution.py:349
  12.9 3.5 %collective-permute-done.5.refs_1_ = bf16[128,512]{1,0:T(8,128)(2,1)S(1)} collective-permute-done((bf16[128,512]{1,0:T(8,128)(2,1)S(1)}, bf16[128,512]{1,0:T(8,128)(2,1)S(1)}, u32[]{:S(2)}, u32[]{:S(2)}) %collective-permute-start.5) | collective-permute-done | bytes 131104 | tf_op jit(solution)/shard_map/ppermute | solution.py:349
  16.4 1.6 %collective-permute-start.7 = (bf16[256,512]{1,0:T(8,128)(2,1)S(1)}, bf16[256,512]{1,0:T(8,128)(2,1)S(1)}, u32[]{:S(2)}, u32[]{:S(2)}) collective-permute-start(bf16[256,512]{1,0:T(8,128)(2,1)S(1)} %shard_map.191.refs_4_.refs_6_), channel_id=1, source_target_pairs={{0,2},{1,3},{2,0},{3,1},{4,6},{5,7},{6,4},{7,5},{8,10},{9,11},{10,... | collective-permute-start | bytes 786440 | tf_op jit(solution)/shard_map/ppermute | solution.py:352
  18.0 0.6 collective-permute-start.2
  18.6 5.1 %collective-permute-done.10.refs_1_ = bf16[128,512]{1,0:T(8,128)(2,1)S(1)} collective-permute-done((bf16[128,512]{1,0:T(8,128)(2,1)S(1)}, bf16[128,512]{1,0:T(8,128)(2,1)S(1)}, u32[]{:S(2)}, u32[]{:S(2)}) %collective-permute-start.10) | collective-permute-done | bytes 131104 | tf_op jit(solution)/shard_map/ppermute | solution.py:349
  23.8 2.7 %collective-permute-start.14 = (bf16[128,512]{1,0:T(8,128)(2,1)S(1)}, bf16[128,512]{1,0:T(8,128)(2,1)S(1)}, u32[]{:S(2)}, u32[]{:S(2)}) collective-permute-start(bf16[128,512]{1,0:T(8,128)(2,1)S(1)} %get-tuple-element.74), channel_id=1, source_target_pairs={{0,24},{4,28},{8,0},{12,4},{16,8},{20,12},{24,16},{28,20},{1,25},{... | collective-permute-start | bytes 393224 | tf_op jit(solution)/shard_map/ppermute | solution.py:349
  26.4 1.7 %collective-permute-start.15 = (bf16[128,512]{1,0:T(8,128)(2,1)S(1)}, bf16[128,512]{1,0:T(8,128)(2,1)S(1)}, u32[]{:S(2)}, u32[]{:S(2)}) collective-permute-start(bf16[128,512]{1,0:T(8,128)(2,1)S(1)} %get-tuple-element.75), channel_id=1, source_target_pairs={{0,28},{4,24},{8,4},{12,0},{16,12},{20,8},{24,20},{28,16},{1,29},{... | collective-permute-start | bytes 393224 | tf_op jit(solution)/shard_map/ppermute | solution.py:349
  28.1 1.9 %collective-permute-done.14.refs_0_ = bf16[128,512]{1,0:T(8,128)(2,1)S(1)} collective-permute-done((bf16[128,512]{1,0:T(8,128)(2,1)S(1)}, bf16[128,512]{1,0:T(8,128)(2,1)S(1)}, u32[]{:S(2)}, u32[]{:S(2)}) %collective-permute-start.14) | collective-permute-done | bytes 131104 | tf_op jit(solution)/shard_map/ppermute | solution.py:349
  30.0 2.3 %collective-permute-done.15.refs_1_ = bf16[128,512]{1,0:T(8,128)(2,1)S(1)} collective-permute-done((bf16[128,512]{1,0:T(8,128)(2,1)S(1)}, bf16[128,512]{1,0:T(8,128)(2,1)S(1)}, u32[]{:S(2)}, u32[]{:S(2)}) %collective-permute-start.15) | collective-permute-done | bytes 131104 | tf_op jit(solution)/shard_map/ppermute | solution.py:349
  32.3 1.5 %collective-permute-start.12 = (bf16[256,512]{1,0:T(8,128)(2,1)S(1)}, bf16[256,512]{1,0:T(8,128)(2,1)S(1)}, u32[]{:S(2)}, u32[]{:S(2)}) collective-permute-start(bf16[256,512]{1,0:T(8,128)(2,1)S(1)} %shard_map.194.refs_0_.refs_10_), channel_id=1, source_target_pairs={{0,2},{1,3},{2,0},{3,1},{4,6},{5,7},{6,4},{7,5},{8,10},{9,11},{10,... | collective-permute-start | bytes 786440 | tf_op jit(solution)/shard_map/ppermute | solution.py:352
  33.9 0.6 collective-permute-start.17
  34.9 3.6 %shard_map.192 = (bf16[704,2048]{1,0:T(8,128)(2,1)S(1)}, bf16[704,2048]{1,0:T(8,128)(2,1)S(1)}, bf16[704,2048]{1,0:T(8,128)(2,1)S(1)}) custom-call(bf16[704,2048]{1,0:T(8,128)(2,1)} %bitcast.35, bf16[704,2048]{1,0:T(8,128)(2,1)} %bitcast.36, bf16[704,2048]{1,0:T(8,128)(2,1)} %bitcast.37), custom_call_target="tpu_custom_call" | custom-call | bytes 17301504 | tf_op jit(solution)/shard_map/pallas_call | solution.py:29
  38.8 2.6 %collective-permute-done.12.refs_2_.refs_12_ = bf16[256,512]{1,0:T(8,128)(2,1)S(1)} collective-permute-done((bf16[256,512]{1,0:T(8,128)(2,1)S(1)}, bf16[256,512]{1,0:T(8,128)(2,1)S(1)}, u32[]{:S(2)}, u32[]{:S(2)}) %collective-permute-start.12) | collective-permute-done | bytes 262176 | tf_op jit(solution)/shard_map/ppermute | solution.py:352
  41.5 2.9 %collective-permute-done.17.refs_6_.refs_16_ = bf16[256,512]{1,0:T(8,128)(2,1)S(1)} collective-permute-done((bf16[256,512]{1,0:T(8,128)(2,1)S(1)}, bf16[256,512]{1,0:T(8,128)(2,1)S(1)}, u32[]{:S(2)}, u32[]{:S(2)}) %collective-permute-start.17) | collective-permute-done | bytes 262176 | tf_op jit(solution)/shard_map/ppermute | solution.py:352
  44.4 0.5 collective-permute-start.18
  44.9 5.0 %shard_map.193 = (bf16[256,704]{1,0:T(8,128)(2,1)S(1)}, bf16[256,704]{1,0:T(8,128)(2,1)S(1)}, bf16[256,704]{1,0:T(8,128)(2,1)S(1)}, bf16[256,512]{1,0:T(8,128)(2...) custom-call(s32[4]{0:T(128)S(1)} %pad_add_fusion.blk_ref, ...), custom_call_target="tpu_custom_call" | custom-call | flops 3690987520 | bytes 12877856 | tf_op jit(solution)/shard_map/pallas_call | solution.py:29
  49.9 0.7 copy-done.7
  50.6 0.7 copy-done.11
  51.4 0.7 copy-done.15
  52.2 5.0 %shard_map.196 = (bf16[256,704]{1,0:T(8,128)(2,1)S(1)}, bf16[256,704]{1,0:T(8,128)(2,1)S(1)}, bf16[256,704]{1,0:T(8,128)(2,1)S(1)}, bf16[256,512]{1,0:T(8,128)(2...) custom-call(s32[4]{0:T(128)S(1)} %pad_add_fusion.blk_ref, ...), custom_call_target="tpu_custom_call" | custom-call | flops 3690987520 | bytes 12877856 | tf_op jit(solution)/shard_map/pallas_call | solution.py:29
  58.4 1.0 shard_map.208.refs_0_
  59.4 2.0 %collective-permute-start.43 = (bf16[128,512]{1,0:T(8,128)(2,1)S(1)}, bf16[128,512]{1,0:T(8,128)(2,1)S(1)}, u32[]{:S(2)}, u32[]{:S(2)}) collective-permute-start(bf16[128,512]{1,0:T(8,128)(2,1)S(1)} %shard_map.208.refs_0_), channel_id=1, source_target_pairs={{0,4},{4,0},{8,12},{12,8},{16,20},{20,16},{24,28},{28,24},{1,5},{5... | collective-permute-start | bytes 393224 | tf_op jit(solution)/shard_map/ppermute | solution.py:349
  61.5 1.6 %collective-permute-start.27 = (bf16[256,512]{1,0:T(8,128)(2,1)S(1)}, bf16[256,512]{1,0:T(8,128)(2,1)S(1)}, u32[]{:S(2)}, u32[]{:S(2)}) collective-permute-start(bf16[256,512]{1,0:T(8,128)(2,1)S(1)} %get-tuple-element.97), channel_id=1, source_target_pairs={{0,2},{1,3},{2,0},{3,1},{4,6},{5,7},{6,4},{7,5},{8,10},{9,11},{10,... | collective-permute-start | bytes 786440 | tf_op jit(solution)/shard_map/ppermute | solution.py:352
  63.2 0.6 collective-permute-start.21
  63.8 1.3 %collective-permute-done.43.refs_1_ = bf16[128,512]{1,0:T(8,128)(2,1)S(1)} collective-permute-done((bf16[128,512]{1,0:T(8,128)(2,1)S(1)}, bf16[128,512]{1,0:T(8,128)(2,1)S(1)}, u32[]{:S(2)}, u32[]{:S(2)}) %collective-permute-start.43) | collective-permute-done | bytes 131104 | tf_op jit(solution)/shard_map/ppermute | solution.py:349
  65.1 0.7 copy-done.6
  65.8 1.7 %collective-permute-start.44 = (bf16[256,512]{1,0:T(8,128)(2,1)S(1)}, bf16[256,512]{1,0:T(8,128)(2,1)}, u32[]{:S(2)}, u32[]{:S(2)}) collective-permute-start(bf16[256,512]{1,0:T(8,128)(2,1)S(1)} %shard_map.209.refs_0_), channel_id=1, source_target_pairs={{0,8},{4,12},{8,16},{12,20},{16,24},{20,28},{24,0},{28,4},{1,9},{5... | collective-permute-start | bytes 786440 | tf_op jit(solution)/shard_map/ppermute | solution.py:349
  67.5 3.2 %collective-permute-done.27.refs_1_ = bf16[256,512]{1,0:T(8,128)(2,1)S(1)} collective-permute-done((bf16[256,512]{1,0:T(8,128)(2,1)S(1)}, bf16[256,512]{1,0:T(8,128)(2,1)S(1)}, u32[]{:S(2)}, u32[]{:S(2)}) %collective-permute-start.27) | collective-permute-done | bytes 262176 | tf_op jit(solution)/shard_map/ppermute | solution.py:352
  70.8 1.8 %collective-permute-start.28 = (bf16[64,512]{1,0:T(8,128)(2,1)S(1)}, bf16[64,512]{1,0:T(8,128)(2,1)S(1)}, u32[]{:S(2)}, u32[]{:S(2)}) collective-permute-start(bf16[64,512]{1,0:T(8,128)(2,1)S(1)} %get-tuple-element.98), channel_id=1, source_target_pairs={{0,16},{4,20},{8,24},{12,28},{16,0},{20,4},{24,8},{28,12},{1,17},{... | collective-permute-start | bytes 196616 | tf_op jit(solution)/shard_map/ppermute | solution.py:349
  72.6 0.8 collective-permute-start.29
  73.3 2.0 %collective-permute-start.30 = (bf16[64,512]{1,0:T(8,128)(2,1)S(1)}, bf16[64,512]{1,0:T(8,128)(2,1)S(1)}, u32[]{:S(2)}, u32[]{:S(2)}) collective-permute-start(bf16[64,512]{1,0:T(8,128)(2,1)S(1)} %get-tuple-element.100), channel_id=1, source_target_pairs={{0,8},{4,12},{8,16},{12,20},{16,24},{20,28},{24,0},{28,4},{1,9},{5... | collective-permute-start | bytes 196616 | tf_op jit(solution)/shard_map/ppermute | solution.py:349
  75.3 1.6 %collective-permute-start.31 = (bf16[64,512]{1,0:T(8,128)(2,1)S(1)}, bf16[64,512]{1,0:T(8,128)(2,1)S(1)}, u32[]{:S(2)}, u32[]{:S(2)}) collective-permute-start(bf16[64,512]{1,0:T(8,128)(2,1)S(1)} %get-tuple-element.101), channel_id=1, source_target_pairs={{0,12},{4,8},{8,20},{12,16},{16,28},{20,24},{24,4},{28,0},{1,13},{... | collective-permute-start | bytes 196616 | tf_op jit(solution)/shard_map/ppermute | solution.py:349
  77.2 1.5 %collective-permute-start.22 = (bf16[64,512]{1,0:T(8,128)(2,1)S(1)}, bf16[64,512]{1,0:T(8,128)(2,1)S(1)}, u32[]{:S(2)}, u32[]{:S(2)}) collective-permute-start(bf16[64,512]{1,0:T(8,128)(2,1)S(1)} %get-tuple-element.89), channel_id=1, source_target_pairs={{0,4},{4,0},{8,12},{12,8},{16,20},{20,16},{24,28},{28,24},{1,5},{5... | collective-permute-start | bytes 196616 | tf_op jit(solution)/shard_map/ppermute | solution.py:349
  78.7 4.0 %collective-permute-done.28.refs_4_ = bf16[64,512]{1,0:T(8,128)(2,1)S(1)} collective-permute-done((bf16[64,512]{1,0:T(8,128)(2,1)S(1)}, bf16[64,512]{1,0:T(8,128)(2,1)S(1)}, u32[]{:S(2)}, u32[]{:S(2)}) %collective-permute-start.28) | collective-permute-done | bytes 65568 | tf_op jit(solution)/shard_map/ppermute | solution.py:349
  82.7 2.0 %collective-permute-done.29.refs_5_ = bf16[64,512]{1,0:T(8,128)(2,1)S(1)} collective-permute-done((bf16[64,512]{1,0:T(8,128)(2,1)S(1)}, bf16[64,512]{1,0:T(8,128)(2,1)S(1)}, u32[]{:S(2)}, u32[]{:S(2)}) %collective-permute-start.29) | collective-permute-done | bytes 65568 | tf_op jit(solution)/shard_map/ppermute | solution.py:349
  84.7 0.7 shard_map.200.sel_ref
  85.5 2.6 %collective-permute-start.45 = (bf16[256,512]{1,0:T(8,128)(2,1)}, bf16[256,512]{1,0:T(8,128)(2,1)}, u32[]{:S(2)}, u32[]{:S(2)}) collective-permute-start(bf16[256,512]{1,0:T(8,128)(2,1)} %collective-permute-done.44.refs_1_), channel_id=1, source_target_pairs={{0,8},{4,12},{8,16},{12,20},{16,24},{20,28},{24,0},{28,4},{1,9},{5... | collective-permute-start | bytes 786440 | tf_op jit(solution)/shard_map/ppermute | solution.py:349
  88.0 1.9 %collective-permute-done.24.refs_3_ = bf16[64,512]{1,0:T(8,128)(2,1)S(1)} collective-permute-done((bf16[64,512]{1,0:T(8,128)(2,1)S(1)}, bf16[64,512]{1,0:T(8,128)(2,1)S(1)}, u32[]{:S(2)}, u32[]{:S(2)}) %collective-permute-start.24) | collective-permute-done | bytes 65568 | tf_op jit(solution)/shard_map/ppermute | solution.py:349
  90.2 1.6 %collective-permute-start.33 = (bf16[128,512]{1,0:T(8,128)(2,1)S(1)}, bf16[128,512]{1,0:T(8,128)(2,1)}, u32[]{:S(2)}, u32[]{:S(2)}) collective-permute-start(bf16[128,512]{1,0:T(8,128)(2,1)S(1)} %shard_map.205.refs_0_), channel_id=1, source_target_pairs={{0,2},{1,3},{2,0},{3,1},{4,6},{5,7},{6,4},{7,5},{8,10},{9,11},{10,... | collective-permute-start | bytes 393224 | tf_op jit(solution)/shard_map/ppermute | solution.py:352
  91.7 3.6 %collective-permute-done.33.refs_2_ = bf16[128,512]{1,0:T(8,128)(2,1)} collective-permute-done((bf16[128,512]{1,0:T(8,128)(2,1)S(1)}, bf16[128,512]{1,0:T(8,128)(2,1)}, u32[]{:S(2)}, u32[]{:S(2)}) %collective-permute-start.33) | collective-permute-done | bytes 131104 | tf_op jit(solution)/shard_map/ppermute | solution.py:352
  96.2 0.9 collective-permute-done.34.refs_3_
  97.1 1.1 shard_map.206
  98.2 0.9 collective-permute-start.35
  99.1 0.9 copy-done.1
  100.1 0.9 copy-done.3
  101.0 0.9 copy-done.5
  102.0 1.0 copy-done.16
  103.0 1.0 copy-done.18
  104.0 3.1 %shard_map.199 = bf16[704,2048]{1,0:T(8,128)(2,1)} custom-call(s32[4]{0:T(128)S(1)} %pad_add_fusion.blk_ref, bf16[256,704]{1,0:T(8,128)(2,1)S(1)} %copy-done.16, bf16[256,704]{1,0:T(8,128)(2,1)S(1)} %copy-done.18, bf16[256,512]{1,0:T(8,128)(2,1)S(1)} %shard_map.190.refs_0_.refs_2_, bf16[256,512]{1,0:T(8,128)(2,1)S(1)} %collective-permute-done.1.refs_1_.refs_3_, ...), custom_call_target="tpu_custom_call" | custom-call | flops 1476395008 | bytes 7798800 | tf_op jit(solution)/shard_map/pallas_call | solution.py:29
  107.1 2.6 %shard_map.212 = (bf16[128,512]{1,0:T(8,128)(2,1)S(1)}, bf16[128,512]{1,0:T(8,128)(2,1)}, bf16[1,512]{1,0:T(2,128)(2,1)S(1)}, bf16[1,512]{1,0:T(2,128)(2,1)S(1)}) custom-call(bf16[128,2048]{1,0:T(8,128)(2,1)S(1)} %get-tuple-element.112.full_ref, bf16[2048,512]{1,0:T(8,128)(2,1)} %wo_far.1, bf16[128,512]{1,0:T(8,128)(2,1)} %gb_far.1, bf16[128,512]{1,0:T(8,128)(2,1)} %co_far.1), custom_call_target="tpu_custom_call" | custom-call | flops 268435456 | bytes 3147776 | tf_op jit(solution)/shard_map/pallas_call | solution.py:29
  109.7 3.1 %collective-permute-start.47 = (bf16[1,512]{1,0:T(2,128)(2,1)S(1)}, bf16[1,512]{1,0:T(2,128)(2,1)S(1)}, u32[]{:S(2)}, u32[]{:S(2)}) collective-permute-start(bf16[1,512]{1,0:T(2,128)(2,1)S(1)} %get-tuple-element.115), channel_id=1, source_target_pairs={{0,4},{4,8},{8,12},{12,16},{16,20},{20,24},{24,28},{1,5},{5,9},{9,... | collective-permute-start | bytes 3080 | tf_op jit(solution)/shard_map/ppermute | solution.py:490
  112.9 3.2 %collective-permute-start.37 = (bf16[128,256]{1,0:T(8,128)(2,1)S(1)}, bf16[128,256]{1,0:T(8,128)(2,1)S(1)}, u32[]{:S(2)}, u32[]{:S(2)}) collective-permute-start(bf16[128,256]{1,0:T(8,128)(2,1)S(1)} %get-tuple-element.106), channel_id=1, source_target_pairs={{0,16},{4,20},{8,24},{12,28},{16,0},{20,4},{24,8},{28,12},{1,17},{... | collective-permute-start | bytes 196616 | tf_op jit(solution)/shard_map/ppermute | solution.py:349
  116.1 0.6 collective-permute-start.38
  116.7 3.1 %shard_map.198 = bf16[704,2048]{1,0:T(8,128)(2,1)} custom-call(s32[4]{0:T(128)S(1)} %pad_add_fusion.blk_ref, bf16[256,704]{1,0:T(8,128)(2,1)S(1)} %copy-done.12, bf16[256,704]{1,0:T(8,128)(2,1)S(1)} %copy-done.14, bf16[256,512]{1,0:T(8,128)(2,1)S(1)} %shard_map.190.refs_0_.refs_2_, bf16[256,512]{1,0:T(8,128)(2,1)S(1)} %collective-permute-done.1.refs_1_.refs_3_, ...), custom_call_target="tpu_custom_call" | custom-call | flops 1476395008 | bytes 7798800 | tf_op jit(solution)/shard_map/pallas_call | solution.py:29
  119.9 1.3 %collective-permute-start.48 = (bf16[1,512]{1,0:T(2,128)(2,1)S(1)}, bf16[1,512]{1,0:T(2,128)(2,1)S(1)}, u32[]{:S(2)}, u32[]{:S(2)}) collective-permute-start(bf16[1,512]{1,0:T(2,128)(2,1)S(1)} %get-tuple-element.116), channel_id=1, source_target_pairs={{4,0},{8,4},{12,8},{16,12},{20,16},{24,20},{28,24},{5,1},{9,5},{13... | collective-permute-start | bytes 3080 | tf_op jit(solution)/shard_map/ppermute | solution.py:491
  122.3 3.1 %shard_map.197 = bf16[704,2048]{1,0:T(8,128)(2,1)} custom-call(s32[4]{0:T(128)S(1)} %pad_add_fusion.blk_ref, bf16[256,704]{1,0:T(8,128)(2,1)S(1)} %copy-done.8, bf16[256,704]{1,0:T(8,128)(2,1)S(1)} %copy-done.10, bf16[256,512]{1,0:T(8,128)(2,1)S(1)} %shard_map.190.refs_0_.refs_2_, bf16[256,512]{1,0:T(8,128)(2,1)S(1)} %collective-permute-done.1.refs_1_.refs_3_, ...), custom_call_target="tpu_custom_call" | custom-call | flops 1476395008 | bytes 7798800 | tf_op jit(solution)/shard_map/pallas_call | solution.py:29
  125.4 1.2 shard_map.210
  126.7 0.8 shard_map.213
  127.6 1.3 shard_map.211
  (113 shorter events, 4.9 us)
Async XLA Ops:
  2.9 10.0 %collective-permute-start.4 = (bf16[128,512]{1,0:T(8,128)(2,1)S(1)}, bf16[128,512]{1,0:T(8,128)(2,1)S(1)}, u32[]{:S(2)}, u32[]{:S(2)}) collective-permute-start(bf16[128,512]{1,0:T(8,128)(2,1)S(1)} %get-tuple-element.65), channel_id=1, source_target_pairs={{0,8},{4,12},{8,16},{12,20},{16,24},{20,28},{24,0},{28,4},{1,9},{5... | collective-permute-start | bytes 393224 | tf_op jit(solution)/shard_map/ppermute | solution.py:349
  6.0 10.4 %collective-permute-start.5 = (bf16[128,512]{1,0:T(8,128)(2,1)S(1)}, bf16[128,512]{1,0:T(8,128)(2,1)S(1)}, u32[]{:S(2)}, u32[]{:S(2)}) collective-permute-start(bf16[128,512]{1,0:T(8,128)(2,1)S(1)} %get-tuple-element.66), channel_id=1, source_target_pairs={{0,12},{4,8},{8,20},{12,16},{16,28},{20,24},{24,4},{28,0},{1,13},{... | collective-permute-start | bytes 393224 | tf_op jit(solution)/shard_map/ppermute | solution.py:349
  8.5 9.5 %collective-permute-start = (bf16[128,512]{1,0:T(8,128)(2,1)S(1)}, bf16[128,512]{1,0:T(8,128)(2,1)S(1)}, u32[]{:S(2)}, u32[]{:S(2)}) collective-permute-start(bf16[128,512]{1,0:T(8,128)(2,1)S(1)} %get-tuple-element.64), channel_id=1, source_target_pairs={{0,4},{4,0},{8,12},{12,8},{16,20},{20,16},{24,28},{28,24},{1,5},{5... | collective-permute-start | bytes 393224 | tf_op jit(solution)/shard_map/ppermute | solution.py:349
  9.0 14.7 %collective-permute-start.10 = (bf16[128,512]{1,0:T(8,128)(2,1)S(1)}, bf16[128,512]{1,0:T(8,128)(2,1)S(1)}, u32[]{:S(2)}, u32[]{:S(2)}) collective-permute-start(bf16[128,512]{1,0:T(8,128)(2,1)S(1)} %get-tuple-element.73), channel_id=1, source_target_pairs={{0,20},{4,16},{8,28},{12,24},{16,4},{20,0},{24,12},{28,8},{1,21},{... | collective-permute-start | bytes 393224 | tf_op jit(solution)/shard_map/ppermute | solution.py:349
  11.2 15.2 %collective-permute-start.9 = (bf16[128,512]{1,0:T(8,128)(2,1)S(1)}, bf16[128,512]{1,0:T(8,128)(2,1)S(1)}, u32[]{:S(2)}, u32[]{:S(2)}) collective-permute-start(bf16[128,512]{1,0:T(8,128)(2,1)S(1)} %get-tuple-element.72), channel_id=1, source_target_pairs={{0,16},{4,20},{8,24},{12,28},{16,0},{20,4},{24,8},{28,12},{1,17},{... | collective-permute-start | bytes 393224 | tf_op jit(solution)/shard_map/ppermute | solution.py:349
  16.4 17.4 %collective-permute-start.7 = (bf16[256,512]{1,0:T(8,128)(2,1)S(1)}, bf16[256,512]{1,0:T(8,128)(2,1)S(1)}, u32[]{:S(2)}, u32[]{:S(2)}) collective-permute-start(bf16[256,512]{1,0:T(8,128)(2,1)S(1)} %shard_map.191.refs_4_.refs_6_), channel_id=1, source_target_pairs={{0,2},{1,3},{2,0},{3,1},{4,6},{5,7},{6,4},{7,5},{8,10},{9,11},{10,... | collective-permute-start | bytes 786440 | tf_op jit(solution)/shard_map/ppermute | solution.py:352
  18.0 16.4 %collective-permute-start.6 = (bf16[256,512]{1,0:T(8,128)(2,1)S(1)}, bf16[256,512]{1,0:T(8,128)(2,1)S(1)}, u32[]{:S(2)}, u32[]{:S(2)}) collective-permute-start(bf16[256,512]{1,0:T(8,128)(2,1)S(1)} %shard_map.191.refs_4_.refs_6_), channel_id=1, source_target_pairs={{0,1},{1,0},{2,3},{3,2},{4,5},{5,4},{6,7},{7,6},{8,9},{9,8},{10,11... | collective-permute-start | bytes 786440 | tf_op jit(solution)/shard_map/ppermute | solution.py:355
  18.0 16.4 %collective-permute-start.2 = (bf16[256,512]{1,0:T(8,128)(2,1)S(1)}, bf16[256,512]{1,0:T(8,128)(2,1)S(1)}, u32[]{:S(2)}, u32[]{:S(2)}) collective-permute-start(bf16[256,512]{1,0:T(8,128)(2,1)S(1)} %shard_map.190.refs_0_.refs_2_), channel_id=1, source_target_pairs={{0,2},{1,3},{2,0},{3,1},{4,6},{5,7},{6,4},{7,5},{8,10},{9,11},{10,... | collective-permute-start | bytes 786440 | tf_op jit(solution)/shard_map/ppermute | solution.py:352
  23.8 6.2 %collective-permute-start.14 = (bf16[128,512]{1,0:T(8,128)(2,1)S(1)}, bf16[128,512]{1,0:T(8,128)(2,1)S(1)}, u32[]{:S(2)}, u32[]{:S(2)}) collective-permute-start(bf16[128,512]{1,0:T(8,128)(2,1)S(1)} %get-tuple-element.74), channel_id=1, source_target_pairs={{0,24},{4,28},{8,0},{12,4},{16,8},{20,12},{24,16},{28,20},{1,25},{... | collective-permute-start | bytes 393224 | tf_op jit(solution)/shard_map/ppermute | solution.py:349
  26.4 5.9 %collective-permute-start.15 = (bf16[128,512]{1,0:T(8,128)(2,1)S(1)}, bf16[128,512]{1,0:T(8,128)(2,1)S(1)}, u32[]{:S(2)}, u32[]{:S(2)}) collective-permute-start(bf16[128,512]{1,0:T(8,128)(2,1)S(1)} %get-tuple-element.75), channel_id=1, source_target_pairs={{0,28},{4,24},{8,4},{12,0},{16,12},{20,8},{24,20},{28,16},{1,29},{... | collective-permute-start | bytes 393224 | tf_op jit(solution)/shard_map/ppermute | solution.py:349
  30.0 8.7 %collective-permute-start.1 = (bf16[256,512]{1,0:T(8,128)(2,1)S(1)}, bf16[256,512]{1,0:T(8,128)(2,1)S(1)}, u32[]{:S(2)}, u32[]{:S(2)}) collective-permute-start(bf16[256,512]{1,0:T(8,128)(2,1)S(1)} %shard_map.190.refs_0_.refs_2_), channel_id=1, source_target_pairs={{0,1},{1,0},{2,3},{3,2},{4,5},{5,4},{6,7},{7,6},{8,9},{9,8},{10,11... | collective-permute-start | bytes 786440 | tf_op jit(solution)/shard_map/ppermute | solution.py:355
  32.3 9.2 %collective-permute-start.12 = (bf16[256,512]{1,0:T(8,128)(2,1)S(1)}, bf16[256,512]{1,0:T(8,128)(2,1)S(1)}, u32[]{:S(2)}, u32[]{:S(2)}) collective-permute-start(bf16[256,512]{1,0:T(8,128)(2,1)S(1)} %shard_map.194.refs_0_.refs_10_), channel_id=1, source_target_pairs={{0,2},{1,3},{2,0},{3,1},{4,6},{5,7},{6,4},{7,5},{8,10},{9,11},{10,... | collective-permute-start | bytes 786440 | tf_op jit(solution)/shard_map/ppermute | solution.py:352
  33.9 10.5 %collective-permute-start.17 = (bf16[256,512]{1,0:T(8,128)(2,1)S(1)}, bf16[256,512]{1,0:T(8,128)(2,1)S(1)}, u32[]{:S(2)}, u32[]{:S(2)}) collective-permute-start(bf16[256,512]{1,0:T(8,128)(2,1)S(1)} %shard_map.195.refs_4_.refs_14_), channel_id=1, source_target_pairs={{0,2},{1,3},{2,0},{3,1},{4,6},{5,7},{6,4},{7,5},{8,10},{9,11},{10,... | collective-permute-start | bytes 786440 | tf_op jit(solution)/shard_map/ppermute | solution.py:352
  34.4 9.9 %collective-permute-start.8 = (bf16[256,512]{1,0:T(8,128)(2,1)S(1)}, bf16[256,512]{1,0:T(8,128)(2,1)S(1)}, u32[]{:S(2)}, u32[]{:S(2)}) collective-permute-start(bf16[256,512]{1,0:T(8,128)(2,1)S(1)} %collective-permute-done.7.refs_6_.refs_8_), channel_id=1, source_target_pairs={{0,1},{1,0},{2,3},{3,2},{4,5},{5,4},{6,7},{7,6},{8,9},{9,8},{10,11... | collective-permute-start | bytes 786440 | tf_op jit(solution)/shard_map/ppermute | solution.py:355
  34.4 10.4 %collective-permute-start.3 = (bf16[256,512]{1,0:T(8,128)(2,1)S(1)}, bf16[256,512]{1,0:T(8,128)(2,1)S(1)}, u32[]{:S(2)}, u32[]{:S(2)}) collective-permute-start(bf16[256,512]{1,0:T(8,128)(2,1)S(1)} %collective-permute-done.2.refs_2_.refs_4_), channel_id=1, source_target_pairs={{0,1},{1,0},{2,3},{3,2},{4,5},{5,4},{6,7},{7,6},{8,9},{9,8},{10,11... | collective-permute-start | bytes 786440 | tf_op jit(solution)/shard_map/ppermute | solution.py:355
  38.7 13.4 %collective-permute-start.11 = (bf16[256,512]{1,0:T(8,128)(2,1)S(1)}, bf16[256,512]{1,0:T(8,128)(2,1)S(1)}, u32[]{:S(2)}, u32[]{:S(2)}) collective-permute-start(bf16[256,512]{1,0:T(8,128)(2,1)S(1)} %shard_map.194.refs_0_.refs_10_), channel_id=1, source_target_pairs={{0,1},{1,0},{2,3},{3,2},{4,5},{5,4},{6,7},{7,6},{8,9},{9,8},{10,11... | collective-permute-start | bytes 786440 | tf_op jit(solution)/shard_map/ppermute | solution.py:355
  41.5 10.7 %collective-permute-start.16 = (bf16[256,512]{1,0:T(8,128)(2,1)S(1)}, bf16[256,512]{1,0:T(8,128)(2,1)S(1)}, u32[]{:S(2)}, u32[]{:S(2)}) collective-permute-start(bf16[256,512]{1,0:T(8,128)(2,1)S(1)} %shard_map.195.refs_4_.refs_14_), channel_id=1, source_target_pairs={{0,1},{1,0},{2,3},{3,2},{4,5},{5,4},{6,7},{7,6},{8,9},{9,8},{10,11... | collective-permute-start | bytes 786440 | tf_op jit(solution)/shard_map/ppermute | solution.py:355
  44.4 7.8 %collective-permute-start.13 = (bf16[256,512]{1,0:T(8,128)(2,1)S(1)}, bf16[256,512]{1,0:T(8,128)(2,1)S(1)}, u32[]{:S(2)}, u32[]{:S(2)}) collective-permute-start(bf16[256,512]{1,0:T(8,128)(2,1)S(1)} %collective-permute-done.12.refs_2_.refs_12_), channel_id=1, source_target_pairs={{0,1},{1,0},{2,3},{3,2},{4,5},{5,4},{6,7},{7,6},{8,9},{9,8},{10,11... | collective-permute-start | bytes 786440 | tf_op jit(solution)/shard_map/ppermute | solution.py:355
  44.4 7.8 %collective-permute-start.18 = (bf16[256,512]{1,0:T(8,128)(2,1)S(1)}, bf16[256,512]{1,0:T(8,128)(2,1)S(1)}, u32[]{:S(2)}, u32[]{:S(2)}) collective-permute-start(bf16[256,512]{1,0:T(8,128)(2,1)S(1)} %collective-permute-done.17.refs_6_.refs_16_), channel_id=1, source_target_pairs={{0,1},{1,0},{2,3},{3,2},{4,5},{5,4},{6,7},{7,6},{8,9},{9,8},{10,11... | collective-permute-start | bytes 786440 | tf_op jit(solution)/shard_map/ppermute | solution.py:355
  52.1 5.1 %copy-start = (bf16[256,512]{1,0:T(8,128)(2,1)}, bf16[256,512]{1,0:T(8,128)(2,1)S(1)}, u32[]{:S(2)}) copy-start(bf16[256,512]{1,0:T(8,128)(2,1)S(1)} %collective-permute-done.16.refs_5_.refs_15_) | copy-start | bytes 786436
  52.1 5.1 %copy-start.2 = (bf16[256,512]{1,0:T(8,128)(2,1)}, bf16[256,512]{1,0:T(8,128)(2,1)S(1)}, u32[]{:S(2)}) copy-start(bf16[256,512]{1,0:T(8,128)(2,1)S(1)} %collective-permute-done.13.refs_3_.refs_13_) | copy-start | bytes 786436
  52.2 5.0 %copy-start.4 = (bf16[256,512]{1,0:T(8,128)(2,1)}, bf16[256,512]{1,0:T(8,128)(2,1)S(1)}, u32[]{:S(2)}) copy-start(bf16[256,512]{1,0:T(8,128)(2,1)S(1)} %collective-permute-done.18.refs_7_.refs_17_) | copy-start | bytes 786436
  57.2 38.1 %copy-start.9 = (bf16[256,704]{1,0:T(8,128)(2,1)}, bf16[256,704]{1,0:T(8,128)(2,1)S(1)}, u32[]{:S(2)}) copy-start(bf16[256,704]{1,0:T(8,128)(2,1)S(1)} %get-tuple-element.79.refs_1_) | copy-start | bytes 1081348
  57.2 38.1 %copy-start.13 = (bf16[256,704]{1,0:T(8,128)(2,1)}, bf16[256,704]{1,0:T(8,128)(2,1)S(1)}, u32[]{:S(2)}) copy-start(bf16[256,704]{1,0:T(8,128)(2,1)S(1)} %get-tuple-element.81.refs_1_) | copy-start | bytes 1081348
  57.2 38.1 %copy-start.17 = (bf16[256,704]{1,0:T(8,128)(2,1)}, bf16[256,704]{1,0:T(8,128)(2,1)S(1)}, u32[]{:S(2)}) copy-start(bf16[256,704]{1,0:T(8,128)(2,1)S(1)} %get-tuple-element.76.refs_1_) | copy-start | bytes 1081348
  57.2 27.5 %copy-start.23 = (s32[128,2]{0,1:T(2,128)S(1)}, s32[128,2]{0,1:T(2,128)}, u32[]{:S(2)}) copy-start(s32[128,2]{0,1:T(2,128)} %param.17) | copy-start | bytes 3076
  57.3 32.6 %copy-start.19 = (bf16[128,512]{1,0:T(8,128)(2,1)S(1)}, bf16[128,512]{1,0:T(8,128)(2,1)}, u32[]{:S(2)}) copy-start(bf16[128,512]{1,0:T(8,128)(2,1)} %og_ref.1) | copy-start | bytes 393220
  57.3 4.1 %collective-permute-start.25 = (bf16[256,512]{1,0:T(8,128)(2,1)S(1)}, bf16[256,512]{1,0:T(8,128)(2,1)S(1)}, u32[]{:S(2)}, u32[]{:S(2)}) collective-permute-start(bf16[256,512]{1,0:T(8,128)(2,1)S(1)} %get-tuple-element.93), channel_id=1, source_target_pairs={{0,1},{1,0},{2,3},{3,2},{4,5},{5,4},{6,7},{7,6},{8,9},{9,8},{10,11... | collective-permute-start | bytes 786440 | tf_op jit(solution)/shard_map/ppermute | solution.py:355
  57.3 4.0 %collective-permute-start.26 = (bf16[256,512]{1,0:T(8,128)(2,1)S(1)}, bf16[256,512]{1,0:T(8,128)(2,1)S(1)}, u32[]{:S(2)}, u32[]{:S(2)}) collective-permute-start(bf16[256,512]{1,0:T(8,128)(2,1)S(1)} %get-tuple-element.95), channel_id=1, source_target_pairs={{0,1},{1,0},{2,3},{3,2},{4,5},{5,4},{6,7},{7,6},{8,9},{9,8},{10,11... | collective-permute-start | bytes 786440 | tf_op jit(solution)/shard_map/ppermute | solution.py:355
  57.8 5.2 %collective-permute-start.19 = (bf16[256,512]{1,0:T(8,128)(2,1)S(1)}, bf16[256,512]{1,0:T(8,128)(2,1)S(1)}, u32[]{:S(2)}, u32[]{:S(2)}) collective-permute-start(bf16[256,512]{1,0:T(8,128)(2,1)S(1)} %get-tuple-element.83), channel_id=1, source_target_pairs={{0,1},{1,0},{2,3},{3,2},{4,5},{5,4},{6,7},{7,6},{8,9},{9,8},{10,11... | collective-permute-start | bytes 786440 | tf_op jit(solution)/shard_map/ppermute | solution.py:355
  57.9 5.1 %collective-permute-start.20 = (bf16[256,512]{1,0:T(8,128)(2,1)S(1)}, bf16[256,512]{1,0:T(8,128)(2,1)S(1)}, u32[]{:S(2)}, u32[]{:S(2)}) collective-permute-start(bf16[256,512]{1,0:T(8,128)(2,1)S(1)} %get-tuple-element.85), channel_id=1, source_target_pairs={{0,1},{1,0},{2,3},{3,2},{4,5},{5,4},{6,7},{7,6},{8,9},{9,8},{10,11... | collective-permute-start | bytes 786440 | tf_op jit(solution)/shard_map/ppermute | solution.py:355
  59.4 5.7 %collective-permute-start.43 = (bf16[128,512]{1,0:T(8,128)(2,1)S(1)}, bf16[128,512]{1,0:T(8,128)(2,1)S(1)}, u32[]{:S(2)}, u32[]{:S(2)}) collective-permute-start(bf16[128,512]{1,0:T(8,128)(2,1)S(1)} %shard_map.208.refs_0_), channel_id=1, source_target_pairs={{0,4},{4,0},{8,12},{12,8},{16,20},{20,16},{24,28},{28,24},{1,5},{5... | collective-permute-start | bytes 393224 | tf_op jit(solution)/shard_map/ppermute | solution.py:349
  61.5 9.2 %collective-permute-start.27 = (bf16[256,512]{1,0:T(8,128)(2,1)S(1)}, bf16[256,512]{1,0:T(8,128)(2,1)S(1)}, u32[]{:S(2)}, u32[]{:S(2)}) collective-permute-start(bf16[256,512]{1,0:T(8,128)(2,1)S(1)} %get-tuple-element.97), channel_id=1, source_target_pairs={{0,2},{1,3},{2,0},{3,1},{4,6},{5,7},{6,4},{7,5},{8,10},{9,11},{10,... | collective-permute-start | bytes 786440 | tf_op jit(solution)/shard_map/ppermute | solution.py:352
  63.2 12.1 %collective-permute-start.21 = (bf16[256,512]{1,0:T(8,128)(2,1)S(1)}, bf16[256,512]{1,0:T(8,128)(2,1)S(1)}, u32[]{:S(2)}, u32[]{:S(2)}) collective-permute-start(bf16[256,512]{1,0:T(8,128)(2,1)S(1)} %get-tuple-element.87), channel_id=1, source_target_pairs={{0,2},{1,3},{2,0},{3,1},{4,6},{5,7},{6,4},{7,5},{8,10},{9,11},{10,... | collective-permute-start | bytes 786440 | tf_op jit(solution)/shard_map/ppermute | solution.py:352
  65.8 11.4 %collective-permute-start.44 = (bf16[256,512]{1,0:T(8,128)(2,1)S(1)}, bf16[256,512]{1,0:T(8,128)(2,1)}, u32[]{:S(2)}, u32[]{:S(2)}) collective-permute-start(bf16[256,512]{1,0:T(8,128)(2,1)S(1)} %shard_map.209.refs_0_), channel_id=1, source_target_pairs={{0,8},{4,12},{8,16},{12,20},{16,24},{20,28},{24,0},{28,4},{1,9},{5... | collective-permute-start | bytes 786440 | tf_op jit(solution)/shard_map/ppermute | solution.py:349
  70.8 11.9 %collective-permute-start.28 = (bf16[64,512]{1,0:T(8,128)(2,1)S(1)}, bf16[64,512]{1,0:T(8,128)(2,1)S(1)}, u32[]{:S(2)}, u32[]{:S(2)}) collective-permute-start(bf16[64,512]{1,0:T(8,128)(2,1)S(1)} %get-tuple-element.98), channel_id=1, source_target_pairs={{0,16},{4,20},{8,24},{12,28},{16,0},{20,4},{24,8},{28,12},{1,17},{... | collective-permute-start | bytes 196616 | tf_op jit(solution)/shard_map/ppermute | solution.py:349
  72.6 12.2 %collective-permute-start.29 = (bf16[64,512]{1,0:T(8,128)(2,1)S(1)}, bf16[64,512]{1,0:T(8,128)(2,1)S(1)}, u32[]{:S(2)}, u32[]{:S(2)}) collective-permute-start(bf16[64,512]{1,0:T(8,128)(2,1)S(1)} %get-tuple-element.99), channel_id=1, source_target_pairs={{0,20},{4,16},{8,28},{12,24},{16,4},{20,0},{24,12},{28,8},{1,21},{... | collective-permute-start | bytes 196616 | tf_op jit(solution)/shard_map/ppermute | solution.py:349
  73.3 12.1 %collective-permute-start.30 = (bf16[64,512]{1,0:T(8,128)(2,1)S(1)}, bf16[64,512]{1,0:T(8,128)(2,1)S(1)}, u32[]{:S(2)}, u32[]{:S(2)}) collective-permute-start(bf16[64,512]{1,0:T(8,128)(2,1)S(1)} %get-tuple-element.100), channel_id=1, source_target_pairs={{0,8},{4,12},{8,16},{12,20},{16,24},{20,28},{24,0},{28,4},{1,9},{5... | collective-permute-start | bytes 196616 | tf_op jit(solution)/shard_map/ppermute | solution.py:349
  75.3 12.7 %collective-permute-start.31 = (bf16[64,512]{1,0:T(8,128)(2,1)S(1)}, bf16[64,512]{1,0:T(8,128)(2,1)S(1)}, u32[]{:S(2)}, u32[]{:S(2)}) collective-permute-start(bf16[64,512]{1,0:T(8,128)(2,1)S(1)} %get-tuple-element.101), channel_id=1, source_target_pairs={{0,12},{4,8},{8,20},{12,16},{16,28},{20,24},{24,4},{28,0},{1,13},{... | collective-permute-start | bytes 196616 | tf_op jit(solution)/shard_map/ppermute | solution.py:349
  77.2 10.8 %collective-permute-start.22 = (bf16[64,512]{1,0:T(8,128)(2,1)S(1)}, bf16[64,512]{1,0:T(8,128)(2,1)S(1)}, u32[]{:S(2)}, u32[]{:S(2)}) collective-permute-start(bf16[64,512]{1,0:T(8,128)(2,1)S(1)} %get-tuple-element.89), channel_id=1, source_target_pairs={{0,4},{4,0},{8,12},{12,8},{16,20},{20,16},{24,28},{28,24},{1,5},{5... | collective-permute-start | bytes 196616 | tf_op jit(solution)/shard_map/ppermute | solution.py:349
  82.7 5.3 %collective-permute-start.23 = (bf16[64,512]{1,0:T(8,128)(2,1)S(1)}, bf16[64,512]{1,0:T(8,128)(2,1)S(1)}, u32[]{:S(2)}, u32[]{:S(2)}) collective-permute-start(bf16[64,512]{1,0:T(8,128)(2,1)S(1)} %get-tuple-element.90), channel_id=1, source_target_pairs={{0,24},{4,28},{8,0},{12,4},{16,8},{20,12},{24,16},{28,20},{1,25},{... | collective-permute-start | bytes 196616 | tf_op jit(solution)/shard_map/ppermute | solution.py:349
  84.7 5.2 %collective-permute-start.24 = (bf16[64,512]{1,0:T(8,128)(2,1)S(1)}, bf16[64,512]{1,0:T(8,128)(2,1)S(1)}, u32[]{:S(2)}, u32[]{:S(2)}) collective-permute-start(bf16[64,512]{1,0:T(8,128)(2,1)S(1)} %get-tuple-element.91), channel_id=1, source_target_pairs={{0,28},{4,24},{8,4},{12,0},{16,12},{20,8},{24,20},{28,16},{1,29},{... | collective-permute-start | bytes 196616 | tf_op jit(solution)/shard_map/ppermute | solution.py:349
  85.5 10.5 %collective-permute-start.45 = (bf16[256,512]{1,0:T(8,128)(2,1)}, bf16[256,512]{1,0:T(8,128)(2,1)}, u32[]{:S(2)}, u32[]{:S(2)}) collective-permute-start(bf16[256,512]{1,0:T(8,128)(2,1)} %collective-permute-done.44.refs_1_), channel_id=1, source_target_pairs={{0,8},{4,12},{8,16},{12,20},{16,24},{20,28},{24,0},{28,4},{1,9},{5... | collective-permute-start | bytes 786440 | tf_op jit(solution)/shard_map/ppermute | solution.py:349
  90.2 5.1 %collective-permute-start.33 = (bf16[128,512]{1,0:T(8,128)(2,1)S(1)}, bf16[128,512]{1,0:T(8,128)(2,1)}, u32[]{:S(2)}, u32[]{:S(2)}) collective-permute-start(bf16[128,512]{1,0:T(8,128)(2,1)S(1)} %shard_map.205.refs_0_), channel_id=1, source_target_pairs={{0,2},{1,3},{2,0},{3,1},{4,6},{5,7},{6,4},{7,5},{8,10},{9,11},{10,... | collective-permute-start | bytes 393224 | tf_op jit(solution)/shard_map/ppermute | solution.py:352
  91.7 4.4 %collective-permute-start.32 = (bf16[128,512]{1,0:T(8,128)(2,1)S(1)}, bf16[128,512]{1,0:T(8,128)(2,1)}, u32[]{:S(2)}, u32[]{:S(2)}) collective-permute-start(bf16[128,512]{1,0:T(8,128)(2,1)S(1)} %shard_map.205.refs_0_), channel_id=1, source_target_pairs={{0,1},{1,0},{2,3},{3,2},{4,5},{5,4},{6,7},{7,6},{8,9},{9,8},{10,11... | collective-permute-start | bytes 393224 | tf_op jit(solution)/shard_map/ppermute | solution.py:355
  95.3 1.8 %collective-permute-start.34 = (bf16[128,512]{1,0:T(8,128)(2,1)}, bf16[128,512]{1,0:T(8,128)(2,1)}, u32[]{:S(2)}, u32[]{:S(2)}) collective-permute-start(bf16[128,512]{1,0:T(8,128)(2,1)} %collective-permute-done.33.refs_2_), channel_id=1, source_target_pairs={{0,1},{1,0},{2,3},{3,2},{4,5},{5,4},{6,7},{7,6},{8,9},{9,8},{10,11... | collective-permute-start | bytes 393224 | tf_op jit(solution)/shard_map/ppermute | solution.py:355
  95.9 23.9 %collective-permute-start.46 = (bf16[256,512]{1,0:T(8,128)(2,1)}, bf16[256,512]{1,0:T(8,128)(2,1)S(1)}, u32[]{:S(2)}, u32[]{:S(2)}) collective-permute-start(bf16[256,512]{1,0:T(8,128)(2,1)} %collective-permute-done.45.refs_2_), channel_id=1, source_target_pairs={{0,8},{4,12},{8,16},{12,20},{16,24},{20,28},{24,0},{28,4},{1,9},{5... | collective-permute-start | bytes 786440 | tf_op jit(solution)/shard_map/ppermute | solution.py:349
  98.2 14.6 %collective-permute-start.35 = (bf16[256,256]{1,0:T(8,128)(2,1)S(1)}, bf16[256,256]{1,0:T(8,128)(2,1)S(1)}, u32[]{:S(2)}, u32[]{:S(2)}) collective-permute-start(bf16[256,256]{1,0:T(8,128)(2,1)S(1)} %get-tuple-element.103), channel_id=1, source_target_pairs={{0,4},{4,0},{8,12},{12,8},{16,20},{20,16},{24,28},{28,24},{1,5},{5... | collective-permute-start | bytes 393224 | tf_op jit(solution)/shard_map/ppermute | solution.py:349
  107.1 9.6 %copy-start.12 = (bf16[256,704]{1,0:T(8,128)(2,1)S(1)}, bf16[256,704]{1,0:T(8,128)(2,1)}, u32[]{:S(2)}) copy-start(bf16[256,704]{1,0:T(8,128)(2,1)} %copy-done.11) | copy-start | bytes 1081348
  107.1 9.6 %copy-start.14 = (bf16[256,704]{1,0:T(8,128)(2,1)S(1)}, bf16[256,704]{1,0:T(8,128)(2,1)}, u32[]{:S(2)}) copy-start(bf16[256,704]{1,0:T(8,128)(2,1)} %copy-done.13) | copy-start | bytes 1081348
  109.7 11.5 %collective-permute-start.47 = (bf16[1,512]{1,0:T(2,128)(2,1)S(1)}, bf16[1,512]{1,0:T(2,128)(2,1)S(1)}, u32[]{:S(2)}, u32[]{:S(2)}) collective-permute-start(bf16[1,512]{1,0:T(2,128)(2,1)S(1)} %get-tuple-element.115), channel_id=1, source_target_pairs={{0,4},{4,8},{8,12},{12,16},{16,20},{20,24},{24,28},{1,5},{5,9},{9,... | collective-permute-start | bytes 3080 | tf_op jit(solution)/shard_map/ppermute | solution.py:490
  112.8 8.5 %collective-permute-start.36 = (bf16[128,256]{1,0:T(8,128)(2,1)S(1)}, bf16[128,256]{1,0:T(8,128)(2,1)S(1)}, u32[]{:S(2)}, u32[]{:S(2)}) collective-permute-start(bf16[128,256]{1,0:T(8,128)(2,1)S(1)} %get-tuple-element.105), channel_id=1, source_target_pairs={{0,8},{4,12},{8,16},{12,20},{16,24},{20,28},{24,0},{28,4},{1,9},{5... | collective-permute-start | bytes 196616 | tf_op jit(solution)/shard_map/ppermute | solution.py:349
  112.9 8.9 %collective-permute-start.37 = (bf16[128,256]{1,0:T(8,128)(2,1)S(1)}, bf16[128,256]{1,0:T(8,128)(2,1)S(1)}, u32[]{:S(2)}, u32[]{:S(2)}) collective-permute-start(bf16[128,256]{1,0:T(8,128)(2,1)S(1)} %get-tuple-element.106), channel_id=1, source_target_pairs={{0,16},{4,20},{8,24},{12,28},{16,0},{20,4},{24,8},{28,12},{1,17},{... | collective-permute-start | bytes 196616 | tf_op jit(solution)/shard_map/ppermute | solution.py:349
  116.1 5.7 %collective-permute-start.38 = (bf16[128,256]{1,0:T(8,128)(2,1)S(1)}, bf16[128,256]{1,0:T(8,128)(2,1)S(1)}, u32[]{:S(2)}, u32[]{:S(2)}) collective-permute-start(bf16[128,256]{1,0:T(8,128)(2,1)S(1)} %get-tuple-element.107), channel_id=1, source_target_pairs={{0,24},{4,28},{8,0},{12,4},{16,8},{20,12},{24,16},{28,20},{1,25},{... | collective-permute-start | bytes 196616 | tf_op jit(solution)/shard_map/ppermute | solution.py:349
  116.7 5.6 %copy-start.8 = (bf16[256,704]{1,0:T(8,128)(2,1)S(1)}, bf16[256,704]{1,0:T(8,128)(2,1)}, u32[]{:S(2)}) copy-start(bf16[256,704]{1,0:T(8,128)(2,1)} %copy-done.7) | copy-start | bytes 1081348
  116.7 5.6 %copy-start.10 = (bf16[256,704]{1,0:T(8,128)(2,1)S(1)}, bf16[256,704]{1,0:T(8,128)(2,1)}, u32[]{:S(2)}) copy-start(bf16[256,704]{1,0:T(8,128)(2,1)} %copy-done.9) | copy-start | bytes 1081348
  119.8 5.6 %copy-start.24 = (bf16[256,512]{1,0:T(8,128)(2,1)}, bf16[256,512]{1,0:T(8,128)(2,1)S(1)}, u32[]{:S(2)}) copy-start(bf16[256,512]{1,0:T(8,128)(2,1)S(1)} %collective-permute-done.46.refs_3_) | copy-start | bytes 786436
  119.9 6.8 %collective-permute-start.48 = (bf16[1,512]{1,0:T(2,128)(2,1)S(1)}, bf16[1,512]{1,0:T(2,128)(2,1)S(1)}, u32[]{:S(2)}, u32[]{:S(2)}) collective-permute-start(bf16[1,512]{1,0:T(2,128)(2,1)S(1)} %get-tuple-element.116), channel_id=1, source_target_pairs={{4,0},{8,4},{12,8},{16,12},{20,16},{24,20},{28,24},{5,1},{9,5},{13... | collective-permute-start | bytes 3080 | tf_op jit(solution)/shard_map/ppermute | solution.py:491
  121.2 6.4 %collective-permute-start.39 = (bf16[128,256]{1,0:T(8,128)(2,1)S(1)}, bf16[128,256]{1,0:T(8,128)(2,1)S(1)}, u32[]{:S(2)}, u32[]{:S(2)}) collective-permute-start(bf16[128,256]{1,0:T(8,128)(2,1)S(1)} %get-tuple-element.104.refs_0_), channel_id=1, source_target_pairs={{0,1},{1,0},{2,3},{3,2},{4,5},{5,4},{6,7},{7,6},{8,9},{9,8},{10,11... | collective-permute-start | bytes 196616 | tf_op jit(solution)/shard_map/ppermute | solution.py:355
  121.3 6.3 %collective-permute-start.40 = (bf16[128,256]{1,0:T(8,128)(2,1)S(1)}, bf16[128,256]{1,0:T(8,128)(2,1)S(1)}, u32[]{:S(2)}, u32[]{:S(2)}) collective-permute-start(bf16[128,256]{1,0:T(8,128)(2,1)S(1)} %collective-permute-done.36.refs_1_), channel_id=1, source_target_pairs={{0,1},{1,0},{2,3},{3,2},{4,5},{5,4},{6,7},{7,6},{8,9},{9,8},{10,11... | collective-permute-start | bytes 196616 | tf_op jit(solution)/shard_map/ppermute | solution.py:355
  121.8 5.8 %collective-permute-start.41 = (bf16[128,256]{1,0:T(8,128)(2,1)S(1)}, bf16[128,256]{1,0:T(8,128)(2,1)S(1)}, u32[]{:S(2)}, u32[]{:S(2)}) collective-permute-start(bf16[128,256]{1,0:T(8,128)(2,1)S(1)} %collective-permute-done.37.refs_2_), channel_id=1, source_target_pairs={{0,1},{1,0},{2,3},{3,2},{4,5},{5,4},{6,7},{7,6},{8,9},{9,8},{10,11... | collective-permute-start | bytes 196616 | tf_op jit(solution)/shard_map/ppermute | solution.py:355
  121.8 5.7 %collective-permute-start.42 = (bf16[128,256]{1,0:T(8,128)(2,1)S(1)}, bf16[128,256]{1,0:T(8,128)(2,1)S(1)}, u32[]{:S(2)}, u32[]{:S(2)}) collective-permute-start(bf16[128,256]{1,0:T(8,128)(2,1)S(1)} %collective-permute-done.38.refs_3_), channel_id=1, source_target_pairs={{0,1},{1,0},{2,3},{3,2},{4,5},{5,4},{6,7},{7,6},{8,9},{9,8},{10,11... | collective-permute-start | bytes 196616 | tf_op jit(solution)/shard_map/ppermute | solution.py:355
  122.3 4.4 %copy-start.21 = (bf16[128,512]{1,0:T(8,128)(2,1)S(1)}, bf16[128,512]{1,0:T(8,128)(2,1)}, u32[]{:S(2)}) copy-start(bf16[128,512]{1,0:T(8,128)(2,1)} %c_ref.1) | copy-start | bytes 393220
  122.3 4.4 %copy-start.22 = (f32[3,512]{1,0:T(4,128)S(1)}, f32[3,512]{1,0:T(4,128)}, u32[]{:S(2)}) copy-start(f32[3,512]{1,0:T(4,128)} %taps_ref.1) | copy-start | bytes 18436
  (10 other events, 12.2 us)

commit v2 on v1

--- a/solution.py
+++ b/solution.py
@@ -112,17 +112,16 @@
     )
 
 
-def load_body(wg, wu, wd, wg_out, wu_out, wd_out, sems):
-    pairs = [(wg, wg_out), (wu, wu_out), (wd, wd_out)]
-    rows = wg.shape[0]
+def load_body(n_row, wg, wu, wd, *refs):
+    rows_in, (wg_out, wu_out, wd_out, joined, sems) = refs[:n_row], refs[n_row:]
+    rows, tok = wg.shape[0], joined.shape[0] // n_row
     step = -(-rows // 8 // LOAD_CUTS) * 8
-    copies = []
-    for f, n in pairs:
+    pairs = [(ref, joined.at[i * tok : (i + 1) * tok, :]) for i, ref in enumerate(rows_in)]
+    for f, n in ((wg, wg_out), (wu, wu_out), (wd, wd_out)):
         for at in range(0, rows, step):
             cut = pl.ds(at, min(step, rows - at))
-            copies.append(
-                pltpu.make_async_copy(f.at[cut, :], n.at[cut, :], sems.at[len(copies)])
-            )
+            pairs.append((f.at[cut, :], n.at[cut, :]))
+    copies = [pltpu.make_async_copy(f, n, sems.at[i]) for i, (f, n) in enumerate(pairs)]
     for copy in copies:
         copy.start()
     for copy in copies:
@@ -397,12 +396,12 @@
         flops=tok * ch,
         scratch=[pltpu.VMEM((tok, ch), BF)] * 2 + [pltpu.SemaphoreType.DMA((2,))],
     )[0]
-    weights = call(
-        load_body, [shape((ff, ch * n_tp))] * 3, weights, smem=0, hbm=range(3),
-        scratch=[pltpu.SemaphoreType.DMA((3 * LOAD_CUTS,))],
-    )
     row = [send_sp(mixed, 0, rx) for rx in range(nx)]
-    row = call(join_body, [shape((nx * tok, ch))], row, smem=0, flops=tok)[0]
+    *weights, row = call(
+        functools.partial(load_body, nx),
+        [shape((ff, ch * n_tp))] * 3 + [shape((nx * tok, ch))], [*weights, *row], smem=0,
+        hbm=range(3 + nx), scratch=[pltpu.SemaphoreType.DMA((3 * LOAD_CUTS + nx,))],
+    )
     mixed_all = [row]
     for _ in range(1, nz):
         row = send_sp(row, 1, 0)

time: 131 us -> 135 us (1.031)
  the two profiles are of different devices: /device:TPU:0 before, /device:TPU:9 now
where the time goes in v2:
time: 135 us; the launch traced here: 134 us
  starting transfers between devices  73.4 us (54%)
  Pallas kernels  34.7 us (26%)
  waiting for transfers between devices  17.3 us (13%)
  local copies, waits for them, and re-layouts  7.24 us (5%)
    pallas_call x24, Pallas kernels, call(): pl.pallas_call(body, out_shape=tuple(outs), in_specs=[SMEM if i < smem el...  34.7 us
    ppermute x22, starting transfers between devices, send_sp(): return lax.ppermute(v, 'sp', sp_perm(rz, rx))  29.9 us
    ppermute x18, starting transfers between devices, send_core(): return lax.ppermute(v, 'tp', [(k, k ^ 1) for k in range(n_tp)])  29.5 us
    ppermute x7, waiting for transfers between devices, send_y(): lax.ppermute(v, 'tp', [(k, (k // 2 + jy) % ny * 2 + k % 2) for k in range...  8.15 us
    unnamed x54, local copies, waits for them, and re-layouts  7.15 us
    ppermute x22, waiting for transfers between devices, send_sp(): return lax.ppermute(v, 'sp', sp_perm(rz, rx))  7.02 us
    ppermute x7, starting transfers between devices, send_y(): lax.ppermute(v, 'tp', [(k, (k // 2 + jy) % ny * 2 + k % 2) for k in range...  5.51 us
    ppermute x1, starting transfers between devices, local(): high = lax.ppermute(first, 'sp', [(b, a) for a, b in up_pairs])  5.15 us
  transfers between devices with their start and end apart: 49, of which 14 were waited for; matrix products, arithmetic and copies ran while one was open for 0% of the time, Pallas kernels for 20%

profile of v2, /device:TPU:9, one launch (start us, length us, event | category | flops | bytes accessed | tf_op | source)
XLA Modules:
  0.0 134.1 jit_solution(2925674911778386865)
XLA Ops:
  0.7 2.1 %shard_map.189 = (bf16[128,512]{1,0:T(8,128)(2,1)S(1)}, bf16[128,512]{1,0:T(8,128)(2,1)S(1)}, bf16[128,512]{1,0:T(8,128)(2,1)S(1)}, bf16[128,512]{1,0:T(8,128)(2...) custom-call(s32[2]{0:T(128)S(1)} %pad_add_fusion.3.me_ref, ...), custom_call_target="tpu_custom_call" | custom-call | flops 134217728 | bytes 1312776 | tf_op jit(solution)/shard_map/pallas_call | solution.py:29
  2.9 1.4 %collective-permute-start.4 = (bf16[128,512]{1,0:T(8,128)(2,1)S(1)}, bf16[128,512]{1,0:T(8,128)(2,1)S(1)}, u32[]{:S(2)}, u32[]{:S(2)}) collective-permute-start(bf16[128,512]{1,0:T(8,128)(2,1)S(1)} %get-tuple-element.66), channel_id=1, source_target_pairs={{0,8},{4,12},{8,16},{12,20},{16,24},{20,28},{24,0},{28,4},{1,9},{5... | collective-permute-start | bytes 393224 | tf_op jit(solution)/shard_map/ppermute | solution.py:348
  4.2 2.2 %collective-permute-start.5 = (bf16[128,512]{1,0:T(8,128)(2,1)S(1)}, bf16[128,512]{1,0:T(8,128)(2,1)S(1)}, u32[]{:S(2)}, u32[]{:S(2)}) collective-permute-start(bf16[128,512]{1,0:T(8,128)(2,1)S(1)} %get-tuple-element.67), channel_id=1, source_target_pairs={{0,12},{4,8},{8,20},{12,16},{16,28},{20,24},{24,4},{28,0},{1,13},{... | collective-permute-start | bytes 393224 | tf_op jit(solution)/shard_map/ppermute | solution.py:348
  6.7 1.0 collective-permute-start.10
  7.7 2.3 %collective-permute-start.11 = (bf16[128,512]{1,0:T(8,128)(2,1)S(1)}, bf16[128,512]{1,0:T(8,128)(2,1)S(1)}, u32[]{:S(2)}, u32[]{:S(2)}) collective-permute-start(bf16[128,512]{1,0:T(8,128)(2,1)S(1)} %get-tuple-element.74), channel_id=1, source_target_pairs={{0,20},{4,16},{8,28},{12,24},{16,4},{20,0},{24,12},{28,8},{1,21},{... | collective-permute-start | bytes 393224 | tf_op jit(solution)/shard_map/ppermute | solution.py:348
  10.2 0.9 collective-permute-done.5.refs_1_
  11.1 1.3 collective-permute-start.7
  12.4 1.2 collective-permute-done.refs_1_
  13.5 8.1 %collective-permute-start.6 = (bf16[256,512]{1,0:T(8,128)(2,1)S(1)}, bf16[256,512]{1,0:T(8,128)(2,1)S(1)}, u32[]{:S(2)}, u32[]{:S(2)}) collective-permute-start(bf16[256,512]{1,0:T(8,128)(2,1)S(1)} %shard_map.191.refs_4_.refs_6_), channel_id=1, source_target_pairs={{0,1},{1,0},{2,3},{3,2},{4,5},{5,4},{6,7},{7,6},{8,9},{9,8},{10,11... | collective-permute-start | bytes 786440 | tf_op jit(solution)/shard_map/ppermute | solution.py:354
  22.0 1.6 %collective-permute-done.11.refs_1_ = bf16[128,512]{1,0:T(8,128)(2,1)S(1)} collective-permute-done((bf16[128,512]{1,0:T(8,128)(2,1)S(1)}, bf16[128,512]{1,0:T(8,128)(2,1)S(1)}, u32[]{:S(2)}, u32[]{:S(2)}) %collective-permute-start.11) | collective-permute-done | bytes 131104 | tf_op jit(solution)/shard_map/ppermute | solution.py:348
  23.6 1.7 %collective-permute-start.16 = (bf16[128,512]{1,0:T(8,128)(2,1)S(1)}, bf16[128,512]{1,0:T(8,128)(2,1)S(1)}, u32[]{:S(2)}, u32[]{:S(2)}) collective-permute-start(bf16[128,512]{1,0:T(8,128)(2,1)S(1)} %get-tuple-element.76), channel_id=1, source_target_pairs={{0,28},{4,24},{8,4},{12,0},{16,12},{20,8},{24,20},{28,16},{1,29},{... | collective-permute-start | bytes 393224 | tf_op jit(solution)/shard_map/ppermute | solution.py:348
  25.3 1.0 shard_map.192.refs_0_
  26.4 1.3 collective-permute-start.9
  27.7 0.7 collective-permute-done.16.refs_1_
  28.3 2.5 %collective-permute-start.1 = (bf16[256,512]{1,0:T(8,128)(2,1)S(1)}, bf16[256,512]{1,0:T(8,128)(2,1)S(1)}, u32[]{:S(2)}, u32[]{:S(2)}) collective-permute-start(bf16[256,512]{1,0:T(8,128)(2,1)S(1)} %shard_map.190.refs_0_.refs_2_), channel_id=1, source_target_pairs={{0,1},{1,0},{2,3},{3,2},{4,5},{5,4},{6,7},{7,6},{8,9},{9,8},{10,11... | collective-permute-start | bytes 786440 | tf_op jit(solution)/shard_map/ppermute | solution.py:354
  30.8 2.1 %collective-permute-done.9.refs_1_ = bf16[128,512]{1,0:T(8,128)(2,1)S(1)} collective-permute-done((bf16[128,512]{1,0:T(8,128)(2,1)S(1)}, bf16[128,512]{1,0:T(8,128)(2,1)S(1)}, u32[]{:S(2)}, u32[]{:S(2)}) %collective-permute-start.9) | collective-permute-done | bytes 131104 | tf_op jit(solution)/shard_map/ppermute | solution.py:348
  33.0 1.2 collective-permute-start.13
  34.2 0.7 collective-permute-start.18
  34.8 0.8 collective-permute-start.8
  35.9 3.7 %shard_map.193 = (bf16[704,2048]{1,0:T(8,128)(2,1)S(1)}, bf16[704,2048]{1,0:T(8,128)(2,1)S(1)}, bf16[704,2048]{1,0:T(8,128)(2,1)S(1)}, bf16[256,512]{1,0:T(8,128)(2,1)S(1)}) custom-call(bf16[704,2048]{1,0:T(8,128)(2,1)} %bitcast.35, bf16[704,2048]{1,0:T(8,128)(2,1)} %bitcast.36, bf16[704,2048]{1,0:T(8,128)(2,1)} %bitcast.37, bf16[128,512]{1,0:T(8,128)(2,1)} %copy-done.6, ...), custom_call_target="tpu_custom_call" | custom-call | bytes 17825792 | tf_op jit(solution)/shard_map/pallas_call | solution.py:29
  39.7 0.5 collective-permute-start.12
  40.3 2.4 %collective-permute-start.17 = (bf16[256,512]{1,0:T(8,128)(2,1)S(1)}, bf16[256,512]{1,0:T(8,128)(2,1)S(1)}, u32[]{:S(2)}, u32[]{:S(2)}) collective-permute-start(bf16[256,512]{1,0:T(8,128)(2,1)S(1)} %shard_map.196.refs_4_.refs_14_), channel_id=1, source_target_pairs={{0,1},{1,0},{2,3},{3,2},{4,5},{5,4},{6,7},{7,6},{8,9},{9,8},{10,11... | collective-permute-start | bytes 786440 | tf_op jit(solution)/shard_map/ppermute | solution.py:354
  42.7 3.2 %collective-permute-done.18.refs_6_.refs_16_ = bf16[256,512]{1,0:T(8,128)(2,1)S(1)} collective-permute-done((bf16[256,512]{1,0:T(8,128)(2,1)S(1)}, bf16[256,512]{1,0:T(8,128)(2,1)S(1)}, u32[]{:S(2)}, u32[]{:S(2)}) %collective-permute-start.18) | collective-permute-done | bytes 262176 | tf_op jit(solution)/shard_map/ppermute | solution.py:351
  45.9 1.4 %collective-permute-start.14 = (bf16[256,512]{1,0:T(8,128)(2,1)S(1)}, bf16[256,512]{1,0:T(8,128)(2,1)S(1)}, u32[]{:S(2)}, u32[]{:S(2)}) collective-permute-start(bf16[256,512]{1,0:T(8,128)(2,1)S(1)} %collective-permute-done.13.refs_2_.refs_12_), channel_id=1, source_target_pairs={{0,1},{1,0},{2,3},{3,2},{4,5},{5,4},{6,7},{7,6},{8,9},{9,8},{10,11... | collective-permute-start | bytes 786440 | tf_op jit(solution)/shard_map/ppermute | solution.py:354
  47.3 5.0 %shard_map.194 = (bf16[256,704]{1,0:T(8,128)(2,1)S(1)}, bf16[256,704]{1,0:T(8,128)(2,1)S(1)}, bf16[256,704]{1,0:T(8,128)(2,1)S(1)}, bf16[256,512]{1,0:T(8,128)(2...) custom-call(s32[4]{0:T(128)S(1)} %pad_add_fusion.blk_ref, ...), custom_call_target="tpu_custom_call" | custom-call | flops 3690987520 | bytes 12877856 | tf_op jit(solution)/shard_map/pallas_call | solution.py:29
  52.3 0.7 copy-done.7
  53.1 0.7 copy-done.11
  53.8 0.7 copy-done.15
  54.6 5.0 %shard_map.197 = (bf16[256,704]{1,0:T(8,128)(2,1)S(1)}, bf16[256,704]{1,0:T(8,128)(2,1)S(1)}, bf16[256,704]{1,0:T(8,128)(2,1)S(1)}, bf16[256,512]{1,0:T(8,128)(2...) custom-call(s32[4]{0:T(128)S(1)} %pad_add_fusion.blk_ref, ...), custom_call_target="tpu_custom_call" | custom-call | flops 3690987520 | bytes 12877856 | tf_op jit(solution)/shard_map/pallas_call | solution.py:29
  59.7 0.6 collective-permute-start.26
  60.4 0.4 collective-permute-start.20
  60.9 0.6 collective-permute-done.26.refs_1_
  62.0 1.3 collective-permute-start.28
  63.4 0.6 collective-permute-start.22
  64.0 1.7 %collective-permute-start.44 = (bf16[256,512]{1,0:T(8,128)(2,1)S(1)}, bf16[256,512]{1,0:T(8,128)(2,1)}, u32[]{:S(2)}, u32[]{:S(2)}) collective-permute-start(bf16[256,512]{1,0:T(8,128)(2,1)S(1)} %get-tuple-element.109.refs_0_), channel_id=1, source_target_pairs={{0,8},{4,12},{8,16},{12,20},{16,24},{20,28},{24,0},{28,4},{1,9},{5... | collective-permute-start | bytes 786440 | tf_op jit(solution)/shard_map/ppermute | solution.py:348
  65.7 3.9 %collective-permute-done.28.refs_1_ = bf16[256,512]{1,0:T(8,128)(2,1)S(1)} collective-permute-done((bf16[256,512]{1,0:T(8,128)(2,1)S(1)}, bf16[256,512]{1,0:T(8,128)(2,1)S(1)}, u32[]{:S(2)}, u32[]{:S(2)}) %collective-permute-start.28) | collective-permute-done | bytes 262176 | tf_op jit(solution)/shard_map/ppermute | solution.py:351
  69.7 3.8 %collective-permute-start.29 = (bf16[64,512]{1,0:T(8,128)(2,1)S(1)}, bf16[64,512]{1,0:T(8,128)(2,1)S(1)}, u32[]{:S(2)}, u32[]{:S(2)}) collective-permute-start(bf16[64,512]{1,0:T(8,128)(2,1)S(1)} %get-tuple-element.99), channel_id=1, source_target_pairs={{0,16},{4,20},{8,24},{12,28},{16,0},{20,4},{24,8},{28,12},{1,17},{... | collective-permute-start | bytes 196616 | tf_op jit(solution)/shard_map/ppermute | solution.py:348
  73.5 0.7 collective-permute-start.31
  74.2 0.9 collective-permute-done.22.refs_1_
  75.1 2.1 %collective-permute-start.32 = (bf16[64,512]{1,0:T(8,128)(2,1)S(1)}, bf16[64,512]{1,0:T(8,128)(2,1)S(1)}, u32[]{:S(2)}, u32[]{:S(2)}) collective-permute-start(bf16[64,512]{1,0:T(8,128)(2,1)S(1)} %get-tuple-element.102), channel_id=1, source_target_pairs={{0,12},{4,8},{8,20},{12,16},{16,28},{20,24},{24,4},{28,0},{1,13},{... | collective-permute-start | bytes 196616 | tf_op jit(solution)/shard_map/ppermute | solution.py:348
  77.3 0.9 collective-permute-start.23
  78.4 5.8 %collective-permute-start.25 = (bf16[64,512]{1,0:T(8,128)(2,1)S(1)}, bf16[64,512]{1,0:T(8,128)(2,1)S(1)}, u32[]{:S(2)}, u32[]{:S(2)}) collective-permute-start(bf16[64,512]{1,0:T(8,128)(2,1)S(1)} %get-tuple-element.92), channel_id=1, source_target_pairs={{0,28},{4,24},{8,4},{12,0},{16,12},{20,8},{24,20},{28,16},{1,29},{... | collective-permute-start | bytes 196616 | tf_op jit(solution)/shard_map/ppermute | solution.py:348
  84.2 0.7 shard_map.201.sel_ref
  85.8 4.7 %collective-permute-start.33 = (bf16[128,512]{1,0:T(8,128)(2,1)S(1)}, bf16[128,512]{1,0:T(8,128)(2,1)}, u32[]{:S(2)}, u32[]{:S(2)}) collective-permute-start(bf16[128,512]{1,0:T(8,128)(2,1)S(1)} %shard_map.206.refs_0_), channel_id=1, source_target_pairs={{0,1},{1,0},{2,3},{3,2},{4,5},{5,4},{6,7},{7,6},{8,9},{9,8},{10,11... | collective-permute-start | bytes 393224 | tf_op jit(solution)/shard_map/ppermute | solution.py:354
  90.6 5.0 %collective-permute-start.35 = (bf16[128,512]{1,0:T(8,128)(2,1)}, bf16[128,512]{1,0:T(8,128)(2,1)}, u32[]{:S(2)}, u32[]{:S(2)}) collective-permute-start(bf16[128,512]{1,0:T(8,128)(2,1)} %collective-permute-done.34.refs_2_), channel_id=1, source_target_pairs={{0,1},{1,0},{2,3},{3,2},{4,5},{5,4},{6,7},{7,6},{8,9},{9,8},{10,11... | collective-permute-start | bytes 393224 | tf_op jit(solution)/shard_map/ppermute | solution.py:354
  95.8 1.2 collective-permute-done.35.refs_3_
  97.0 1.1 shard_map.207
  98.2 0.9 copy-done.1
  99.1 0.9 copy-done.3
  100.1 0.9 copy-done.5
  101.0 1.0 copy-done.16
  102.0 1.0 copy-done.18
  103.0 3.1 %shard_map.200 = bf16[704,2048]{1,0:T(8,128)(2,1)} custom-call(s32[4]{0:T(128)S(1)} %pad_add_fusion.blk_ref, bf16[256,704]{1,0:T(8,128)(2,1)S(1)} %copy-done.16, bf16[256,704]{1,0:T(8,128)(2,1)S(1)} %copy-done.18, bf16[256,512]{1,0:T(8,128)(2,1)S(1)} %shard_map.190.refs_0_.refs_2_, bf16[256,512]{1,0:T(8,128)(2,1)S(1)} %collective-permute-done.1.refs_1_.refs_3_, ...), custom_call_target="tpu_custom_call" | custom-call | flops 1476395008 | bytes 7798800 | tf_op jit(solution)/shard_map/pallas_call | solution.py:29
  106.2 2.6 %shard_map.211 = (bf16[128,512]{1,0:T(8,128)(2,1)S(1)}, bf16[128,512]{1,0:T(8,128)(2,1)}, bf16[1,512]{1,0:T(2,128)(2,1)S(1)}, bf16[1,512]{1,0:T(2,128)(2,1)S(1)}) custom-call(bf16[128,2048]{1,0:T(8,128)(2,1)S(1)} %get-tuple-element.114.full_ref, bf16[2048,512]{1,0:T(8,128)(2,1)} %wo_far.1, bf16[128,512]{1,0:T(8,128)(2,1)} %gb_far.1, bf16[128,512]{1,0:T(8,128)(2,1)} %co_far.1), custom_call_target="tpu_custom_call" | custom-call | flops 268435456 | bytes 3147776 | tf_op jit(solution)/shard_map/pallas_call | solution.py:29
  108.7 3.4 %collective-permute-start.47 = (bf16[1,512]{1,0:T(2,128)(2,1)S(1)}, bf16[1,512]{1,0:T(2,128)(2,1)S(1)}, u32[]{:S(2)}, u32[]{:S(2)}) collective-permute-start(bf16[1,512]{1,0:T(2,128)(2,1)S(1)} %get-tuple-element.117), channel_id=1, source_target_pairs={{0,4},{4,8},{8,12},{12,16},{16,20},{20,24},{24,28},{1,5},{5,9},{9,... | collective-permute-start | bytes 3080 | tf_op jit(solution)/shard_map/ppermute | solution.py:489
  112.5 3.6 %collective-permute-start.38 = (bf16[128,256]{1,0:T(8,128)(2,1)S(1)}, bf16[128,256]{1,0:T(8,128)(2,1)S(1)}, u32[]{:S(2)}, u32[]{:S(2)}) collective-permute-start(bf16[128,256]{1,0:T(8,128)(2,1)S(1)} %get-tuple-element.107), channel_id=1, source_target_pairs={{0,16},{4,20},{8,24},{12,28},{16,0},{20,4},{24,8},{28,12},{1,17},{... | collective-permute-start | bytes 196616 | tf_op jit(solution)/shard_map/ppermute | solution.py:348
  116.5 3.1 %shard_map.199 = bf16[704,2048]{1,0:T(8,128)(2,1)} custom-call(s32[4]{0:T(128)S(1)} %pad_add_fusion.blk_ref, bf16[256,704]{1,0:T(8,128)(2,1)S(1)} %copy-done.12, bf16[256,704]{1,0:T(8,128)(2,1)S(1)} %copy-done.14, bf16[256,512]{1,0:T(8,128)(2,1)S(1)} %shard_map.190.refs_0_.refs_2_, bf16[256,512]{1,0:T(8,128)(2,1)S(1)} %collective-permute-done.1.refs_1_.refs_3_, ...), custom_call_target="tpu_custom_call" | custom-call | flops 1476395008 | bytes 7798800 | tf_op jit(solution)/shard_map/pallas_call | solution.py:29
  119.6 5.2 %collective-permute-start.48 = (bf16[1,512]{1,0:T(2,128)(2,1)S(1)}, bf16[1,512]{1,0:T(2,128)(2,1)S(1)}, u32[]{:S(2)}, u32[]{:S(2)}) collective-permute-start(bf16[1,512]{1,0:T(2,128)(2,1)S(1)} %get-tuple-element.118), channel_id=1, source_target_pairs={{4,0},{8,4},{12,8},{16,12},{20,16},{24,20},{28,24},{5,1},{9,5},{13... | collective-permute-start | bytes 3080 | tf_op jit(solution)/shard_map/ppermute | solution.py:490
  124.8 2.1 %collective-permute-start.40 = (bf16[128,256]{1,0:T(8,128)(2,1)S(1)}, bf16[128,256]{1,0:T(8,128)(2,1)S(1)}, u32[]{:S(2)}, u32[]{:S(2)}) collective-permute-start(bf16[128,256]{1,0:T(8,128)(2,1)S(1)} %get-tuple-element.105.refs_0_), channel_id=1, source_target_pairs={{0,1},{1,0},{2,3},{3,2},{4,5},{5,4},{6,7},{7,6},{8,9},{9,8},{10,11... | collective-permute-start | bytes 196616 | tf_op jit(solution)/shard_map/ppermute | solution.py:354
  127.0 0.4 collective-permute-start.42
  127.6 3.1 %shard_map.198 = bf16[704,2048]{1,0:T(8,128)(2,1)} custom-call(s32[4]{0:T(128)S(1)} %pad_add_fusion.blk_ref, bf16[256,704]{1,0:T(8,128)(2,1)S(1)} %copy-done.8, bf16[256,704]{1,0:T(8,128)(2,1)S(1)} %copy-done.10, bf16[256,512]{1,0:T(8,128)(2,1)S(1)} %shard_map.190.refs_0_.refs_2_, bf16[256,512]{1,0:T(8,128)(2,1)S(1)} %collective-permute-done.1.refs_1_.refs_3_, ...), custom_call_target="tpu_custom_call" | custom-call | flops 1476395008 | bytes 7798800 | tf_op jit(solution)/shard_map/pallas_call | solution.py:29
  130.7 1.2 shard_map.209
  132.0 0.8 shard_map.212
  132.9 1.3 shard_map.210
  (116 shorter events, 4.6 us)
Async XLA Ops:
  2.9 7.1 %collective-permute-start.4 = (bf16[128,512]{1,0:T(8,128)(2,1)S(1)}, bf16[128,512]{1,0:T(8,128)(2,1)S(1)}, u32[]{:S(2)}, u32[]{:S(2)}) collective-permute-start(bf16[128,512]{1,0:T(8,128)(2,1)S(1)} %get-tuple-element.66), channel_id=1, source_target_pairs={{0,8},{4,12},{8,16},{12,20},{16,24},{20,28},{24,0},{28,4},{1,9},{5... | collective-permute-start | bytes 393224 | tf_op jit(solution)/shard_map/ppermute | solution.py:348
  4.2 6.8 %collective-permute-start.5 = (bf16[128,512]{1,0:T(8,128)(2,1)S(1)}, bf16[128,512]{1,0:T(8,128)(2,1)S(1)}, u32[]{:S(2)}, u32[]{:S(2)}) collective-permute-start(bf16[128,512]{1,0:T(8,128)(2,1)S(1)} %get-tuple-element.67), channel_id=1, source_target_pairs={{0,12},{4,8},{8,20},{12,16},{16,28},{20,24},{24,4},{28,0},{1,13},{... | collective-permute-start | bytes 393224 | tf_op jit(solution)/shard_map/ppermute | solution.py:348
  6.4 7.1 %collective-permute-start = (bf16[128,512]{1,0:T(8,128)(2,1)S(1)}, bf16[128,512]{1,0:T(8,128)(2,1)S(1)}, u32[]{:S(2)}, u32[]{:S(2)}) collective-permute-start(bf16[128,512]{1,0:T(8,128)(2,1)S(1)} %get-tuple-element.65), channel_id=1, source_target_pairs={{0,4},{4,0},{8,12},{12,8},{16,20},{20,16},{24,28},{28,24},{1,5},{5... | collective-permute-start | bytes 393224 | tf_op jit(solution)/shard_map/ppermute | solution.py:348
  6.7 15.0 %collective-permute-start.10 = (bf16[128,512]{1,0:T(8,128)(2,1)S(1)}, bf16[128,512]{1,0:T(8,128)(2,1)S(1)}, u32[]{:S(2)}, u32[]{:S(2)}) collective-permute-start(bf16[128,512]{1,0:T(8,128)(2,1)S(1)} %get-tuple-element.73), channel_id=1, source_target_pairs={{0,16},{4,20},{8,24},{12,28},{16,0},{20,4},{24,8},{28,12},{1,17},{... | collective-permute-start | bytes 393224 | tf_op jit(solution)/shard_map/ppermute | solution.py:348
  7.7 16.0 %collective-permute-start.11 = (bf16[128,512]{1,0:T(8,128)(2,1)S(1)}, bf16[128,512]{1,0:T(8,128)(2,1)S(1)}, u32[]{:S(2)}, u32[]{:S(2)}) collective-permute-start(bf16[128,512]{1,0:T(8,128)(2,1)S(1)} %get-tuple-element.74), channel_id=1, source_target_pairs={{0,20},{4,16},{8,28},{12,24},{16,4},{20,0},{24,12},{28,8},{1,21},{... | collective-permute-start | bytes 393224 | tf_op jit(solution)/shard_map/ppermute | solution.py:348
  10.0 16.4 %collective-permute-start.15 = (bf16[128,512]{1,0:T(8,128)(2,1)S(1)}, bf16[128,512]{1,0:T(8,128)(2,1)S(1)}, u32[]{:S(2)}, u32[]{:S(2)}) collective-permute-start(bf16[128,512]{1,0:T(8,128)(2,1)S(1)} %get-tuple-element.75), channel_id=1, source_target_pairs={{0,24},{4,28},{8,0},{12,4},{16,8},{20,12},{24,16},{28,20},{1,25},{... | collective-permute-start | bytes 393224 | tf_op jit(solution)/shard_map/ppermute | solution.py:348
  11.1 23.1 %collective-permute-start.7 = (bf16[256,512]{1,0:T(8,128)(2,1)S(1)}, bf16[256,512]{1,0:T(8,128)(2,1)S(1)}, u32[]{:S(2)}, u32[]{:S(2)}) collective-permute-start(bf16[256,512]{1,0:T(8,128)(2,1)S(1)} %shard_map.191.refs_4_.refs_6_), channel_id=1, source_target_pairs={{0,2},{1,3},{2,0},{3,1},{4,6},{5,7},{6,4},{7,5},{8,10},{9,11},{10,... | collective-permute-start | bytes 786440 | tf_op jit(solution)/shard_map/ppermute | solution.py:351
  13.5 21.3 %collective-permute-start.6 = (bf16[256,512]{1,0:T(8,128)(2,1)S(1)}, bf16[256,512]{1,0:T(8,128)(2,1)S(1)}, u32[]{:S(2)}, u32[]{:S(2)}) collective-permute-start(bf16[256,512]{1,0:T(8,128)(2,1)S(1)} %shard_map.191.refs_4_.refs_6_), channel_id=1, source_target_pairs={{0,1},{1,0},{2,3},{3,2},{4,5},{5,4},{6,7},{7,6},{8,9},{9,8},{10,11... | collective-permute-start | bytes 786440 | tf_op jit(solution)/shard_map/ppermute | solution.py:354
  21.7 14.0 %collective-permute-start.2 = (bf16[256,512]{1,0:T(8,128)(2,1)S(1)}, bf16[256,512]{1,0:T(8,128)(2,1)S(1)}, u32[]{:S(2)}, u32[]{:S(2)}) collective-permute-start(bf16[256,512]{1,0:T(8,128)(2,1)S(1)} %shard_map.190.refs_0_.refs_2_), channel_id=1, source_target_pairs={{0,2},{1,3},{2,0},{3,1},{4,6},{5,7},{6,4},{7,5},{8,10},{9,11},{10,... | collective-permute-start | bytes 786440 | tf_op jit(solution)/shard_map/ppermute | solution.py:351
  23.6 4.7 %collective-permute-start.16 = (bf16[128,512]{1,0:T(8,128)(2,1)S(1)}, bf16[128,512]{1,0:T(8,128)(2,1)S(1)}, u32[]{:S(2)}, u32[]{:S(2)}) collective-permute-start(bf16[128,512]{1,0:T(8,128)(2,1)S(1)} %get-tuple-element.76), channel_id=1, source_target_pairs={{0,28},{4,24},{8,4},{12,0},{16,12},{20,8},{24,20},{28,16},{1,29},{... | collective-permute-start | bytes 393224 | tf_op jit(solution)/shard_map/ppermute | solution.py:348
  26.3 9.6 %copy-start.6 = (bf16[128,512]{1,0:T(8,128)(2,1)}, bf16[128,512]{1,0:T(8,128)(2,1)S(1)}, u32[]{:S(2)}) copy-start(bf16[128,512]{1,0:T(8,128)(2,1)S(1)} %shard_map.192.refs_0_) | copy-start | bytes 393220
  26.4 6.6 %collective-permute-start.9 = (bf16[128,512]{1,0:T(8,128)(2,1)S(1)}, bf16[128,512]{1,0:T(8,128)(2,1)S(1)}, u32[]{:S(2)}, u32[]{:S(2)}) collective-permute-start(bf16[128,512]{1,0:T(8,128)(2,1)S(1)} %shard_map.192.refs_0_), channel_id=1, source_target_pairs={{0,4},{4,0},{8,12},{12,8},{16,20},{20,16},{24,28},{28,24},{1,5},{5... | collective-permute-start | bytes 393224 | tf_op jit(solution)/shard_map/ppermute | solution.py:348
  28.3 11.4 %collective-permute-start.1 = (bf16[256,512]{1,0:T(8,128)(2,1)S(1)}, bf16[256,512]{1,0:T(8,128)(2,1)S(1)}, u32[]{:S(2)}, u32[]{:S(2)}) collective-permute-start(bf16[256,512]{1,0:T(8,128)(2,1)S(1)} %shard_map.190.refs_0_.refs_2_), channel_id=1, source_target_pairs={{0,1},{1,0},{2,3},{3,2},{4,5},{5,4},{6,7},{7,6},{8,9},{9,8},{10,11... | collective-permute-start | bytes 786440 | tf_op jit(solution)/shard_map/ppermute | solution.py:354
  33.0 7.3 %collective-permute-start.13 = (bf16[256,512]{1,0:T(8,128)(2,1)S(1)}, bf16[256,512]{1,0:T(8,128)(2,1)S(1)}, u32[]{:S(2)}, u32[]{:S(2)}) collective-permute-start(bf16[256,512]{1,0:T(8,128)(2,1)S(1)} %shard_map.195.refs_0_.refs_10_), channel_id=1, source_target_pairs={{0,2},{1,3},{2,0},{3,1},{4,6},{5,7},{6,4},{7,5},{8,10},{9,11},{10,... | collective-permute-start | bytes 786440 | tf_op jit(solution)/shard_map/ppermute | solution.py:351
  34.2 11.7 %collective-permute-start.18 = (bf16[256,512]{1,0:T(8,128)(2,1)S(1)}, bf16[256,512]{1,0:T(8,128)(2,1)S(1)}, u32[]{:S(2)}, u32[]{:S(2)}) collective-permute-start(bf16[256,512]{1,0:T(8,128)(2,1)S(1)} %shard_map.196.refs_4_.refs_14_), channel_id=1, source_target_pairs={{0,2},{1,3},{2,0},{3,1},{4,6},{5,7},{6,4},{7,5},{8,10},{9,11},{10,... | collective-permute-start | bytes 786440 | tf_op jit(solution)/shard_map/ppermute | solution.py:351
  34.8 12.5 %collective-permute-start.8 = (bf16[256,512]{1,0:T(8,128)(2,1)S(1)}, bf16[256,512]{1,0:T(8,128)(2,1)S(1)}, u32[]{:S(2)}, u32[]{:S(2)}) collective-permute-start(bf16[256,512]{1,0:T(8,128)(2,1)S(1)} %collective-permute-done.7.refs_6_.refs_8_), channel_id=1, source_target_pairs={{0,1},{1,0},{2,3},{3,2},{4,5},{5,4},{6,7},{7,6},{8,9},{9,8},{10,11... | collective-permute-start | bytes 786440 | tf_op jit(solution)/shard_map/ppermute | solution.py:354
  35.7 11.6 %collective-permute-start.3 = (bf16[256,512]{1,0:T(8,128)(2,1)S(1)}, bf16[256,512]{1,0:T(8,128)(2,1)S(1)}, u32[]{:S(2)}, u32[]{:S(2)}) collective-permute-start(bf16[256,512]{1,0:T(8,128)(2,1)S(1)} %collective-permute-done.2.refs_2_.refs_4_), channel_id=1, source_target_pairs={{0,1},{1,0},{2,3},{3,2},{4,5},{5,4},{6,7},{7,6},{8,9},{9,8},{10,11... | collective-permute-start | bytes 786440 | tf_op jit(solution)/shard_map/ppermute | solution.py:354
  39.7 24.3 %copy-start.19 = (bf16[256,512]{1,0:T(8,128)(2,1)}, bf16[256,512]{1,0:T(8,128)(2,1)S(1)}, u32[]{:S(2)}) copy-start(bf16[256,512]{1,0:T(8,128)(2,1)S(1)} %get-tuple-element.109.refs_0_) | copy-start | bytes 786436
  39.7 14.9 %collective-permute-start.12 = (bf16[256,512]{1,0:T(8,128)(2,1)S(1)}, bf16[256,512]{1,0:T(8,128)(2,1)S(1)}, u32[]{:S(2)}, u32[]{:S(2)}) collective-permute-start(bf16[256,512]{1,0:T(8,128)(2,1)S(1)} %shard_map.195.refs_0_.refs_10_), channel_id=1, source_target_pairs={{0,1},{1,0},{2,3},{3,2},{4,5},{5,4},{6,7},{7,6},{8,9},{9,8},{10,11... | collective-permute-start | bytes 786440 | tf_op jit(solution)/shard_map/ppermute | solution.py:354
  40.3 14.3 %collective-permute-start.17 = (bf16[256,512]{1,0:T(8,128)(2,1)S(1)}, bf16[256,512]{1,0:T(8,128)(2,1)S(1)}, u32[]{:S(2)}, u32[]{:S(2)}) collective-permute-start(bf16[256,512]{1,0:T(8,128)(2,1)S(1)} %shard_map.196.refs_4_.refs_14_), channel_id=1, source_target_pairs={{0,1},{1,0},{2,3},{3,2},{4,5},{5,4},{6,7},{7,6},{8,9},{9,8},{10,11... | collective-permute-start | bytes 786440 | tf_op jit(solution)/shard_map/ppermute | solution.py:354
  45.9 8.7 %collective-permute-start.14 = (bf16[256,512]{1,0:T(8,128)(2,1)S(1)}, bf16[256,512]{1,0:T(8,128)(2,1)S(1)}, u32[]{:S(2)}, u32[]{:S(2)}) collective-permute-start(bf16[256,512]{1,0:T(8,128)(2,1)S(1)} %collective-permute-done.13.refs_2_.refs_12_), channel_id=1, source_target_pairs={{0,1},{1,0},{2,3},{3,2},{4,5},{5,4},{6,7},{7,6},{8,9},{9,8},{10,11... | collective-permute-start | bytes 786440 | tf_op jit(solution)/shard_map/ppermute | solution.py:354
  47.3 7.3 %collective-permute-start.19 = (bf16[256,512]{1,0:T(8,128)(2,1)S(1)}, bf16[256,512]{1,0:T(8,128)(2,1)S(1)}, u32[]{:S(2)}, u32[]{:S(2)}) collective-permute-start(bf16[256,512]{1,0:T(8,128)(2,1)S(1)} %collective-permute-done.18.refs_6_.refs_16_), channel_id=1, source_target_pairs={{0,1},{1,0},{2,3},{3,2},{4,5},{5,4},{6,7},{7,6},{8,9},{9,8},{10,11... | collective-permute-start | bytes 786440 | tf_op jit(solution)/shard_map/ppermute | solution.py:354
  54.6 5.1 %copy-start = (bf16[256,512]{1,0:T(8,128)(2,1)}, bf16[256,512]{1,0:T(8,128)(2,1)S(1)}, u32[]{:S(2)}) copy-start(bf16[256,512]{1,0:T(8,128)(2,1)S(1)} %collective-permute-done.17.refs_5_.refs_15_) | copy-start | bytes 786436
  54.6 5.0 %copy-start.2 = (bf16[256,512]{1,0:T(8,128)(2,1)}, bf16[256,512]{1,0:T(8,128)(2,1)S(1)}, u32[]{:S(2)}) copy-start(bf16[256,512]{1,0:T(8,128)(2,1)S(1)} %collective-permute-done.14.refs_3_.refs_13_) | copy-start | bytes 786436
  54.6 5.0 %copy-start.4 = (bf16[256,512]{1,0:T(8,128)(2,1)}, bf16[256,512]{1,0:T(8,128)(2,1)S(1)}, u32[]{:S(2)}) copy-start(bf16[256,512]{1,0:T(8,128)(2,1)S(1)} %collective-permute-done.19.refs_7_.refs_17_) | copy-start | bytes 786436
  59.7 30.9 %copy-start.9 = (bf16[256,704]{1,0:T(8,128)(2,1)}, bf16[256,704]{1,0:T(8,128)(2,1)S(1)}, u32[]{:S(2)}) copy-start(bf16[256,704]{1,0:T(8,128)(2,1)S(1)} %get-tuple-element.80.refs_1_) | copy-start | bytes 1081348
  59.7 30.9 %copy-start.13 = (bf16[256,704]{1,0:T(8,128)(2,1)}, bf16[256,704]{1,0:T(8,128)(2,1)S(1)}, u32[]{:S(2)}) copy-start(bf16[256,704]{1,0:T(8,128)(2,1)S(1)} %get-tuple-element.82.refs_1_) | copy-start | bytes 1081348
  59.7 30.9 %copy-start.17 = (bf16[256,704]{1,0:T(8,128)(2,1)}, bf16[256,704]{1,0:T(8,128)(2,1)S(1)}, u32[]{:S(2)}) copy-start(bf16[256,704]{1,0:T(8,128)(2,1)S(1)} %get-tuple-element.77.refs_1_) | copy-start | bytes 1081348
  59.7 24.5 %copy-start.24 = (s32[128,2]{0,1:T(2,128)S(1)}, s32[128,2]{0,1:T(2,128)}, u32[]{:S(2)}) copy-start(s32[128,2]{0,1:T(2,128)} %param.17) | copy-start | bytes 3076
  59.7 25.8 %copy-start.20 = (bf16[128,512]{1,0:T(8,128)(2,1)S(1)}, bf16[128,512]{1,0:T(8,128)(2,1)}, u32[]{:S(2)}) copy-start(bf16[128,512]{1,0:T(8,128)(2,1)} %og_ref.1) | copy-start | bytes 393220
  59.7 1.7 %collective-permute-start.26 = (bf16[256,512]{1,0:T(8,128)(2,1)S(1)}, bf16[256,512]{1,0:T(8,128)(2,1)S(1)}, u32[]{:S(2)}, u32[]{:S(2)}) collective-permute-start(bf16[256,512]{1,0:T(8,128)(2,1)S(1)} %get-tuple-element.94), channel_id=1, source_target_pairs={{0,1},{1,0},{2,3},{3,2},{4,5},{5,4},{6,7},{7,6},{8,9},{9,8},{10,11... | collective-permute-start | bytes 786440 | tf_op jit(solution)/shard_map/ppermute | solution.py:354
  60.3 1.5 %collective-permute-start.27 = (bf16[256,512]{1,0:T(8,128)(2,1)S(1)}, bf16[256,512]{1,0:T(8,128)(2,1)S(1)}, u32[]{:S(2)}, u32[]{:S(2)}) collective-permute-start(bf16[256,512]{1,0:T(8,128)(2,1)S(1)} %get-tuple-element.96), channel_id=1, source_target_pairs={{0,1},{1,0},{2,3},{3,2},{4,5},{5,4},{6,7},{7,6},{8,9},{9,8},{10,11... | collective-permute-start | bytes 786440 | tf_op jit(solution)/shard_map/ppermute | solution.py:354
  60.4 2.9 %collective-permute-start.20 = (bf16[256,512]{1,0:T(8,128)(2,1)S(1)}, bf16[256,512]{1,0:T(8,128)(2,1)S(1)}, u32[]{:S(2)}, u32[]{:S(2)}) collective-permute-start(bf16[256,512]{1,0:T(8,128)(2,1)S(1)} %get-tuple-element.84), channel_id=1, source_target_pairs={{0,1},{1,0},{2,3},{3,2},{4,5},{5,4},{6,7},{7,6},{8,9},{9,8},{10,11... | collective-permute-start | bytes 786440 | tf_op jit(solution)/shard_map/ppermute | solution.py:354
  60.8 2.4 %collective-permute-start.21 = (bf16[256,512]{1,0:T(8,128)(2,1)S(1)}, bf16[256,512]{1,0:T(8,128)(2,1)S(1)}, u32[]{:S(2)}, u32[]{:S(2)}) collective-permute-start(bf16[256,512]{1,0:T(8,128)(2,1)S(1)} %get-tuple-element.86), channel_id=1, source_target_pairs={{0,1},{1,0},{2,3},{3,2},{4,5},{5,4},{6,7},{7,6},{8,9},{9,8},{10,11... | collective-permute-start | bytes 786440 | tf_op jit(solution)/shard_map/ppermute | solution.py:354
  62.0 7.7 %collective-permute-start.28 = (bf16[256,512]{1,0:T(8,128)(2,1)S(1)}, bf16[256,512]{1,0:T(8,128)(2,1)S(1)}, u32[]{:S(2)}, u32[]{:S(2)}) collective-permute-start(bf16[256,512]{1,0:T(8,128)(2,1)S(1)} %get-tuple-element.98), channel_id=1, source_target_pairs={{0,2},{1,3},{2,0},{3,1},{4,6},{5,7},{6,4},{7,5},{8,10},{9,11},{10,... | collective-permute-start | bytes 786440 | tf_op jit(solution)/shard_map/ppermute | solution.py:351
  63.4 11.8 %collective-permute-start.22 = (bf16[256,512]{1,0:T(8,128)(2,1)S(1)}, bf16[256,512]{1,0:T(8,128)(2,1)S(1)}, u32[]{:S(2)}, u32[]{:S(2)}) collective-permute-start(bf16[256,512]{1,0:T(8,128)(2,1)S(1)} %get-tuple-element.88), channel_id=1, source_target_pairs={{0,2},{1,3},{2,0},{3,1},{4,6},{5,7},{6,4},{7,5},{8,10},{9,11},{10,... | collective-permute-start | bytes 786440 | tf_op jit(solution)/shard_map/ppermute | solution.py:351
  64.0 13.3 %collective-permute-start.44 = (bf16[256,512]{1,0:T(8,128)(2,1)S(1)}, bf16[256,512]{1,0:T(8,128)(2,1)}, u32[]{:S(2)}, u32[]{:S(2)}) collective-permute-start(bf16[256,512]{1,0:T(8,128)(2,1)S(1)} %get-tuple-element.109.refs_0_), channel_id=1, source_target_pairs={{0,8},{4,12},{8,16},{12,20},{16,24},{20,28},{24,0},{28,4},{1,9},{5... | collective-permute-start | bytes 786440 | tf_op jit(solution)/shard_map/ppermute | solution.py:348
  69.7 8.5 %collective-permute-start.29 = (bf16[64,512]{1,0:T(8,128)(2,1)S(1)}, bf16[64,512]{1,0:T(8,128)(2,1)S(1)}, u32[]{:S(2)}, u32[]{:S(2)}) collective-permute-start(bf16[64,512]{1,0:T(8,128)(2,1)S(1)} %get-tuple-element.99), channel_id=1, source_target_pairs={{0,16},{4,20},{8,24},{12,28},{16,0},{20,4},{24,8},{28,12},{1,17},{... | collective-permute-start | bytes 196616 | tf_op jit(solution)/shard_map/ppermute | solution.py:348
  73.5 4.9 %collective-permute-start.30 = (bf16[64,512]{1,0:T(8,128)(2,1)S(1)}, bf16[64,512]{1,0:T(8,128)(2,1)S(1)}, u32[]{:S(2)}, u32[]{:S(2)}) collective-permute-start(bf16[64,512]{1,0:T(8,128)(2,1)S(1)} %get-tuple-element.100), channel_id=1, source_target_pairs={{0,20},{4,16},{8,28},{12,24},{16,4},{20,0},{24,12},{28,8},{1,21},{... | collective-permute-start | bytes 196616 | tf_op jit(solution)/shard_map/ppermute | solution.py:348
  73.5 11.4 %collective-permute-start.31 = (bf16[64,512]{1,0:T(8,128)(2,1)S(1)}, bf16[64,512]{1,0:T(8,128)(2,1)S(1)}, u32[]{:S(2)}, u32[]{:S(2)}) collective-permute-start(bf16[64,512]{1,0:T(8,128)(2,1)S(1)} %get-tuple-element.101), channel_id=1, source_target_pairs={{0,8},{4,12},{8,16},{12,20},{16,24},{20,28},{24,0},{28,4},{1,9},{5... | collective-permute-start | bytes 196616 | tf_op jit(solution)/shard_map/ppermute | solution.py:348
  75.1 10.0 %collective-permute-start.32 = (bf16[64,512]{1,0:T(8,128)(2,1)S(1)}, bf16[64,512]{1,0:T(8,128)(2,1)S(1)}, u32[]{:S(2)}, u32[]{:S(2)}) collective-permute-start(bf16[64,512]{1,0:T(8,128)(2,1)S(1)} %get-tuple-element.102), channel_id=1, source_target_pairs={{0,12},{4,8},{8,20},{12,16},{16,28},{20,24},{24,4},{28,0},{1,13},{... | collective-permute-start | bytes 196616 | tf_op jit(solution)/shard_map/ppermute | solution.py:348
  77.3 7.9 %collective-permute-start.23 = (bf16[64,512]{1,0:T(8,128)(2,1)S(1)}, bf16[64,512]{1,0:T(8,128)(2,1)S(1)}, u32[]{:S(2)}, u32[]{:S(2)}) collective-permute-start(bf16[64,512]{1,0:T(8,128)(2,1)S(1)} %get-tuple-element.90), channel_id=1, source_target_pairs={{0,4},{4,0},{8,12},{12,8},{16,20},{20,16},{24,28},{28,24},{1,5},{5... | collective-permute-start | bytes 196616 | tf_op jit(solution)/shard_map/ppermute | solution.py:348
  78.2 7.0 %collective-permute-start.24 = (bf16[64,512]{1,0:T(8,128)(2,1)S(1)}, bf16[64,512]{1,0:T(8,128)(2,1)S(1)}, u32[]{:S(2)}, u32[]{:S(2)}) collective-permute-start(bf16[64,512]{1,0:T(8,128)(2,1)S(1)} %get-tuple-element.91), channel_id=1, source_target_pairs={{0,24},{4,28},{8,0},{12,4},{16,8},{20,12},{24,16},{28,20},{1,25},{... | collective-permute-start | bytes 196616 | tf_op jit(solution)/shard_map/ppermute | solution.py:348
  78.4 7.1 %collective-permute-start.25 = (bf16[64,512]{1,0:T(8,128)(2,1)S(1)}, bf16[64,512]{1,0:T(8,128)(2,1)S(1)}, u32[]{:S(2)}, u32[]{:S(2)}) collective-permute-start(bf16[64,512]{1,0:T(8,128)(2,1)S(1)} %get-tuple-element.92), channel_id=1, source_target_pairs={{0,28},{4,24},{8,4},{12,0},{16,12},{20,8},{24,20},{28,16},{1,29},{... | collective-permute-start | bytes 196616 | tf_op jit(solution)/shard_map/ppermute | solution.py:348
  84.9 10.8 %collective-permute-start.45 = (bf16[256,512]{1,0:T(8,128)(2,1)}, bf16[256,512]{1,0:T(8,128)(2,1)}, u32[]{:S(2)}, u32[]{:S(2)}) collective-permute-start(bf16[256,512]{1,0:T(8,128)(2,1)} %collective-permute-done.44.refs_1_), channel_id=1, source_target_pairs={{0,8},{4,12},{8,16},{12,20},{16,24},{20,28},{24,0},{28,4},{1,9},{5... | collective-permute-start | bytes 786440 | tf_op jit(solution)/shard_map/ppermute | solution.py:348
  85.7 4.8 %collective-permute-start.34 = (bf16[128,512]{1,0:T(8,128)(2,1)S(1)}, bf16[128,512]{1,0:T(8,128)(2,1)}, u32[]{:S(2)}, u32[]{:S(2)}) collective-permute-start(bf16[128,512]{1,0:T(8,128)(2,1)S(1)} %shard_map.206.refs_0_), channel_id=1, source_target_pairs={{0,2},{1,3},{2,0},{3,1},{4,6},{5,7},{6,4},{7,5},{8,10},{9,11},{10,... | collective-permute-start | bytes 393224 | tf_op jit(solution)/shard_map/ppermute | solution.py:351
  85.8 10.0 %collective-permute-start.33 = (bf16[128,512]{1,0:T(8,128)(2,1)S(1)}, bf16[128,512]{1,0:T(8,128)(2,1)}, u32[]{:S(2)}, u32[]{:S(2)}) collective-permute-start(bf16[128,512]{1,0:T(8,128)(2,1)S(1)} %shard_map.206.refs_0_), channel_id=1, source_target_pairs={{0,1},{1,0},{2,3},{3,2},{4,5},{5,4},{6,7},{7,6},{8,9},{9,8},{10,11... | collective-permute-start | bytes 393224 | tf_op jit(solution)/shard_map/ppermute | solution.py:354
  90.6 6.4 %collective-permute-start.35 = (bf16[128,512]{1,0:T(8,128)(2,1)}, bf16[128,512]{1,0:T(8,128)(2,1)}, u32[]{:S(2)}, u32[]{:S(2)}) collective-permute-start(bf16[128,512]{1,0:T(8,128)(2,1)} %collective-permute-done.34.refs_2_), channel_id=1, source_target_pairs={{0,1},{1,0},{2,3},{3,2},{4,5},{5,4},{6,7},{7,6},{8,9},{9,8},{10,11... | collective-permute-start | bytes 393224 | tf_op jit(solution)/shard_map/ppermute | solution.py:354
  95.7 23.9 %collective-permute-start.46 = (bf16[256,512]{1,0:T(8,128)(2,1)}, bf16[256,512]{1,0:T(8,128)(2,1)S(1)}, u32[]{:S(2)}, u32[]{:S(2)}) collective-permute-start(bf16[256,512]{1,0:T(8,128)(2,1)} %collective-permute-done.45.refs_2_), channel_id=1, source_target_pairs={{0,8},{4,12},{8,16},{12,20},{16,24},{20,28},{24,0},{28,4},{1,9},{5... | collective-permute-start | bytes 786440 | tf_op jit(solution)/shard_map/ppermute | solution.py:348
  98.1 14.0 %collective-permute-start.36 = (bf16[256,256]{1,0:T(8,128)(2,1)S(1)}, bf16[256,256]{1,0:T(8,128)(2,1)S(1)}, u32[]{:S(2)}, u32[]{:S(2)}) collective-permute-start(bf16[256,256]{1,0:T(8,128)(2,1)S(1)} %get-tuple-element.104), channel_id=1, source_target_pairs={{0,4},{4,0},{8,12},{12,8},{16,20},{20,16},{24,28},{28,24},{1,5},{5... | collective-permute-start | bytes 393224 | tf_op jit(solution)/shard_map/ppermute | solution.py:348
  106.1 10.3 %copy-start.12 = (bf16[256,704]{1,0:T(8,128)(2,1)S(1)}, bf16[256,704]{1,0:T(8,128)(2,1)}, u32[]{:S(2)}) copy-start(bf16[256,704]{1,0:T(8,128)(2,1)} %copy-done.11) | copy-start | bytes 1081348
  106.2 10.3 %copy-start.14 = (bf16[256,704]{1,0:T(8,128)(2,1)S(1)}, bf16[256,704]{1,0:T(8,128)(2,1)}, u32[]{:S(2)}) copy-start(bf16[256,704]{1,0:T(8,128)(2,1)} %copy-done.13) | copy-start | bytes 1081348
  108.7 16.1 %collective-permute-start.47 = (bf16[1,512]{1,0:T(2,128)(2,1)S(1)}, bf16[1,512]{1,0:T(2,128)(2,1)S(1)}, u32[]{:S(2)}, u32[]{:S(2)}) collective-permute-start(bf16[1,512]{1,0:T(2,128)(2,1)S(1)} %get-tuple-element.117), channel_id=1, source_target_pairs={{0,4},{4,8},{8,12},{12,16},{16,20},{20,24},{24,28},{1,5},{5,9},{9,... | collective-permute-start | bytes 3080 | tf_op jit(solution)/shard_map/ppermute | solution.py:489
  112.1 14.8 %collective-permute-start.37 = (bf16[128,256]{1,0:T(8,128)(2,1)S(1)}, bf16[128,256]{1,0:T(8,128)(2,1)S(1)}, u32[]{:S(2)}, u32[]{:S(2)}) collective-permute-start(bf16[128,256]{1,0:T(8,128)(2,1)S(1)} %get-tuple-element.106), channel_id=1, source_target_pairs={{0,8},{4,12},{8,16},{12,20},{16,24},{20,28},{24,0},{28,4},{1,9},{5... | collective-permute-start | bytes 196616 | tf_op jit(solution)/shard_map/ppermute | solution.py:348
  112.5 14.5 %collective-permute-start.38 = (bf16[128,256]{1,0:T(8,128)(2,1)S(1)}, bf16[128,256]{1,0:T(8,128)(2,1)S(1)}, u32[]{:S(2)}, u32[]{:S(2)}) collective-permute-start(bf16[128,256]{1,0:T(8,128)(2,1)S(1)} %get-tuple-element.107), channel_id=1, source_target_pairs={{0,16},{4,20},{8,24},{12,28},{16,0},{20,4},{24,8},{28,12},{1,17},{... | collective-permute-start | bytes 196616 | tf_op jit(solution)/shard_map/ppermute | solution.py:348
  116.2 11.3 %collective-permute-start.39 = (bf16[128,256]{1,0:T(8,128)(2,1)S(1)}, bf16[128,256]{1,0:T(8,128)(2,1)S(1)}, u32[]{:S(2)}, u32[]{:S(2)}) collective-permute-start(bf16[128,256]{1,0:T(8,128)(2,1)S(1)} %get-tuple-element.108), channel_id=1, source_target_pairs={{0,24},{4,28},{8,0},{12,4},{16,8},{20,12},{24,16},{28,20},{1,25},{... | collective-permute-start | bytes 196616 | tf_op jit(solution)/shard_map/ppermute | solution.py:348
  116.5 11.1 %copy-start.8 = (bf16[256,704]{1,0:T(8,128)(2,1)S(1)}, bf16[256,704]{1,0:T(8,128)(2,1)}, u32[]{:S(2)}) copy-start(bf16[256,704]{1,0:T(8,128)(2,1)} %copy-done.7) | copy-start | bytes 1081348
  116.5 11.1 %copy-start.10 = (bf16[256,704]{1,0:T(8,128)(2,1)S(1)}, bf16[256,704]{1,0:T(8,128)(2,1)}, u32[]{:S(2)}) copy-start(bf16[256,704]{1,0:T(8,128)(2,1)} %copy-done.9) | copy-start | bytes 1081348
  119.6 11.1 %copy-start.25 = (bf16[256,512]{1,0:T(8,128)(2,1)}, bf16[256,512]{1,0:T(8,128)(2,1)S(1)}, u32[]{:S(2)}) copy-start(bf16[256,512]{1,0:T(8,128)(2,1)S(1)} %collective-permute-done.46.refs_3_) | copy-start | bytes 786436
  119.6 12.3 %collective-permute-start.48 = (bf16[1,512]{1,0:T(2,128)(2,1)S(1)}, bf16[1,512]{1,0:T(2,128)(2,1)S(1)}, u32[]{:S(2)}, u32[]{:S(2)}) collective-permute-start(bf16[1,512]{1,0:T(2,128)(2,1)S(1)} %get-tuple-element.118), channel_id=1, source_target_pairs={{4,0},{8,4},{12,8},{16,12},{20,16},{24,20},{28,24},{5,1},{9,5},{13... | collective-permute-start | bytes 3080 | tf_op jit(solution)/shard_map/ppermute | solution.py:490
  124.8 8.0 %collective-permute-start.40 = (bf16[128,256]{1,0:T(8,128)(2,1)S(1)}, bf16[128,256]{1,0:T(8,128)(2,1)S(1)}, u32[]{:S(2)}, u32[]{:S(2)}) collective-permute-start(bf16[128,256]{1,0:T(8,128)(2,1)S(1)} %get-tuple-element.105.refs_0_), channel_id=1, source_target_pairs={{0,1},{1,0},{2,3},{3,2},{4,5},{5,4},{6,7},{7,6},{8,9},{9,8},{10,11... | collective-permute-start | bytes 196616 | tf_op jit(solution)/shard_map/ppermute | solution.py:354
  127.0 5.9 %collective-permute-start.41 = (bf16[128,256]{1,0:T(8,128)(2,1)S(1)}, bf16[128,256]{1,0:T(8,128)(2,1)S(1)}, u32[]{:S(2)}, u32[]{:S(2)}) collective-permute-start(bf16[128,256]{1,0:T(8,128)(2,1)S(1)} %collective-permute-done.37.refs_1_), channel_id=1, source_target_pairs={{0,1},{1,0},{2,3},{3,2},{4,5},{5,4},{6,7},{7,6},{8,9},{9,8},{10,11... | collective-permute-start | bytes 196616 | tf_op jit(solution)/shard_map/ppermute | solution.py:354
  127.0 5.8 %collective-permute-start.42 = (bf16[128,256]{1,0:T(8,128)(2,1)S(1)}, bf16[128,256]{1,0:T(8,128)(2,1)S(1)}, u32[]{:S(2)}, u32[]{:S(2)}) collective-permute-start(bf16[128,256]{1,0:T(8,128)(2,1)S(1)} %collective-permute-done.38.refs_2_), channel_id=1, source_target_pairs={{0,1},{1,0},{2,3},{3,2},{4,5},{5,4},{6,7},{7,6},{8,9},{9,8},{10,11... | collective-permute-start | bytes 196616 | tf_op jit(solution)/shard_map/ppermute | solution.py:354
  127.5 5.4 %collective-permute-start.43 = (bf16[128,256]{1,0:T(8,128)(2,1)S(1)}, bf16[128,256]{1,0:T(8,128)(2,1)S(1)}, u32[]{:S(2)}, u32[]{:S(2)}) collective-permute-start(bf16[128,256]{1,0:T(8,128)(2,1)S(1)} %collective-permute-done.39.refs_3_), channel_id=1, source_target_pairs={{0,1},{1,0},{2,3},{3,2},{4,5},{5,4},{6,7},{7,6},{8,9},{9,8},{10,11... | collective-permute-start | bytes 196616 | tf_op jit(solution)/shard_map/ppermute | solution.py:354
  (12 other events, 21.6 us)
